TPU v7x, 512 devices: a whole 4x4x16 slice. The times are simulated.
512 devices in a mesh: sp: 16 (over y, x), tp: 32 (over z, core).
Axes of the slice: x: 4, y: 4, z: 16, core: 2. Of those that a mesh axis runs over, the one named last changes fastest.
Arguments:
- stream: bfloat16 [8192, 4096], P('sp', 'tp'), may hold values from -6 to 6
- gain_first: bfloat16 [4096], P('tp'), may hold values from 0.099609375 to 1.8984375
- query_first: bfloat16 [4096, 4096], P('sp', 'tp'), may hold values from -0.09375 to 0.09375
- key_first: bfloat16 [4096, 4096], P('sp', 'tp'), may hold values from -0.09375 to 0.09375
- value_first: bfloat16 [4096, 4096], P('sp', 'tp'), may hold values from -0.09375 to 0.09375
- offset_first: float32 [32, 15, 31], P('tp'), may hold values from -4 to 254
- gain_second: bfloat16 [4096], P('tp'), may hold values from 0.099609375 to 1.8984375
- query_second: bfloat16 [4096, 4096], P('sp', 'tp'), may hold values from -0.09375 to 0.09375
- key_second: bfloat16 [4096, 4096], P('sp', 'tp'), may hold values from -0.09375 to 0.09375
- value_second: bfloat16 [4096, 4096], P('sp', 'tp'), may hold values from -0.09375 to 0.09375
- offset_second: float32 [32, 15, 31], P('tp'), may hold values from -4 to 254
Outputs:
- result: bfloat16 [8192, 4096], P('sp', 'tp')
All inputs are finite; a program needn't handle non-finite values.
Results may differ from a plain program's by a relative error of at most 0.008.
Values may be sent and summed in bfloat16 or wider, within the bound.
No kernel may reach another device: no remote copies, remote signals or barrier semaphores. Data moves between devices by JAX's collectives and lax.ppermute only.
A program may use at most 64 MiB of HBM per device.

v0:
```python
import jax
import jax.numpy as jnp
import numpy as np
from jax import lax
from jax.sharding import PartitionSpec as P

GRID_W = 64


epsilon = 1e-06


def turned_gather(arrays, axis, dims):
    turned = [jnp.moveaxis(a, dim, 0) for a, dim in zip(arrays, dims)]
    both = jnp.concatenate([t.reshape(len(t), -1) for t in turned], axis=1)
    filled, at, gathered = (lax.all_gather(both, axis, axis=0, tiled=True), 0, [])
    for t, dim in zip(turned, dims):
        section = filled[:, at : at + t[0].size].reshape(-1, *t.shape[1:])
        gathered.append(jnp.moveaxis(section, 0, dim))
        at += t[0].size
    return tuple(gathered)


def padded_2(block, sides, width):
    for axis, dim in sides:
        count = lax.axis_size(axis)
        forward = [(i, i + 1) for i in range(count - 1)]
        backward = [(target, source) for source, target in forward]
        low = lax.ppermute(
            lax.slice_in_dim(block, block.shape[dim] - width, None, axis=dim), axis, forward
        )
        high = lax.ppermute(lax.slice_in_dim(block, 0, width, axis=dim), axis, backward)
        block = jnp.concatenate([low, block, high], axis=dim)
    return block


def sent_together(arrays, axis, dim, along):
    ends, at = ([], 0)
    for a in arrays[:-1]:
        at += a.shape[along]
        ends.append(at)
    both = jnp.concatenate(arrays, axis=along)
    return tuple(jnp.split(lax.all_gather(both, axis, axis=dim, tiled=True), ends, axis=along))


def attend(query, keys, values, table, row_start, total_rows):
    rows_here, width, heads, head_size = query.shape
    blocks = width // 16
    query_cols = np.arange(width).reshape(blocks, 16)
    window_start = np.clip(query_cols - 8, 0, width - 16)
    key_cols = np.clip(np.arange(blocks) * 16 - 8, 0, width - 32)[:, None] + np.arange(32)
    column_ok = (key_cols[:, None, :] >= window_start[:, :, None]) & (
        key_cols[:, None, :] < window_start[:, :, None] + 16
    )
    column_offset = np.clip(key_cols[:, None, :] - query_cols[:, :, None] + 15, 0, 30)
    column_bias = table[:, :, column_offset]
    mask = jnp.asarray(column_ok)[None, :, :, None, :]
    factor = head_size ** (-0.5)

    def one_row(index):
        grid_row = row_start + index
        first = jnp.clip(grid_row - 4, 0, total_rows - 8)
        local = first - row_start + 4
        key_block = lax.dynamic_slice_in_dim(keys, local, 8, 0)[:, key_cols]
        value_block = lax.dynamic_slice_in_dim(values, local, 8, 0)[:, key_cols]
        query_row = lax.dynamic_index_in_dim(query, index, 0, keepdims=False).reshape(
            blocks, 16, heads, head_size
        )
        scores = (
            jnp.einsum(
                "jqhe,mjkhe->hjqmk", query_row, key_block, preferred_element_type=jnp.float32
            )
            * factor
        )
        row_offset = first + jnp.arange(8, dtype=jnp.int32) - grid_row + 7
        row_bias = jnp.transpose(jnp.take(column_bias, row_offset, axis=1), (0, 2, 3, 1, 4))
        scores = jnp.where(mask, scores + row_bias, -1e30)
        weight = jax.nn.softmax(scores.reshape(heads, blocks, 16, 256), axis=-1)
        rounded = weight.astype(jnp.bfloat16).reshape(heads, blocks, 16, 8, 32)
        output = jnp.einsum(
            "hjqmk,mjkhe->jqhe", rounded, value_block, preferred_element_type=jnp.float32
        )
        return output.reshape(width, heads * head_size)

    return jax.vmap(one_row)(jnp.arange(rows_here, dtype=jnp.int32))


def layer(stream, gain, table, whole_weights):
    tokens_dev, local_width = stream.shape
    widened = stream.astype(jnp.float32)
    full_rows, full_gain = turned_gather((stream, gain), "tp", (1, 0))
    full_wide = full_rows.astype(jnp.float32)
    mean_square = jnp.mean(full_wide * full_wide, axis=-1, keepdims=True)
    normed = (full_wide * lax.rsqrt(mean_square + epsilon) * full_gain.astype(jnp.float32)).astype(
        jnp.bfloat16
    )
    query = jnp.dot(normed, whole_weights[0], preferred_element_type=jnp.float32)
    key_part = jnp.dot(normed, whole_weights[1], preferred_element_type=jnp.float32)
    value_part = jnp.dot(normed, whole_weights[2], preferred_element_type=jnp.float32)
    heads_dev = table.shape[0]
    rows_dev = tokens_dev // GRID_W
    shape = (rows_dev, GRID_W, heads_dev, local_width // heads_dev)
    query = query.astype(jnp.bfloat16).reshape(shape)
    paired = jnp.stack(
        [
            key_part.astype(jnp.bfloat16).reshape(shape),
            value_part.astype(jnp.bfloat16).reshape(shape),
        ]
    )
    padded = padded_2(paired, (("sp", 1),), 4)
    row_start = lax.axis_index("sp") * rows_dev
    output = attend(query, padded[0], padded[1], table, row_start, rows_dev * lax.axis_size("sp"))
    return (widened + output.reshape(tokens_dev, local_width)).astype(jnp.bfloat16)


def body(
    stream,
    gain_first,
    query_first,
    key_first,
    value_first,
    offset_first,
    gain_second,
    query_second,
    key_second,
    value_second,
    offset_second,
):
    fetched = sent_together(
        (query_first, key_first, value_first, query_second, key_second, value_second), "sp", 0, 1
    )
    first_set = fetched[:3]
    second_set = fetched[3:]
    middle = layer(stream, gain_first, offset_first, first_set)
    return layer(middle, gain_second, offset_second, second_set)


def solution(mesh):
    placed = (
        P("sp", "tp"),
        P("tp"),
        P("sp", "tp"),
        P("sp", "tp"),
        P("sp", "tp"),
        P("tp", None, None),
        P("tp"),
        P("sp", "tp"),
        P("sp", "tp"),
        P("sp", "tp"),
        P("tp", None, None),
    )
    return jax.shard_map(body, mesh=mesh, in_specs=placed, out_specs=P("sp", "tp"), check_vma=False)
```

profile of v0, /device:TPU:6, one launch (start us, length us, event | category | flops | bytes accessed | tf_op | source)
XLA Modules:
  0.0 339.2 jit_solution(11450175371349849308)
XLA Ops:
  6.5 1.6 pad_maximum_fusion.2
  8.2 0.9 constant_dynamic-update-slice_fusion.5
  9.1 0.9 constant_dynamic-update-slice_fusion.4
  9.9 0.9 constant_dynamic-update-slice_fusion.3
  10.8 0.9 constant_dynamic-update-slice_fusion.2
  11.7 0.9 constant_dynamic-update-slice_fusion.1
  12.5 0.9 constant_dynamic-update-slice_fusion
  14.4 0.8 copy.40
  15.9 5.5 %gather_fusion.5 = f32[2048,15]{1,0:T(8,128)S(1)} fusion(f32[15,31]{0,1:T(8,128)S(1)} %bitcast.128, s32[2048]{0:T(1024)S(1)} %broadcast_clamp_fusion), kind=kCustom, calls=%fused_computation.7 | custom fusion | bytes 253952 | tf_op jit(solution)/shard_map/gather | solution.py:56
  22.0 2.0 gather_fusion.12
  24.1 70.7 %all-gather.4.cloned.1.call-done = bf16[4096,513]{0,1:T(8,128)(2,1)} async-done(((bf16[128,513]{0,1:T(8,128)(2,1)}), bf16[4096,513]{0,1:T(8,128)(2,1)}) %all-gather.4.cloned.1.call-update) | async-done | bytes 4202512 | tf_op jit(solution)/shard_map/all_gather | solution.py:16
  94.8 3.1 fusion
  97.9 0.9 slice_convert_fusion.1
  98.7 5.9 %fusion.2 = bf16[4096,512]{0,1:T(8,128)(2,1)} fusion(f32[4096]{0:T(1024)S(1)} %bitcast.154, f32[512]{0:T(512)S(1)} %add_rsqrt_fusion.1, bf16[4096,513]{0,1:T(8,128)(2,1)} %all-gather.4.cloned.1.call-done), kind=kLoop, calls=%fused_computation.20 | loop fusion | flops 8388608 | bytes 8407040 | tf_op jit(solution)/shard_map/convert_element_type | solution.py:94
  104.6 65.2 %all-gather.6.cloned.1.call-done = bf16[4096,768]{1,0:T(8,128)(2,1)} async-done(((bf16[256,768]{1,0:T(8,128)(2,1)}), bf16[4096,768]{1,0:T(8,128)(2,1)}) %all-gather.6.cloned.1.call-update) | async-done | bytes 6291472 | tf_op jit(solution)/shard_map/all_gather | solution.py:43
  169.8 3.9 %convolution_convert_fusion.5 = bf16[512,128]{1,0:T(8,128)(2,1)S(1)} fusion(bf16[4096,512]{0,1:T(8,128)(2,1)} %fusion.2, bf16[4096,768]{1,0:T(8,128)(2,1)} %all-gather.6.cloned.1.call-done), kind=kOutput, calls=%fused_computation.53 | convolution fusion | flops 536936448 | bytes 5373952 | tf_op jit(solution)/shard_map/dot_general | solution.py:98
  173.7 2.5 convolution_convert_fusion.4
  176.2 3.3 collective-permute-start
  179.5 2.7 collective-permute-start.1
  182.3 2.5 convolution_convert_fusion.3
  185.3 3.2 collective-permute-done.1
  188.6 0.8 gather_fusion.3
  191.6 2.6 gather_fusion.4
  194.1 2.6 gather_fusion.1
  196.7 5.2 %fusion.41 = (f32[8,4,16]{2,1,0:T(4,128)S(1)}, f32[8,1,4,16,8,32]{5,3,4,2,0,1:T(8,128)S(1)}) fusion(f32[8,1,8,4,16,32]{5,4,3,2,0,1:T(8,128)} %bitcast.132, pred[8,8]{1,0:T(8,128)(4,1)S(1)} %compare_and_fusion, bf16[8,4,16,128,1]{3,2,4,1,0:T(8,128)(2,1)S(1)} %bitcast.142, bf16[4,32,8,8,128]{4,3,2,1,0:T(8,128)(2,1)} %bitcast.135, ...), kind=kOutput, calls=%fused_computation.105 | convolution fusion | flops 34209280 | bytes 3280960 | tf_op jit(solution)/shard_map/vmap(jqhe,mjkhe->hjqmk)/dot_general | solution.py:70
  202.4 1.1 copy-done.2
  203.5 2.0 fusion.14
  206.3 5.6 %gather_fusion.11 = f32[2048,15]{1,0:T(8,128)S(1)} fusion(f32[15,31]{0,1:T(8,128)S(1)} %bitcast.129, s32[2048]{0:T(1024)S(1)} %broadcast_clamp_fusion), kind=kCustom, calls=%fused_computation.13 | custom fusion | bytes 253952 | tf_op jit(solution)/shard_map/gather | solution.py:56
  213.3 74.9 %all-gather.8.cloned.1.call-done = bf16[4096,513]{0,1:T(8,128)(2,1)} async-done(((bf16[128,513]{0,1:T(8,128)(2,1)}), bf16[4096,513]{0,1:T(8,128)(2,1)}) %all-gather.8.cloned.1.call-update) | async-done | bytes 4202512 | tf_op jit(solution)/shard_map/all_gather | solution.py:16
  288.1 3.2 fusion.3
  291.4 0.9 slice_convert_fusion
  292.2 4.0 %fusion.5 = bf16[4096,512]{0,1:T(8,128)(2,1)S(1)} fusion(f32[4096]{0:T(1024)S(1)} %bitcast.155, f32[512]{0:T(512)S(1)} %add_rsqrt_fusion, bf16[4096,513]{0,1:T(8,128)(2,1)} %all-gather.8.cloned.1.call-done), kind=kLoop, calls=%fused_computation.23 | loop fusion | flops 8388608 | bytes 8407040 | tf_op jit(solution)/shard_map/convert_element_type | solution.py:94
  296.2 1.2 convolution_convert_fusion.1
  297.5 1.2 convolution_convert_fusion.2
  298.8 3.4 collective-permute-start.2
  302.2 2.7 collective-permute-start.3
  304.9 1.2 convolution_convert_fusion
  306.1 1.2 gather_fusion.8
  307.4 4.1 %collective-permute-done.3 = bf16[2,4,64,1,128]{4,2,1,3,0:T(8,128)(2,1)S(1)} collective-permute-done((bf16[2,4,64,1,128]{4,2,1,3,0:T(8,128)(2,1)S(1)}, bf16[2,4,64,1,128]{4,2,1,3,0:T(8,128)(2,1)S(1)}, u32[]{:S(2)}, u32[]{:S(2)}) %collective-permute-start.3) | collective-permute-done | bytes 131104 | tf_op jit(solution)/shard_map/ppermute | solution.py:32
  311.6 1.7 gather_fusion.9
  313.3 1.9 copy.47
  315.2 2.5 gather_fusion.10
  317.8 1.6 gather_fusion.6
  319.4 1.9 copy.43
  321.4 2.5 gather_fusion.7
  323.9 4.5 %fusion.42 = (f32[8,4,16]{2,1,0:T(4,128)S(1)}, f32[8,1,4,16,8,32]{5,3,4,2,0,1:T(8,128)S(1)}) fusion(f32[8,1,8,4,16,32]{5,4,3,2,0,1:T(8,128)S(1)} %bitcast.133, pred[8,8]{1,0:T(8,128)(4,1)S(1)} %copy-done.9, bf16[8,4,16,128,1]{3,2,4,1,0:T(8,128)(2,1)S(1)} %bitcast.141, bf16[4,32,8,8,128]{4,3,2,1,0:T(8,128)(2,1)} %bitcast.134, ...), kind=kOutput, calls=%fused_computation.106 | convolution fusion | flops 34209280 | bytes 3280960 | tf_op jit(solution)/shard_map/vmap(jqhe,mjkhe->hjqmk)/dot_general | solution.py:70
  329.0 1.1 copy-done.1
  330.0 2.0 fusion.9
  (67 shorter events, 9.4 us)
Async XLA Ops:
  6.5 88.3 %all-gather.4.cloned.1.call-start = ((), (), s32[]{:S(2)}) async-start(), calls=%async_computation | async-start | bytes 4392960 | tf_op jit(solution)/shard_map/all_gather | solution.py:16
  8.2 161.6 %all-gather.6.cloned.1.call-start = ((), (), s32[]{:S(2)}) async-start(), calls=%async_computation.1 | async-start | bytes 6684672 | tf_op jit(solution)/shard_map/all_gather | solution.py:43
  13.4 0.7 copy-start.3
  14.2 274.0 %all-gather.8.cloned.1.call-start = ((), (), s32[]{:S(2)}) async-start(), calls=%async_computation.2 | async-start | bytes 4392960 | tf_op jit(solution)/shard_map/all_gather | solution.py:16
  22.0 2.0 copy-start.12
  24.1 172.6 %copy-start.8 = (pred[8,8]{1,0:T(8,128)(4,1)}, pred[8,8]{1,0:T(8,128)(4,1)S(1)}, u32[]{:S(2)}) copy-start(pred[8,8]{1,0:T(8,128)(4,1)S(1)} %compare_and_fusion) | copy-start | bytes 196
  169.8 3.9 %copy-start = (bf16[4096,512]{0,1:T(8,128)(2,1)S(1)}, bf16[4096,512]{0,1:T(8,128)(2,1)}, u32[]{:S(2)}) copy-start(bf16[4096,512]{0,1:T(8,128)(2,1)} %fusion.2) | copy-start | bytes 12582916
  176.2 9.1 %collective-permute-start = (bf16[2,4,64,1,128]{4,2,1,3,0:T(8,128)(2,1)S(1)}, bf16[2,4,64,1,128]{4,2,1,3,0:T(8,128)(2,1)S(1)}, u32[]{:S(2)}, u32[]{:S(2)}) collective-permute-start(bf16[2,4,64,1,128]{4,2,1,3,0:T(8,128)(2,1)S(1)} %get-tuple-element.12), channel_id=1, source_target_pairs={{0,32},{32,64},{64,96},{96,128},{128,160},{160,192},{192,224},{224... | collective-permute-start | bytes 393224 | tf_op jit(solution)/shard_map/ppermute | solution.py:29
  179.5 9.0 %collective-permute-start.1 = (bf16[2,4,64,1,128]{4,2,1,3,0:T(8,128)(2,1)S(1)}, bf16[2,4,64,1,128]{4,2,1,3,0:T(8,128)(2,1)S(1)}, u32[]{:S(2)}, u32[]{:S(2)}) collective-permute-start(bf16[2,4,64,1,128]{4,2,1,3,0:T(8,128)(2,1)S(1)} %get-tuple-element.13), channel_id=1, source_target_pairs={{32,0},{64,32},{96,64},{128,96},{160,128},{192,160},{224,192},{256... | collective-permute-start | bytes 393224 | tf_op jit(solution)/shard_map/ppermute | solution.py:32
  194.1 2.6 copy-start.6
  201.9 1.6 copy-start.2
  203.5 2.0 copy-start.5
  203.5 2.0 copy-start.11
  203.5 2.7 copy-start.10
  288.1 8.1 %slice-start = ((s8[6291456]{0:T(1024)(128)(4,1)}), s8[4194304]{0:T(1024)(128)(4,1)S(1)}, s32[]{:S(2)}) async-start(s8[6291456]{0:T(1024)(128)(4,1)} %bitcast.158), calls=%async_computation.3 | async-start | bytes 8388608
  292.2 4.0 %slice-start.1 = ((s8[6291456]{0:T(1024)(128)(4,1)}), s8[2097152]{0:T(1024)(128)(4,1)S(1)}, s32[]{:S(2)}) async-start(s8[6291456]{0:T(1024)(128)(4,1)} %bitcast.158), calls=%async_computation.4 | async-start | bytes 4194304
  298.8 8.6 %collective-permute-start.2 = (bf16[2,4,64,1,128]{4,2,1,3,0:T(8,128)(2,1)S(1)}, bf16[2,4,64,1,128]{4,2,1,3,0:T(8,128)(2,1)S(1)}, u32[]{:S(2)}, u32[]{:S(2)}) collective-permute-start(bf16[2,4,64,1,128]{4,2,1,3,0:T(8,128)(2,1)S(1)} %get-tuple-element.10), channel_id=1, source_target_pairs={{0,32},{32,64},{64,96},{96,128},{128,160},{160,192},{192,224},{224... | collective-permute-start | bytes 393224 | tf_op jit(solution)/shard_map/ppermute | solution.py:29
  302.2 9.4 %collective-permute-start.3 = (bf16[2,4,64,1,128]{4,2,1,3,0:T(8,128)(2,1)S(1)}, bf16[2,4,64,1,128]{4,2,1,3,0:T(8,128)(2,1)S(1)}, u32[]{:S(2)}, u32[]{:S(2)}) collective-permute-start(bf16[2,4,64,1,128]{4,2,1,3,0:T(8,128)(2,1)S(1)} %get-tuple-element.11), channel_id=1, source_target_pairs={{32,0},{64,32},{96,64},{128,96},{160,128},{192,160},{224,192},{256... | collective-permute-start | bytes 393224 | tf_op jit(solution)/shard_map/ppermute | solution.py:32
  321.3 2.6 copy-start.4
  321.3 2.5 copy-start.7
  321.3 2.5 copy-start.9
  328.4 1.6 copy-start.1
Sparse Core Ops, SparseCore 0:
  9.4 85.3 all-gather.3
  97.8 71.9 all-gather.5
  206.4 81.7 all-gather.7
where the time goes:
time: 340 us; the launch traced here: 339 us
  waiting for transfers between devices  218 us (64%)
  local copies, waits for them, and re-layouts  46.2 us (14%)
  matrix products  26.2 us (8%)
  other arithmetic  23.1 us (7%)
  between operations  13.5 us (4%)
  starting transfers between devices  12.2 us (4%)
    all_gather x2, waiting for transfers between devices, turned_gather(): lax.all_gather(both, axis, axis=0, tiled=True)  146 us
    all_gather x1, waiting for transfers between devices, sent_together(): lax.all_gather(both, axis, axis=dim, tiled=True)  65.2 us
    gather x4, local copies, waits for them, and re-layouts, attend(): column_bias = table[:, :, column_offset]  12.3 us
    gather x6, local copies, waits for them, and re-layouts, one_row(): key_block = lax.dynamic_slice_in_dim(keys, local, 8, 0)[:, key_cols]  10.2 us
    gather x6, local copies, waits for them, and re-layouts, one_row(): value_block = lax.dynamic_slice_in_dim(values, local, 8, 0)[:, key_cols]  10.1 us
    convert_element_type x2, other arithmetic, layer(): (full_wide * lax.rsqrt(mean_square + epsilon) * full_gain.astype(jnp.floa...  9.88 us
    dot_general x2, matrix products, one_row(): jnp.einsum('jqhe,mjkhe->hjqmk', query_row, key_block, preferred_element_t...  9.71 us
    unnamed x37, local copies, waits for them, and re-layouts  8.13 us
  transfers between devices with their start and end apart: 7, of which 5 were waited for; matrix products, arithmetic and copies ran while one was open for 11% of the time, Pallas kernels for 0%

commit v1 on v0

v1 whole, which is shorter than its diff:
```python
import functools

import jax
import jax.numpy as jnp
import numpy as np
from jax import lax
from jax.experimental import pallas as pl
from jax.experimental.pallas import tpu as pltpu
from jax.sharding import PartitionSpec as P

GRID_W = 64
EPSILON = 1e-06
SCALE_FIRST = 2.0**13
SCALE_SECOND = 2.0**6
WINDOW_ROWS = 8
HALO = 4
MASKED = -1e30


def vmem():
    return pl.BlockSpec(memory_space=pltpu.VMEM)


def bias_kernel(first_ref, second_ref, first_out, second_out):
    width = GRID_W
    col = lax.broadcasted_iota(jnp.int32, (width, 2 * width), 0)
    key = lax.broadcasted_iota(jnp.int32, (width, 2 * width), 1) % width
    start = jnp.clip(col - 8, 0, width - 16)
    inside = (key >= start) & (key < start + 16)
    for table_ref, out_ref in ((first_ref, first_out), (second_ref, second_out)):
        table = table_ref[0]
        low = jnp.pad(table, ((0, 1), (0, 2 * width - 31)))
        both = low + pltpu.roll(pltpu.roll(low, 15, 0), width, 1)
        for m in range(14):
            row = jnp.broadcast_to(both[m : m + 1, :], (width, 2 * width))
            turned = pltpu.roll(row, 2 * width - 15, 1, stride=1, stride_axis=0)
            out_ref[m] = jnp.where(inside, turned, MASKED)


def biases(first, second):
    shape = jax.ShapeDtypeStruct((14, GRID_W, 2 * GRID_W), jnp.float32)
    return pl.pallas_call(
        bias_kernel,
        out_shape=(shape, shape),
        in_specs=[vmem(), vmem()],
        out_specs=(vmem(), vmem()),
        name="biases",
    )(first, second)


def project_kernel(x_ref, gain_ref, w_ref, q_ref, k_ref, v_ref, normed):
    blocks, tokens, size = x_ref.shape
    total = jnp.zeros((tokens, size), jnp.float32)
    for f in range(blocks):
        part = x_ref[f].astype(jnp.float32)
        total = total + part * part
    mean = jnp.sum(total, axis=1, keepdims=True) * (1.0 / (blocks * size))
    rate = lax.rsqrt(mean + EPSILON)
    for f in range(blocks):
        part = x_ref[f].astype(jnp.float32)
        gain = gain_ref[f : f + 1, :].astype(jnp.float32)
        normed[:, f * size : (f + 1) * size] = (part * rate * gain).astype(jnp.bfloat16)
    half = tokens // 2
    for t in range(2):
        rows = slice(t * half, (t + 1) * half)
        out = jnp.dot(normed[rows, :], w_ref[...], preferred_element_type=jnp.float32)
        out = out.astype(jnp.bfloat16)
        q_ref[rows, :] = out[:, :size]
        k_ref[rows, :] = out[:, size : 2 * size]
        v_ref[rows, :] = out[:, 2 * size :]


def project(x, gain, weights):
    blocks, tokens, size = x.shape
    shape = jax.ShapeDtypeStruct((tokens, size), jnp.bfloat16)
    return pl.pallas_call(
        project_kernel,
        out_shape=(shape,) * 3,
        in_specs=[vmem()] * 3,
        out_specs=(vmem(),) * 3,
        scratch_shapes=[pltpu.VMEM((tokens, blocks * size), jnp.bfloat16)],
        cost_estimate=pl.CostEstimate(
            flops=2 * tokens * blocks * size * 3 * size, bytes_accessed=8 << 20, transcendentals=0
        ),
        name="project",
    )(x, gain, weights)


def attend_kernel(at_ref, q_ref, k_ref, v_ref, klo_ref, khi_ref, vlo_ref, vhi_ref, bias_ref, x_ref, out_ref, keys, values):
    width = GRID_W
    tokens, size = q_ref.shape
    rows = tokens // width
    edge = HALO * width
    keys[:edge] = klo_ref[...]
    keys[edge : edge + tokens] = k_ref[...]
    keys[edge + tokens :] = khi_ref[...]
    values[:edge] = vlo_ref[...]
    values[edge : edge + tokens] = v_ref[...]
    values[edge + tokens :] = vhi_ref[...]
    row_start, last = at_ref[0], at_ref[1]
    factor = size ** (-0.5)
    for r in range(rows):
        grid_row = row_start + r
        first = jnp.clip(grid_row - HALO, 0, last)
        at = pl.multiple_of((first - row_start + HALO) * width, width)
        offset = first - grid_row + 7
        span = pl.ds(at, WINDOW_ROWS * width)
        query = q_ref[r * width : (r + 1) * width, :]
        scores = lax.dot_general(
            query, keys[span, :], (((1,), (1,)), ((), ())), preferred_element_type=jnp.float32
        )
        parts = [
            scores[:, 2 * p * width : 2 * (p + 1) * width] * factor + bias_ref[offset + 2 * p]
            for p in range(WINDOW_ROWS // 2)
        ]
        top = functools.reduce(jnp.maximum, parts)
        top = jnp.max(top, axis=1, keepdims=True)
        parts = [jnp.exp(part - top) for part in parts]
        total = jnp.sum(functools.reduce(jnp.add, parts), axis=1, keepdims=True)
        weight = jnp.concatenate([(part / total).astype(jnp.bfloat16) for part in parts], axis=1)
        attended = jnp.dot(weight, values[span, :], preferred_element_type=jnp.float32)
        here = slice(r * width, (r + 1) * width)
        out_ref[here, :] = (x_ref[here, :].astype(jnp.float32) + attended).astype(jnp.bfloat16)


def attend(at, query, key, value, low, high, bias, x):
    tokens, size = query.shape
    long = tokens + 2 * HALO * GRID_W
    return pl.pallas_call(
        attend_kernel,
        out_shape=jax.ShapeDtypeStruct((tokens, size), jnp.bfloat16),
        in_specs=[pl.BlockSpec(memory_space=pltpu.SMEM)] + [vmem()] * 9,
        out_specs=vmem(),
        scratch_shapes=[pltpu.VMEM((long, size), jnp.bfloat16)] * 2,
        cost_estimate=pl.CostEstimate(
            flops=4 * tokens * size * WINDOW_ROWS * GRID_W, bytes_accessed=2 << 20, transcendentals=tokens * 512
        ),
        name="attend",
    )(at, query, key, value, low[0], high[0], low[1], high[1], bias, x)


def layer(x, gathered, gain, weights, bias, at):
    query, key, value = project(gathered, gain, weights)
    count = lax.axis_size("sp")
    forward = [(i, i + 1) for i in range(count - 1)]
    backward = [(target, source) for source, target in forward]
    edge = HALO * GRID_W
    low = lax.ppermute(jnp.stack([key[-edge:], value[-edge:]]), "sp", forward)
    high = lax.ppermute(jnp.stack([key[:edge], value[:edge]]), "sp", backward)
    return attend(at, query, key, value, low, high, bias, x)


def body(
    stream,
    gain_first,
    query_first,
    key_first,
    value_first,
    offset_first,
    gain_second,
    query_second,
    key_second,
    value_second,
    offset_second,
):
    tokens, size = stream.shape
    rows = tokens // GRID_W
    first_set = lax.all_gather(
        jnp.concatenate([query_first, key_first, value_first], 1), "sp", axis=0, tiled=True
    )
    second_set = lax.all_gather(
        jnp.concatenate([query_second, key_second, value_second], 1), "sp", axis=0, tiled=True
    )
    bias_first, bias_second = biases(offset_first, offset_second)
    start = lax.axis_index("sp") * rows
    total_rows = rows * lax.axis_size("sp")
    at = jnp.stack([start, jnp.int32(total_rows - WINDOW_ROWS)]).astype(jnp.int32)

    gains = jnp.pad(jnp.stack([gain_first, gain_second]), ((0, 14), (0, 0)))
    sent = (jnp.concatenate([stream, gains]).astype(jnp.float32) * SCALE_FIRST).astype(jnp.float16)
    held = lax.all_gather(sent, "tp", axis=0, tiled=False)
    held = (held.astype(jnp.float32) * (1.0 / SCALE_FIRST)).astype(jnp.bfloat16)
    middle = layer(stream, held[:, :tokens], held[:, tokens], first_set, bias_first, at)

    sent = (middle.astype(jnp.float32) * SCALE_SECOND).astype(jnp.float16)
    again = lax.all_gather(sent, "tp", axis=0, tiled=False)
    again = (again.astype(jnp.float32) * (1.0 / SCALE_SECOND)).astype(jnp.bfloat16)
    return layer(middle, again, held[:, tokens + 1], second_set, bias_second, at)


def solution(mesh):
    placed = (
        P("sp", "tp"),
        P("tp"),
        P("sp", "tp"),
        P("sp", "tp"),
        P("sp", "tp"),
        P("tp", None, None),
        P("tp"),
        P("sp", "tp"),
        P("sp", "tp"),
        P("sp", "tp"),
        P("tp", None, None),
    )
    return jax.shard_map(body, mesh=mesh, in_specs=placed, out_specs=P("sp", "tp"), check_vma=False)
```

time: 340 us -> 191 us (0.56)
  waiting for transfers between devices: 218 us -> 14 us
  blocking collectives: 0 us -> 96.3 us
  local copies, waits for them, and re-layouts: 46.2 us -> 11.5 us
  matrix products: 26.2 us -> 0 us
  Pallas kernels: 0 us -> 25.8 us
  other arithmetic: 23.1 us -> 10.2 us
  starting transfers between devices: 12.2 us -> 16.4 us
    all_gather x3 -> x2, waiting for transfers between devices: 211 us -> 8.4 us  [the longest x1 8.4 us: body(): lax.all_gather(jnp.concatenate([query_first, key_first, value_first], 1),...]
    all_gather x0 -> x2, blocking collectives: none -> 96.3 us  [the longest x1 50.7 us: body(): held = lax.all_gather(sent, 'tp', axis=0, tiled=False)]
    gather x20 -> x0, local copies, waits for them, and re-layouts: 37 us -> none  [the longest x4 12.3 us: attend(): column_bias = table[:, :, column_offset]]
    dot_general x10 -> x0, matrix products: 26.2 us -> none  [the longest x2 9.71 us: one_row(): jnp.einsum('jqhe,mjkhe->hjqmk', query_row, key_block, preferred_element_t...]
    pallas_call x0 -> x5, Pallas kernels: none -> 25.8 us  [the longest x2 14.2 us: project(): pl.pallas_call(project_kernel, out_shape=(shape,) * 3, in_specs=[vmem()]...]
    reduce_sum x4 -> x0, other arithmetic: 7.35 us -> none  [the longest x2 6.31 us: layer(): mean_square = jnp.mean(full_wide * full_wide, axis=-1, keepdims=True)]
    unnamed x37 -> x6, local copies, waits for them, and re-layouts: 8.13 us -> 1.2 us
    convert_element_type x6 -> x4, other arithmetic: 12.3 us -> 5.69 us  [the longest x1 2.41 us: body(): (again.astype(jnp.float32) * (1.0 / SCALE_SECOND)).astype(jnp.bfloat16)]
  transfers between devices with their start and end apart: 7 -> 6, of which waited for: 5 -> 4; matrix products, arithmetic and copies ran while one was open for 11% -> 9% of each run, Pallas kernels for 0% -> 7%
where the time goes in v1:
time: 191 us; the launch traced here: 188 us
  blocking collectives  96.3 us (50%)
  Pallas kernels  25.8 us (14%)
  starting transfers between devices  16.4 us (9%)
  waiting for transfers between devices  14 us (7%)
  between operations  13.5 us (7%)
  local copies, waits for them, and re-layouts  11.5 us (6%)
  other arithmetic  10.2 us (5%)
    all_gather x1, blocking collectives, body(): held = lax.all_gather(sent, 'tp', axis=0, tiled=False)  50.7 us
    all_gather x1, blocking collectives, body(): again = lax.all_gather(sent, 'tp', axis=0, tiled=False)  45.6 us
    pallas_call x2, Pallas kernels, project(): pl.pallas_call(project_kernel, out_shape=(shape,) * 3, in_specs=[vmem()]...  14.2 us
    ppermute x2, starting transfers between devices, layer(): low = lax.ppermute(jnp.stack([key[-edge:], value[-edge:]]), 'sp', forward)  11.9 us
    pallas_call x2, Pallas kernels, attend(): pl.pallas_call(attend_kernel, out_shape=jax.ShapeDtypeStruct((tokens, siz...  9.63 us
    all_gather x1, waiting for transfers between devices, body(): lax.all_gather(jnp.concatenate([query_first, key_first, value_first], 1),...  8.4 us
    ppermute x2, starting transfers between devices, layer(): high = lax.ppermute(jnp.stack([key[:edge], value[:edge]]), 'sp', backward)  4.48 us
    slice x2, local copies, waits for them, and re-layouts, body(): held[:, :tokens]  4.28 us
  transfers between devices with their start and end apart: 6, of which 4 were waited for; matrix products, arithmetic and copies ran while one was open for 9% of the time, Pallas kernels for 7%

profile of v1, /device:TPU:6, one launch (start us, length us, event | category | flops | bytes accessed | tf_op | source)
XLA Modules:
  0.0 187.7 jit_solution(12484852385495340766)
XLA Ops:
  6.5 0.0 all-gather.6.cloned.1.call-start
  6.5 1.6 pad_maximum_fusion
  8.2 0.0 all-gather.6.cloned.1.call-update
  8.2 0.0 all-gather.8.cloned.1.call-start
  8.2 1.6 pad_maximum_fusion.1
  9.9 0.0 all-gather.8.cloned.1.call-update
  9.9 0.7 fusion.3
  10.6 0.9 multiply_convert_fusion.2
  11.5 50.7 %all-gather.9 = f16[32,528,128]{2,1,0:T(8,128)(2,1)S(1)} all-gather(f16[1,528,128]{2,1,0:T(8,128)(2,1)S(1)} %multiply_convert_fusion.2), channel_id=1, replica_groups=mesh['sp'=16,'tp'=32] {'tp'}, dimensions={0}, use_global_device_ids=true | all-gather | bytes 4460544 | tf_op jit(solution)/shard_map/all_gather | solution.py:181
  62.2 1.4 multiply_convert_fusion
  63.6 0.6 slice_bitcast_fusion.16
  64.2 0.7 slice.76
  64.9 3.6 %copy.21.x_ref = bf16[32,512,128]{2,1,0:T(8,128)(2,1)} copy(bf16[32,512,128]{2,0,1:T(8,128)(2,1)S(1)} %slice.76) | data formatting | bytes 8388608 | tf_op jit(solution)/shard_map/slice | solution.py:183
  68.5 0.0 copy-start
  68.5 0.0 copy-start.1
  68.5 8.4 %all-gather.6.cloned.1.call-done.w_ref = bf16[4096,384]{1,0:T(8,128)(2,1)} async-done(((bf16[256,384]{1,0:T(8,128)(2,1)}), bf16[4096,384]{1,0:T(8,128)(2,1)}) %all-gather.6.cloned.1.call-update) | async-done | bytes 3145744 | tf_op jit(solution)/shard_map/all_gather | solution.py:168
  76.9 7.1 %project.2 = (bf16[512,128]{1,0:T(8,128)(2,1)}, bf16[512,128]{1,0:T(8,128)(2,1)}, bf16[512,128]{1,0:T(8,128)(2,1)}) custom-call(bf16[32,512,128]{2,1,0:T(8,128)(2,1)} %copy.21.x_ref, bf16[32,128]{1,0:T(8,128)(2,1)} %get-tuple-element.22.gain_ref, bf16[4096,384]{1,0:T(8,128)(2,1)} %all-gather.6.cloned.1.call-done.w_ref), custom_call_target="tpu_custom_call" | custom-call | flops 1610612736 | bytes 8388608 | tf_op jit(solution)/shard_map/project/pallas_call | solution.py:76
  84.0 1.0 slice_bitcast_fusion.12
  85.0 2.6 %collective-permute-start.1 = (bf16[2,256,128]{2,1,0:T(8,128)(2,1)S(1)}, bf16[2,256,128]{2,1,0:T(8,128)(2,1)S(1)}, u32[]{:S(2)}, u32[]{:S(2)}) collective-permute-start(bf16[2,256,128]{2,1,0:T(8,128)(2,1)S(1)} %pad_maximum_fusion.3), channel_id=1, source_target_pairs={{32,0},{64,32},{96,64},{128,96},{160,128},{192,160},{224,192},{256... | collective-permute-start | bytes 393224 | tf_op jit(solution)/shard_map/ppermute | solution.py:149
  87.5 0.6 pad_add_fusion.at_ref
  88.1 0.0 copy-done
  88.1 0.6 copy.22.first_ref
  88.7 0.0 copy-done.1
  88.7 0.6 copy.23.second_ref
  89.3 1.9 %biases.1 = (f32[14,64,128]{2,1,0:T(8,128)}, f32[14,64,128]{2,1,0:T(8,128)}) custom-call(f32[1,15,31]{2,1,0:T(8,128)} %copy.22.first_ref, f32[1,15,31]{2,1,0:T(8,128)} %copy.23.second_ref), custom_call_target="tpu_custom_call" | custom-call | tf_op jit(solution)/shard_map/biases/pallas_call | solution.py:42
  91.2 5.4 %collective-permute-start = (bf16[2,256,128]{2,1,0:T(8,128)(2,1)S(1)}, bf16[2,256,128]{2,1,0:T(8,128)(2,1)S(1)}, u32[]{:S(2)}, u32[]{:S(2)}) collective-permute-start(bf16[2,256,128]{2,1,0:T(8,128)(2,1)S(1)} %pad_maximum_fusion.2), channel_id=1, source_target_pairs={{0,32},{32,64},{64,96},{96,128},{128,160},{160,192},{192,224},{224... | collective-permute-start | bytes 393224 | tf_op jit(solution)/shard_map/ppermute | solution.py:148
  96.6 0.0 collective-permute-done.1
  96.6 0.7 slice_bitcast_fusion.4
  97.3 3.0 %collective-permute-done = bf16[2,256,128]{2,1,0:T(8,128)(2,1)S(1)} collective-permute-done((bf16[2,256,128]{2,1,0:T(8,128)(2,1)S(1)}, bf16[2,256,128]{2,1,0:T(8,128)(2,1)S(1)}, u32[]{:S(2)}, u32[]{:S(2)}) %collective-permute-start) | collective-permute-done | bytes 131104 | tf_op jit(solution)/shard_map/ppermute | solution.py:148
  100.3 0.7 slice_bitcast_fusion.5
  100.9 4.8 %attend.2.x_ref = bf16[512,128]{1,0:T(8,128)(2,1)} custom-call(s32[2]{0:T(128)} %pad_add_fusion.at_ref, bf16[512,128]{1,0:T(8,128)(2,1)} %get-tuple-element.13.q_ref, bf16[512,128]{1,0:T(8,128)(2,1)} %get-tuple-element.14.k_ref, bf16[512,128]{1,0:T(8,128)(2,1)} %get-tuple-element.15.v_ref, bf16[256,128]{1,0:T(8,128)(2,1)} %get-tuple-element.34.klo_ref, ...), custom_call_target="tpu_custom_call" | custom-call | flops 134217728 | bytes 2097152 | tf_op jit(solution)/shard_map/attend/pallas_call | solution.py:129
  105.8 0.9 multiply_convert_fusion.3
  106.7 45.6 %all-gather.10 = f16[16384,128]{1,0:T(8,128)(2,1)S(1)} all-gather(f16[512,128]{1,0:T(8,128)(2,1)S(1)} %multiply_convert_fusion.3), channel_id=2, replica_groups=mesh['sp'=16,'tp'=32] {'tp'}, dimensions={0}, use_global_device_ids=true | all-gather | bytes 4325376 | tf_op jit(solution)/shard_map/all_gather | solution.py:186
  152.3 2.4 %multiply_convert_fusion.1 = bf16[16384,128]{1,0:T(8,128)(2,1)} fusion(f16[16384,128]{1,0:T(8,128)(2,1)S(1)} %all-gather.10), kind=kLoop, calls=%fused_computation.1 | loop fusion | flops 6291456 | bytes 8388608 | tf_op jit(solution)/shard_map/convert_element_type | solution.py:187
  154.7 0.0 all-gather.8.cloned.1.call-done.w_ref
  154.7 7.1 %project.3 = (bf16[512,128]{1,0:T(8,128)(2,1)}, bf16[512,128]{1,0:T(8,128)(2,1)}, bf16[512,128]{1,0:T(8,128)(2,1)}) custom-call(bf16[32,512,128]{2,1,0:T(8,128)(2,1)} %bitcast.43, bf16[32,128]{1,0:T(8,128)(2,1)} %get-tuple-element.21.gain_ref, bf16[4096,384]{1,0:T(8,128)(2,1)} %all-gather.8.cloned.1.call-done.w_ref), custom_call_target="tpu_custom_call" | custom-call | flops 1610612736 | bytes 8388608 | tf_op jit(solution)/shard_map/project/pallas_call | solution.py:76
  161.9 0.9 slice_bitcast_fusion.9
  162.8 0.9 slice_bitcast_fusion.8
  163.7 1.9 %collective-permute-start.3 = (bf16[2,256,128]{2,1,0:T(8,128)(2,1)S(1)}, bf16[2,256,128]{2,1,0:T(8,128)(2,1)S(1)}, u32[]{:S(2)}, u32[]{:S(2)}) collective-permute-start(bf16[2,256,128]{2,1,0:T(8,128)(2,1)S(1)} %pad_maximum_fusion.5), channel_id=1, source_target_pairs={{32,0},{64,32},{96,64},{128,96},{160,128},{192,160},{224,192},{256... | collective-permute-start | bytes 393224 | tf_op jit(solution)/shard_map/ppermute | solution.py:149
  165.6 6.5 %collective-permute-start.2 = (bf16[2,256,128]{2,1,0:T(8,128)(2,1)S(1)}, bf16[2,256,128]{2,1,0:T(8,128)(2,1)S(1)}, u32[]{:S(2)}, u32[]{:S(2)}) collective-permute-start(bf16[2,256,128]{2,1,0:T(8,128)(2,1)S(1)} %pad_maximum_fusion.4), channel_id=1, source_target_pairs={{0,32},{32,64},{64,96},{96,128},{128,160},{160,192},{192,224},{224... | collective-permute-start | bytes 393224 | tf_op jit(solution)/shard_map/ppermute | solution.py:148
  172.1 2.1 %collective-permute-done.3 = bf16[2,256,128]{2,1,0:T(8,128)(2,1)S(1)} collective-permute-done((bf16[2,256,128]{2,1,0:T(8,128)(2,1)S(1)}, bf16[2,256,128]{2,1,0:T(8,128)(2,1)S(1)}, u32[]{:S(2)}, u32[]{:S(2)}) %collective-permute-start.3) | collective-permute-done | bytes 131104 | tf_op jit(solution)/shard_map/ppermute | solution.py:149
  174.2 0.7 slice_bitcast_fusion
  174.8 0.5 collective-permute-done.2
  175.4 0.7 slice_bitcast_fusion.1
  176.0 4.8 %attend.3 = bf16[512,128]{1,0:T(8,128)(2,1)} custom-call(s32[2]{0:T(128)} %pad_add_fusion.at_ref, bf16[512,128]{1,0:T(8,128)(2,1)} %get-tuple-element.17.q_ref, bf16[512,128]{1,0:T(8,128)(2,1)} %get-tuple-element.18.k_ref, bf16[512,128]{1,0:T(8,128)(2,1)} %get-tuple-element.19.v_ref, bf16[256,128]{1,0:T(8,128)(2,1)} %get-tuple-element.26.klo_ref, ...), custom_call_target="tpu_custom_call" | custom-call | flops 134217728 | bytes 2097152 | tf_op jit(solution)/shard_map/attend/pallas_call | solution.py:129
  (4 shorter events, 0.1 us)
Async XLA Ops:
  6.5 70.4 %all-gather.6.cloned.1.call-start = ((), (), s32[]{:S(2)}) async-start(), calls=%async_computation | async-start | bytes 3342336 | tf_op jit(solution)/shard_map/all_gather | solution.py:168
  8.2 146.5 %all-gather.8.cloned.1.call-start = ((), (), s32[]{:S(2)}) async-start(), calls=%async_computation.1 | async-start | bytes 3342336 | tf_op jit(solution)/shard_map/all_gather | solution.py:171
  68.5 19.6 %copy-start = (f32[1,15,31]{2,0,1:T(1,128)S(1)}, f32[1,15,31]{2,0,1:T(1,128)}, u32[]{:S(2)}) copy-start(f32[1,15,31]{2,0,1:T(1,128)} %param.16) | copy-start | bytes 5584
  68.5 20.2 %copy-start.1 = (f32[1,15,31]{2,0,1:T(1,128)S(1)}, f32[1,15,31]{2,0,1:T(1,128)}, u32[]{:S(2)}) copy-start(f32[1,15,31]{2,0,1:T(1,128)} %param.21) | copy-start | bytes 5584
  85.0 11.7 %collective-permute-start.1 = (bf16[2,256,128]{2,1,0:T(8,128)(2,1)S(1)}, bf16[2,256,128]{2,1,0:T(8,128)(2,1)S(1)}, u32[]{:S(2)}, u32[]{:S(2)}) collective-permute-start(bf16[2,256,128]{2,1,0:T(8,128)(2,1)S(1)} %pad_maximum_fusion.3), channel_id=1, source_target_pairs={{32,0},{64,32},{96,64},{128,96},{160,128},{192,160},{224,192},{256... | collective-permute-start | bytes 393224 | tf_op jit(solution)/shard_map/ppermute | solution.py:149
  91.2 9.0 %collective-permute-start = (bf16[2,256,128]{2,1,0:T(8,128)(2,1)S(1)}, bf16[2,256,128]{2,1,0:T(8,128)(2,1)S(1)}, u32[]{:S(2)}, u32[]{:S(2)}) collective-permute-start(bf16[2,256,128]{2,1,0:T(8,128)(2,1)S(1)} %pad_maximum_fusion.2), channel_id=1, source_target_pairs={{0,32},{32,64},{64,96},{96,128},{128,160},{160,192},{192,224},{224... | collective-permute-start | bytes 393224 | tf_op jit(solution)/shard_map/ppermute | solution.py:148
  163.7 10.5 %collective-permute-start.3 = (bf16[2,256,128]{2,1,0:T(8,128)(2,1)S(1)}, bf16[2,256,128]{2,1,0:T(8,128)(2,1)S(1)}, u32[]{:S(2)}, u32[]{:S(2)}) collective-permute-start(bf16[2,256,128]{2,1,0:T(8,128)(2,1)S(1)} %pad_maximum_fusion.5), channel_id=1, source_target_pairs={{32,0},{64,32},{96,64},{128,96},{160,128},{192,160},{224,192},{256... | collective-permute-start | bytes 393224 | tf_op jit(solution)/shard_map/ppermute | solution.py:149
  165.6 9.8 %collective-permute-start.2 = (bf16[2,256,128]{2,1,0:T(8,128)(2,1)S(1)}, bf16[2,256,128]{2,1,0:T(8,128)(2,1)S(1)}, u32[]{:S(2)}, u32[]{:S(2)}) collective-permute-start(bf16[2,256,128]{2,1,0:T(8,128)(2,1)S(1)} %pad_maximum_fusion.4), channel_id=1, source_target_pairs={{0,32},{32,64},{64,96},{96,128},{128,160},{160,192},{192,224},{224... | collective-permute-start | bytes 393224 | tf_op jit(solution)/shard_map/ppermute | solution.py:148
Sparse Core Ops, SparseCore 0:
  10.3 66.5 all-gather.5
  79.9 62.0 all-gather.7

commit v2 on v1

v2 whole, which is shorter than its diff:
```python
import functools

import jax
import jax.numpy as jnp
import numpy as np
from jax import lax
from jax.experimental import pallas as pl
from jax.experimental.pallas import tpu as pltpu
from jax.sharding import PartitionSpec as P

GRID_W = 64
EPSILON = 1e-06
SCALE_FIRST = 2.0**13
SCALE_SECOND = 2.0**6
WINDOW_ROWS = 8
HALO = 4
MASKED = -1e30
PROJECT_VMEM = 24 << 20
ATTEND_VMEM = 12 << 20


def vmem():
    return pl.BlockSpec(memory_space=pltpu.VMEM)


def bias_kernel(first_ref, second_ref, first_out, second_out):
    width = GRID_W
    col = lax.broadcasted_iota(jnp.int32, (width, 2 * width), 0)
    key = lax.broadcasted_iota(jnp.int32, (width, 2 * width), 1) % width
    start = jnp.clip(col - 8, 0, width - 16)
    inside = (key >= start) & (key < start + 16)
    for table_ref, out_ref in ((first_ref, first_out), (second_ref, second_out)):
        table = table_ref[0]
        low = jnp.pad(table, ((0, 1), (0, 2 * width - 31)))
        both = low + pltpu.roll(pltpu.roll(low, 15, 0), width, 1)
        for m in range(14):
            row = jnp.broadcast_to(both[m : m + 1, :], (width, 2 * width))
            turned = pltpu.roll(row, 2 * width - 15, 1, stride=1, stride_axis=0)
            out_ref[m] = jnp.where(inside, turned, MASKED)


def biases(first, second):
    shape = jax.ShapeDtypeStruct((14, GRID_W, 2 * GRID_W), jnp.float32)
    return pl.pallas_call(
        bias_kernel,
        out_shape=(shape, shape),
        in_specs=[vmem(), vmem()],
        out_specs=(vmem(), vmem()),
        compiler_params=pltpu.CompilerParams(vmem_limit_bytes=ATTEND_VMEM),
        name="biases",
    )(first, second)


def project_kernel(half, gain_row, scale, x_ref, gain_ref, w_ref, q_ref, kv_ref, normed):
    blocks, _, size = x_ref.shape
    tokens = q_ref.shape[0]
    rows = slice(half * tokens, (half + 1) * tokens)
    total = jnp.zeros((tokens, size), jnp.float32)
    for f in range(blocks):
        part = x_ref[f, rows, :].astype(jnp.float32)
        total = total + part * part
    mean = jnp.sum(total, axis=1, keepdims=True) * (1.0 / (blocks * size * scale * scale))
    rate = lax.rsqrt(mean + EPSILON) * (1.0 / scale)
    for f in range(blocks):
        part = x_ref[f, rows, :].astype(jnp.float32)
        gain = gain_ref[f, gain_row : gain_row + 1, :].astype(jnp.float32) * (1.0 / SCALE_FIRST)
        normed[:, f * size : (f + 1) * size] = (part * rate * gain).astype(jnp.bfloat16)
    out = jnp.dot(normed[...], w_ref[...], preferred_element_type=jnp.float32).astype(jnp.bfloat16)
    q_ref[...] = out[:, :size]
    kv_ref[0] = out[:, size : 2 * size]
    kv_ref[1] = out[:, 2 * size :]


def project(half, gain_row, scale, x, gain, weights, tokens):
    blocks, _, size = x.shape
    part = tokens // 2
    return pl.pallas_call(
        functools.partial(project_kernel, half, gain_row, scale),
        out_shape=(
            jax.ShapeDtypeStruct((part, size), jnp.bfloat16),
            jax.ShapeDtypeStruct((2, part, size), jnp.bfloat16),
        ),
        in_specs=[vmem()] * 3,
        out_specs=(vmem(),) * 2,
        scratch_shapes=[pltpu.VMEM((part, blocks * size), jnp.bfloat16)],
        cost_estimate=pl.CostEstimate(
            flops=2 * part * blocks * size * 3 * size, bytes_accessed=8 << 20, transcendentals=0
        ),
        compiler_params=pltpu.CompilerParams(vmem_limit_bytes=PROJECT_VMEM),
        name="project",
    )(x, gain, weights)


def attend_kernel(at_ref, qa_ref, qb_ref, low_ref, a_ref, b_ref, high_ref, bias_ref, x_ref, out_ref, keys, values):
    width = GRID_W
    half, size = qa_ref.shape
    rows = 2 * half // width
    for i, ref in enumerate((low_ref, a_ref, b_ref, high_ref)):
        keys[i * half : (i + 1) * half] = ref[0]
        values[i * half : (i + 1) * half] = ref[1]
    row_start, last = at_ref[0], at_ref[1]
    factor = size ** (-0.5)
    for r in range(rows):
        grid_row = row_start + r
        first = jnp.clip(grid_row - HALO, 0, last)
        at = pl.multiple_of((first - row_start + HALO) * width, width)
        offset = first - grid_row + 7
        span = pl.ds(at, WINDOW_ROWS * width)
        source, inner = (qa_ref, r) if r < rows // 2 else (qb_ref, r - rows // 2)
        query = source[inner * width : (inner + 1) * width, :]
        scores = lax.dot_general(
            query, keys[span, :], (((1,), (1,)), ((), ())), preferred_element_type=jnp.float32
        )
        parts = [
            scores[:, 2 * p * width : 2 * (p + 1) * width] * factor + bias_ref[offset + 2 * p]
            for p in range(WINDOW_ROWS // 2)
        ]
        top = functools.reduce(jnp.maximum, parts)
        top = jnp.max(top, axis=1, keepdims=True)
        parts = [jnp.exp(part - top) for part in parts]
        total = jnp.sum(functools.reduce(jnp.add, parts), axis=1, keepdims=True)
        inverse = 1.0 / total
        weight = jnp.concatenate([(part * inverse).astype(jnp.bfloat16) for part in parts], axis=1)
        attended = jnp.dot(weight, values[span, :], preferred_element_type=jnp.float32)
        here = slice(r * width, (r + 1) * width)
        out_ref[here, :] = (x_ref[here, :].astype(jnp.float32) + attended).astype(jnp.bfloat16)


def attend(at, queries, low, own, high, bias, x):
    tokens, size = x.shape
    long = tokens + 2 * HALO * GRID_W
    return pl.pallas_call(
        attend_kernel,
        out_shape=jax.ShapeDtypeStruct((tokens, size), jnp.bfloat16),
        in_specs=[pl.BlockSpec(memory_space=pltpu.SMEM)] + [vmem()] * 8,
        out_specs=vmem(),
        scratch_shapes=[pltpu.VMEM((long, size), jnp.bfloat16)] * 2,
        cost_estimate=pl.CostEstimate(
            flops=4 * tokens * size * WINDOW_ROWS * GRID_W, bytes_accessed=2 << 20, transcendentals=tokens * 512
        ),
        compiler_params=pltpu.CompilerParams(vmem_limit_bytes=ATTEND_VMEM),
        name="attend",
    )(at, *queries, low, *own, high, bias, x)


def layer(x, gathered, gain_row, scale, gains, weights, bias, at):
    tokens = x.shape[0]
    count = lax.axis_size("sp")
    forward = [(i, i + 1) for i in range(count - 1)]
    backward = [(target, source) for source, target in forward]
    query_high, own_high = project(1, gain_row, scale, gathered, gains, weights, tokens)
    low = lax.ppermute(own_high, "sp", forward)
    query_low, own_low = project(0, gain_row, scale, gathered, gains, weights, tokens)
    high = lax.ppermute(own_low, "sp", backward)
    return attend(at, (query_low, query_high), low, (own_low, own_high), high, bias, x)


def body(
    stream,
    gain_first,
    query_first,
    key_first,
    value_first,
    offset_first,
    gain_second,
    query_second,
    key_second,
    value_second,
    offset_second,
):
    tokens, size = stream.shape
    rows = tokens // GRID_W
    first_set = lax.all_gather(
        jnp.concatenate([query_first, key_first, value_first], 1), "sp", axis=0, tiled=True
    )
    second_set = lax.all_gather(
        jnp.concatenate([query_second, key_second, value_second], 1), "sp", axis=0, tiled=True
    )
    bias_first, bias_second = biases(offset_first, offset_second)
    start = lax.axis_index("sp") * rows
    total_rows = rows * lax.axis_size("sp")
    at = jnp.stack([start, jnp.int32(total_rows - WINDOW_ROWS)]).astype(jnp.int32)

    gains = jnp.pad(jnp.stack([gain_first, gain_second]), ((0, 14), (0, 0)))
    sent = (jnp.concatenate([stream, gains]).astype(jnp.float32) * SCALE_FIRST).astype(jnp.float16)
    held = lax.all_gather(sent, "tp", axis=0, tiled=False).astype(jnp.bfloat16)
    gains = held[:, tokens:]
    middle = layer(stream, held, 0, SCALE_FIRST, gains, first_set, bias_first, at)
    sent = (middle.astype(jnp.float32) * SCALE_SECOND).astype(jnp.float16)
    again = lax.all_gather(sent, "tp", axis=0, tiled=False).astype(jnp.bfloat16)
    return layer(middle, again, 1, SCALE_SECOND, gains, second_set, bias_second, at)


def solution(mesh):
    placed = (
        P("sp", "tp"),
        P("tp"),
        P("sp", "tp"),
        P("sp", "tp"),
        P("sp", "tp"),
        P("tp", None, None),
        P("tp"),
        P("sp", "tp"),
        P("sp", "tp"),
        P("sp", "tp"),
        P("tp", None, None),
    )
    return jax.shard_map(body, mesh=mesh, in_specs=placed, out_specs=P("sp", "tp"), check_vma=False)
```

time: 191 us -> 178 us (0.932); the launches traced: 188 us -> 178 us
  Pallas kernels: 25.8 us -> 14.8 us
  waiting for transfers between devices: 14 us -> 23.7 us
  starting transfers between devices: 16.4 us -> 11.9 us
  other arithmetic: 10.2 us -> 7.88 us
    unnamed x6 -> x18, local copies, waits for them, and re-layouts: 1.2 us -> 10.2 us
    pallas_call x2 -> x4, Pallas kernels: 14.2 us -> 6.98 us  [project(): pl.pallas_call(functools.partial(project_kernel, half, gain_row, scale),...]
    ppermute x4, waiting for transfers between devices: 5.56 us -> 11.7 us  [the longest x2 11.7 us: layer(): high = lax.ppermute(own_low, 'sp', backward)]
    ppermute x4, starting transfers between devices: 16.4 us -> 11.8 us  [the longest x2 6.41 us: layer(): high = lax.ppermute(own_low, 'sp', backward)]
    slice x2 -> x1, local copies, waits for them, and re-layouts: 4.28 us -> 0.01 us  [body(): gains = held[:, tokens:]]
    all_gather x1, waiting for transfers between devices: 8.4 us -> 11.9 us  [body(): lax.all_gather(jnp.concatenate([query_first, key_first, value_first], 1),...]
    squeeze x5 -> x0, local copies, waits for them, and re-layouts: 3.28 us -> none  [the longest x2 1.34 us: attend(): high[1]]
    another operation x3 -> x0, local copies, waits for them, and re-layouts: 2.72 us -> none  [layer(): high = lax.ppermute(jnp.stack([key[:edge], value[:edge]]), 'sp', backward)]
  transfers between devices with their start and end apart: 6 -> 6, of which waited for: 4 -> 3; matrix products, arithmetic and copies ran while one was open for 9% -> 4% of each run, Pallas kernels for 7% -> 5%
where the time goes in v2:
time: 178 us
  blocking collectives  95.9 us (54%)
  waiting for transfers between devices  23.7 us (13%)
  Pallas kernels  14.8 us (8%)
  between operations  13.6 us (8%)
  starting transfers between devices  11.9 us (7%)
  local copies, waits for them, and re-layouts  10.2 us (6%)
  other arithmetic  7.88 us (4%)
    all_gather x1, blocking collectives, body(): held = lax.all_gather(sent, 'tp', axis=0, tiled=False).astype(jnp.bfloat16)  50.7 us
    all_gather x1, blocking collectives, body(): again = lax.all_gather(sent, 'tp', axis=0, tiled=False).astype(jnp.bfloat16)  45.2 us
    all_gather x1, waiting for transfers between devices, body(): lax.all_gather(jnp.concatenate([query_first, key_first, value_first], 1),...  11.9 us
    ppermute x2, waiting for transfers between devices, layer(): high = lax.ppermute(own_low, 'sp', backward)  11.7 us
    unnamed x18, local copies, waits for them, and re-layouts  10.2 us
    pallas_call x2, Pallas kernels, attend(): pl.pallas_call(attend_kernel, out_shape=jax.ShapeDtypeStruct((tokens, siz...  7.43 us
    pallas_call x4, Pallas kernels, project(): pl.pallas_call(functools.partial(project_kernel, half, gain_row, scale),...  6.98 us
    ppermute x2, starting transfers between devices, layer(): high = lax.ppermute(own_low, 'sp', backward)  6.41 us
  transfers between devices with their start and end apart: 6, of which 3 were waited for; matrix products, arithmetic and copies ran while one was open for 4% of the time, Pallas kernels for 5%

profile of v2, /device:TPU:6, one launch (start us, length us, event | category | flops | bytes accessed | tf_op | source)
XLA Modules:
  0.0 178.0 jit_solution(7119882892377684839)
XLA Ops:
  6.5 0.0 all-gather.6.cloned.1.call-start
  6.5 1.6 pad_maximum_fusion
  8.2 0.0 all-gather.6.cloned.1.call-update
  8.2 0.0 all-gather.8.cloned.1.call-start
  8.2 1.6 pad_maximum_fusion.1
  9.8 0.0 all-gather.8.cloned.1.call-update
  9.9 0.7 fusion.3
  10.6 0.9 multiply_convert_fusion
  11.5 50.7 %all-gather.9 = f16[32,528,128]{2,1,0:T(8,128)(2,1)S(1)} all-gather(f16[1,528,128]{2,1,0:T(8,128)(2,1)S(1)} %multiply_convert_fusion), channel_id=1, replica_groups=mesh['sp'=16,'tp'=32] {'tp'}, dimensions={0}, use_global_device_ids=true | all-gather | bytes 4460544 | tf_op jit(solution)/shard_map/all_gather | solution.py:186
  62.2 0.7 convert_element_type.36.x_ref
  63.0 0.0 copy-start
  63.0 2.0 %copy-done = bf16[32,528,128]{2,1,0:T(8,128)(2,1)} copy-done((bf16[32,528,128]{2,1,0:T(8,128)(2,1)}, bf16[32,528,128]{2,1,0:T(8,128)(2,1)S(1)}, u32[]{:S(2)}) %copy-start) | copy-done | bytes 4325400
  64.9 11.9 %all-gather.6.cloned.1.call-done.w_ref = bf16[4096,384]{1,0:T(8,128)(2,1)} async-done(((bf16[256,384]{1,0:T(8,128)(2,1)}), bf16[4096,384]{1,0:T(8,128)(2,1)}) %all-gather.6.cloned.1.call-update) | async-done | bytes 3145744 | tf_op jit(solution)/shard_map/all_gather | solution.py:173
  76.9 0.0 copy-start.1
  76.9 2.2 %copy-done.1 = bf16[32,528,128]{2,1,0:T(8,128)(2,1)S(1)} copy-done((bf16[32,528,128]{2,1,0:T(8,128)(2,1)S(1)}, bf16[32,528,128]{2,1,0:T(8,128)(2,1)}, u32[]{:S(2)}) %copy-start.1) | copy-done | bytes 4325400
  79.1 0.0 copy-start.4
  79.1 1.9 %copy-done.4 = bf16[4096,384]{1,0:T(8,128)(2,1)S(1)} copy-done((bf16[4096,384]{1,0:T(8,128)(2,1)S(1)}, bf16[4096,384]{1,0:T(8,128)(2,1)}, u32[]{:S(2)}) %copy-start.4) | copy-done | bytes 3145752
  81.0 1.7 project.5
  82.8 0.0 copy-start.6
  82.8 0.0 copy-start.7
  82.8 0.0 copy-start.5
  82.8 3.5 %collective-permute-start = (bf16[2,256,128]{2,1,0:T(8,128)(2,1)S(1)}, bf16[2,256,128]{2,1,0:T(8,128)(2,1)S(1)}, u32[]{:S(2)}, u32[]{:S(2)}) collective-permute-start(bf16[2,256,128]{2,1,0:T(8,128)(2,1)S(1)} %get-tuple-element.17.b_ref), channel_id=1, source_target_pairs={{0,32},{32,64},{64,96},{96,128},{128,160},{160,192},{192,224},{224... | collective-permute-start | bytes 393224 | tf_op jit(solution)/shard_map/ppermute | solution.py:152
  86.3 1.7 project.4
  88.0 2.5 %collective-permute-start.1 = (bf16[2,256,128]{2,1,0:T(8,128)(2,1)S(1)}, bf16[2,256,128]{2,1,0:T(8,128)(2,1)S(1)}, u32[]{:S(2)}, u32[]{:S(2)}) collective-permute-start(bf16[2,256,128]{2,1,0:T(8,128)(2,1)S(1)} %get-tuple-element.18.a_ref), channel_id=1, source_target_pairs={{32,0},{64,32},{96,64},{128,96},{160,128},{192,160},{224,192},{256... | collective-permute-start | bytes 393224 | tf_op jit(solution)/shard_map/ppermute | solution.py:154
  90.5 0.0 copy-done.6
  90.5 0.0 copy-done.7
  90.6 0.4 biases.1
  91.0 0.1 pad_add_fusion.at_ref
  91.1 0.0 collective-permute-done.low_ref
  91.1 5.9 %collective-permute-done.1.high_ref = bf16[2,256,128]{2,1,0:T(8,128)(2,1)S(1)} collective-permute-done((bf16[2,256,128]{2,1,0:T(8,128)(2,1)S(1)}, bf16[2,256,128]{2,1,0:T(8,128)(2,1)S(1)}, u32[]{:S(2)}, u32[]{:S(2)}) %collective-permute-start.1) | collective-permute-done | bytes 131104 | tf_op jit(solution)/shard_map/ppermute | solution.py:154
  97.0 0.0 copy-done.5
  97.0 3.4 %attend.2.x_ref = bf16[512,128]{1,0:T(8,128)(2,1)S(1)} custom-call(s32[2]{0:T(128)S(1)} %pad_add_fusion.at_ref, bf16[256,128]{1,0:T(8,128)(2,1)S(1)} %get-tuple-element.15.qa_ref, bf16[256,128]{1,0:T(8,128)(2,1)S(1)} %get-tuple-element.16.qb_ref, bf16[2,256,128]{2,1,0:T(8,128)(2,1)S(1)} %collective-permute-done.low_ref, ...), custom_call_target="tpu_custom_call" | custom-call | flops 134217728 | bytes 2097152 | tf_op jit(solution)/shard_map/attend/pallas_call | solution.py:132
  100.4 45.2 %all-gather.10 = f16[16384,128]{1,0:T(8,128)(2,1)S(1)} all-gather(f16[512,128]{1,0:T(8,128)(2,1)S(1)} %multiply_convert_fusion.1), channel_id=2, replica_groups=mesh['sp'=16,'tp'=32] {'tp'}, dimensions={0}, use_global_device_ids=true | all-gather | bytes 4325376 | tf_op jit(solution)/shard_map/all_gather | solution.py:190
  145.6 2.2 %convert_element_type.40 = bf16[16384,128]{1,0:T(8,128)(2,1)} convert(f16[16384,128]{1,0:T(8,128)(2,1)S(1)} %all-gather.10) | non-fusion elementwise | flops 2097152 | bytes 8388608 | tf_op jit(solution)/shard_map/convert_element_type | solution.py:190
  147.8 0.0 all-gather.8.cloned.1.call-done.w_ref
  147.8 0.0 copy-start.2
  147.8 2.2 %copy-done.2 = bf16[16384,128]{1,0:T(8,128)(2,1)S(1)} copy-done((bf16[16384,128]{1,0:T(8,128)(2,1)S(1)}, bf16[16384,128]{1,0:T(8,128)(2,1)}, u32[]{:S(2)}) %copy-start.2) | copy-done | bytes 4194328
  150.0 0.0 copy-start.3
  150.0 1.9 %copy-done.3 = bf16[4096,384]{1,0:T(8,128)(2,1)S(1)} copy-done((bf16[4096,384]{1,0:T(8,128)(2,1)S(1)}, bf16[4096,384]{1,0:T(8,128)(2,1)}, u32[]{:S(2)}) %copy-start.3) | copy-done | bytes 3145752
  151.9 1.8 project.7
  153.6 1.9 %collective-permute-start.2 = (bf16[2,256,128]{2,1,0:T(8,128)(2,1)S(1)}, bf16[2,256,128]{2,1,0:T(8,128)(2,1)S(1)}, u32[]{:S(2)}, u32[]{:S(2)}) collective-permute-start(bf16[2,256,128]{2,1,0:T(8,128)(2,1)S(1)} %get-tuple-element.22.b_ref), channel_id=1, source_target_pairs={{0,32},{32,64},{64,96},{96,128},{128,160},{160,192},{192,224},{224... | collective-permute-start | bytes 393224 | tf_op jit(solution)/shard_map/ppermute | solution.py:152
  155.6 1.8 project.6
  157.3 3.9 %collective-permute-start.3 = (bf16[2,256,128]{2,1,0:T(8,128)(2,1)S(1)}, bf16[2,256,128]{2,1,0:T(8,128)(2,1)S(1)}, u32[]{:S(2)}, u32[]{:S(2)}) collective-permute-start(bf16[2,256,128]{2,1,0:T(8,128)(2,1)S(1)} %get-tuple-element.23.a_ref), channel_id=1, source_target_pairs={{32,0},{64,32},{96,64},{128,96},{160,128},{192,160},{224,192},{256... | collective-permute-start | bytes 393224 | tf_op jit(solution)/shard_map/ppermute | solution.py:154
  161.2 0.0 collective-permute-done.2.low_ref
  161.3 5.8 %collective-permute-done.3.high_ref = bf16[2,256,128]{2,1,0:T(8,128)(2,1)S(1)} collective-permute-done((bf16[2,256,128]{2,1,0:T(8,128)(2,1)S(1)}, bf16[2,256,128]{2,1,0:T(8,128)(2,1)S(1)}, u32[]{:S(2)}, u32[]{:S(2)}) %collective-permute-start.3) | collective-permute-done | bytes 131104 | tf_op jit(solution)/shard_map/ppermute | solution.py:154
  167.1 4.0 %attend.3 = bf16[512,128]{1,0:T(8,128)(2,1)} custom-call(s32[2]{0:T(128)S(1)} %pad_add_fusion.at_ref, bf16[256,128]{1,0:T(8,128)(2,1)S(1)} %get-tuple-element.20.qa_ref, bf16[256,128]{1,0:T(8,128)(2,1)S(1)} %get-tuple-element.21.qb_ref, bf16[2,256,128]{2,1,0:T(8,128)(2,1)S(1)} %collective-permute-done.2.low_ref, ...), custom_call_target="tpu_custom_call" | custom-call | flops 134217728 | bytes 2097152 | tf_op jit(solution)/shard_map/attend/pallas_call | solution.py:132
  (4 shorter events, 0.1 us)
Async XLA Ops:
  6.5 70.4 %all-gather.6.cloned.1.call-start = ((), (), s32[]{:S(2)}) async-start(), calls=%async_computation | async-start | bytes 3342336 | tf_op jit(solution)/shard_map/all_gather | solution.py:173
  8.2 139.6 %all-gather.8.cloned.1.call-start = ((), (), s32[]{:S(2)}) async-start(), calls=%async_computation.1 | async-start | bytes 3342336 | tf_op jit(solution)/shard_map/all_gather | solution.py:176
  63.0 2.0 %copy-start = (bf16[32,528,128]{2,1,0:T(8,128)(2,1)}, bf16[32,528,128]{2,1,0:T(8,128)(2,1)S(1)}, u32[]{:S(2)}) copy-start(bf16[32,528,128]{2,1,0:T(8,128)(2,1)S(1)} %convert_element_type.36.x_ref) | copy-start | bytes 12976132
  76.9 2.2 %copy-start.1 = (bf16[32,528,128]{2,1,0:T(8,128)(2,1)S(1)}, bf16[32,528,128]{2,1,0:T(8,128)(2,1)}, u32[]{:S(2)}) copy-start(bf16[32,528,128]{2,1,0:T(8,128)(2,1)} %copy-done) | copy-start | bytes 12976132
  79.1 1.9 %copy-start.4 = (bf16[4096,384]{1,0:T(8,128)(2,1)S(1)}, bf16[4096,384]{1,0:T(8,128)(2,1)}, u32[]{:S(2)}) copy-start(bf16[4096,384]{1,0:T(8,128)(2,1)} %all-gather.6.cloned.1.call-done.w_ref) | copy-start | bytes 9437188
  82.8 7.8 %copy-start.6 = (f32[1,15,31]{2,0,1:T(1,128)S(1)}, f32[1,15,31]{2,0,1:T(1,128)}, u32[]{:S(2)}) copy-start(f32[1,15,31]{2,0,1:T(1,128)} %param.16) | copy-start | bytes 5584
  82.8 7.8 %copy-start.7 = (f32[1,15,31]{2,0,1:T(1,128)S(1)}, f32[1,15,31]{2,0,1:T(1,128)}, u32[]{:S(2)}) copy-start(f32[1,15,31]{2,0,1:T(1,128)} %param.21) | copy-start | bytes 5584
  82.8 14.2 %copy-start.5 = (bf16[512,128]{1,0:T(8,128)(2,1)S(1)}, bf16[512,128]{1,0:T(8,128)(2,1)}, u32[]{:S(2)}) copy-start(bf16[512,128]{1,0:T(8,128)(2,1)} %x_ref.1) | copy-start | bytes 393220
  82.8 8.3 %collective-permute-start = (bf16[2,256,128]{2,1,0:T(8,128)(2,1)S(1)}, bf16[2,256,128]{2,1,0:T(8,128)(2,1)S(1)}, u32[]{:S(2)}, u32[]{:S(2)}) collective-permute-start(bf16[2,256,128]{2,1,0:T(8,128)(2,1)S(1)} %get-tuple-element.17.b_ref), channel_id=1, source_target_pairs={{0,32},{32,64},{64,96},{96,128},{128,160},{160,192},{192,224},{224... | collective-permute-start | bytes 393224 | tf_op jit(solution)/shard_map/ppermute | solution.py:152
  88.0 9.0 %collective-permute-start.1 = (bf16[2,256,128]{2,1,0:T(8,128)(2,1)S(1)}, bf16[2,256,128]{2,1,0:T(8,128)(2,1)S(1)}, u32[]{:S(2)}, u32[]{:S(2)}) collective-permute-start(bf16[2,256,128]{2,1,0:T(8,128)(2,1)S(1)} %get-tuple-element.18.a_ref), channel_id=1, source_target_pairs={{32,0},{64,32},{96,64},{128,96},{160,128},{192,160},{224,192},{256... | collective-permute-start | bytes 393224 | tf_op jit(solution)/shard_map/ppermute | solution.py:154
  147.8 2.2 %copy-start.2 = (bf16[16384,128]{1,0:T(8,128)(2,1)S(1)}, bf16[16384,128]{1,0:T(8,128)(2,1)}, u32[]{:S(2)}) copy-start(bf16[16384,128]{1,0:T(8,128)(2,1)} %convert_element_type.40) | copy-start | bytes 12582916
  150.0 1.9 %copy-start.3 = (bf16[4096,384]{1,0:T(8,128)(2,1)S(1)}, bf16[4096,384]{1,0:T(8,128)(2,1)}, u32[]{:S(2)}) copy-start(bf16[4096,384]{1,0:T(8,128)(2,1)} %all-gather.8.cloned.1.call-done.w_ref) | copy-start | bytes 9437188
  153.6 7.7 %collective-permute-start.2 = (bf16[2,256,128]{2,1,0:T(8,128)(2,1)S(1)}, bf16[2,256,128]{2,1,0:T(8,128)(2,1)S(1)}, u32[]{:S(2)}, u32[]{:S(2)}) collective-permute-start(bf16[2,256,128]{2,1,0:T(8,128)(2,1)S(1)} %get-tuple-element.22.b_ref), channel_id=1, source_target_pairs={{0,32},{32,64},{64,96},{96,128},{128,160},{160,192},{192,224},{224... | collective-permute-start | bytes 393224 | tf_op jit(solution)/shard_map/ppermute | solution.py:152
  157.3 9.8 %collective-permute-start.3 = (bf16[2,256,128]{2,1,0:T(8,128)(2,1)S(1)}, bf16[2,256,128]{2,1,0:T(8,128)(2,1)S(1)}, u32[]{:S(2)}, u32[]{:S(2)}) collective-permute-start(bf16[2,256,128]{2,1,0:T(8,128)(2,1)S(1)} %get-tuple-element.23.a_ref), channel_id=1, source_target_pairs={{32,0},{64,32},{96,64},{128,96},{160,128},{192,160},{224,192},{256... | collective-permute-start | bytes 393224 | tf_op jit(solution)/shard_map/ppermute | solution.py:154
Sparse Core Ops, SparseCore 0:
  10.3 66.5 all-gather.5
  79.9 61.9 all-gather.7

commit v3 on v2

--- a/solution.py
+++ b/solution.py
@@ -155,6 +155,16 @@
     return attend(at, (query_low, query_high), low, (own_low, own_high), high, bias, x)
 
 
+def replicated(weights):
+    block = jnp.concatenate(weights, 1)
+    return jnp.broadcast_to(block[None], (lax.axis_size("sp"), *block.shape))
+
+
+def spread(blocks):
+    got = lax.all_to_all(blocks, "sp", 0, 0, tiled=True)
+    return got.reshape(-1, blocks.shape[-1])
+
+
 def body(
     stream,
     gain_first,
@@ -170,12 +180,8 @@
 ):
     tokens, size = stream.shape
     rows = tokens // GRID_W
-    first_set = lax.all_gather(
-        jnp.concatenate([query_first, key_first, value_first], 1), "sp", axis=0, tiled=True
-    )
-    second_set = lax.all_gather(
-        jnp.concatenate([query_second, key_second, value_second], 1), "sp", axis=0, tiled=True
-    )
+    first_set = spread(replicated((query_first, key_first, value_first)))
+    second_blocks = replicated((query_second, key_second, value_second))
     bias_first, bias_second = biases(offset_first, offset_second)
     start = lax.axis_index("sp") * rows
     total_rows = rows * lax.axis_size("sp")
@@ -186,6 +192,8 @@
     held = lax.all_gather(sent, "tp", axis=0, tiled=False).astype(jnp.bfloat16)
     gains = held[:, tokens:]
     middle = layer(stream, held, 0, SCALE_FIRST, gains, first_set, bias_first, at)
+    middle, second_blocks = lax.optimization_barrier((middle, second_blocks))
+    second_set = spread(second_blocks)
     sent = (middle.astype(jnp.float32) * SCALE_SECOND).astype(jnp.float16)
     again = lax.all_gather(sent, "tp", axis=0, tiled=False).astype(jnp.bfloat16)
     return layer(middle, again, 1, SCALE_SECOND, gains, second_set, bias_second, at)

time: 178 us -> 162 us (0.910)
  starting transfers between devices: 11.9 us -> 27.5 us
  between operations: 13.6 us -> 0.23 us
  waiting for transfers between devices: 23.7 us -> 12.8 us
  blocking collectives: 95.9 us -> 90.4 us
  other arithmetic: 7.88 us -> 4.04 us
    all_to_all x0 -> x2, starting transfers between devices: none -> 15.8 us  [spread(): got = lax.all_to_all(blocks, 'sp', 0, 0, tiled=True)]
    all_gather x2 -> x0, waiting for transfers between devices: 11.9 us -> none  [the longest x1 11.9 us: body(): lax.all_gather(jnp.concatenate([query_first, key_first, value_first], 1),...]
    broadcast_in_dim x0 -> x2, local copies, waits for them, and re-layouts: none -> 4.17 us  [replicated(): return jnp.broadcast_to(block[None], (lax.axis_size('sp'), *block.shape))]
    unnamed x18 -> x28, local copies, waits for them, and re-layouts: 10.2 us -> 7.22 us
    all_gather x1, blocking collectives: 50.7 us -> 47.9 us  [body(): held = lax.all_gather(sent, 'tp', axis=0, tiled=False).astype(jnp.bfloat16)]
    all_gather x1, blocking collectives: 45.2 us -> 42.5 us  [body(): again = lax.all_gather(sent, 'tp', axis=0, tiled=False).astype(jnp.bfloat16)]
    concatenate x2, other arithmetic: 3.23 us -> 0.96 us  [replicated(): block = jnp.concatenate(weights, 1)]
    ppermute x2, waiting for transfers between devices: 0.05 us -> 2.23 us  [layer(): low = lax.ppermute(own_high, 'sp', forward)]
  transfers between devices with their start and end apart: 6 -> 6, of which waited for: 3 -> 4; matrix products, arithmetic and copies ran while one was open for 4% -> 2% of each run, Pallas kernels for 5% -> 0%
where the time goes in v3:
time: 162 us; the launch traced here: 161 us
  blocking collectives  90.4 us (56%)
  starting transfers between devices  27.5 us (17%)
  Pallas kernels  15 us (9%)
  waiting for transfers between devices  12.8 us (8%)
  local copies, waits for them, and re-layouts  11.4 us (7%)
  other arithmetic  4.04 us (2%)
    all_gather x1, blocking collectives, body(): held = lax.all_gather(sent, 'tp', axis=0, tiled=False).astype(jnp.bfloat16)  47.9 us
    all_gather x1, blocking collectives, body(): again = lax.all_gather(sent, 'tp', axis=0, tiled=False).astype(jnp.bfloat16)  42.5 us
    all_to_all x2, starting transfers between devices, spread(): got = lax.all_to_all(blocks, 'sp', 0, 0, tiled=True)  15.8 us
    ppermute x2, waiting for transfers between devices, layer(): high = lax.ppermute(own_low, 'sp', backward)  10.6 us
    pallas_call x2, Pallas kernels, attend(): pl.pallas_call(attend_kernel, out_shape=jax.ShapeDtypeStruct((tokens, siz...  7.43 us
    unnamed x28, local copies, waits for them, and re-layouts  7.22 us
    pallas_call x4, Pallas kernels, project(): pl.pallas_call(functools.partial(project_kernel, half, gain_row, scale),...  7.14 us
    ppermute x2, starting transfers between devices, layer(): low = lax.ppermute(own_high, 'sp', forward)  6.88 us
  transfers between devices with their start and end apart: 6, of which 4 were waited for; matrix products, arithmetic and copies ran while one was open for 2% of the time, Pallas kernels for 0%

profile of v3, /device:TPU:6, one launch (start us, length us, event | category | flops | bytes accessed | tf_op | source)
XLA Modules:
  0.0 161.4 jit_solution(16054903439639758345)
XLA Ops:
  0.0 0.9 pad_maximum_fusion
  0.9 0.0 copy-start.11
  0.9 0.0 copy-start.12
  1.0 0.0 copy-start.3
  1.0 2.1 %broadcast_in_dim.4 = bf16[16,256,384]{2,1,0:T(8,128)(2,1)} broadcast(bf16[256,384]{1,0:T(8,128)(2,1)S(1)} %pad_maximum_fusion), dimensions={1,2} | broadcast | bytes 3342336 | tf_op jit(solution)/shard_map/broadcast_in_dim | solution.py:160
  3.1 9.4 %all-to-all-start = ((bf16[16,256,384]{2,1,0:T(8,128)(2,1)}), bf16[16,256,384]{2,1,0:T(8,128)(2,1)S(1)}, u32[]{:S(2)}, u32[]{:S(2)}) async-start(bf16[16,256,384]{2,1,0:T(8,128)(2,1)} %broadcast_in_dim.4), calls=%async_computation | async-start | bytes 6291456 | tf_op jit(solution)/shard_map/all_to_all | solution.py:164
  12.4 0.0 copy-done.11
  12.4 0.0 copy-done.12
  12.4 0.0 copy-done.3
  12.5 47.9 %all-gather.3 = f16[32,528,128]{2,1,0:T(8,128)(2,1)S(1)} all-gather(f16[1,528,128]{2,1,0:T(8,128)(2,1)S(1)} %multiply_convert_fusion), channel_id=1, replica_groups=mesh['sp'=16,'tp'=32] {'tp'}, dimensions={0}, use_global_device_ids=true | all-gather | bytes 4460544 | tf_op jit(solution)/shard_map/all_gather | solution.py:192
  60.4 0.7 convert_element_type.36.x_ref
  61.2 0.0 copy-start
  61.2 2.0 %copy-done = bf16[32,528,128]{2,1,0:T(8,128)(2,1)} copy-done((bf16[32,528,128]{2,1,0:T(8,128)(2,1)}, bf16[32,528,128]{2,1,0:T(8,128)(2,1)S(1)}, u32[]{:S(2)}) %copy-start) | copy-done | bytes 4325400
  63.2 0.0 all-to-all-done
  63.2 2.2 %copy-done.1 = bf16[32,528,128]{2,1,0:T(8,128)(2,1)S(1)} copy-done((bf16[32,528,128]{2,1,0:T(8,128)(2,1)S(1)}, bf16[32,528,128]{2,1,0:T(8,128)(2,1)}, u32[]{:S(2)}) %copy-start.1) | copy-done | bytes 4325400
  65.4 1.7 %project.5 = (bf16[256,128]{1,0:T(8,128)(2,1)S(1)}, bf16[2,256,128]{2,1,0:T(8,128)(2,1)S(1)}) custom-call(bf16[32,528,128]{2,1,0:T(8,128)(2,1)S(1)} %copy-done.1, bf16[32,16,128]{2,1,0:T(8,128)(2,1)S(1)} %slice.4.gain_ref, bf16[4096,384]{1,0:T(8,128)(2,1)S(1)} %bitcast.13), custom_call_target="tpu_custom_call" | custom-call | flops 805306368 | bytes 8388608 | tf_op jit(solution)/shard_map/project/pallas_call | solution.py:77
  67.2 0.0 copy-start.9
  67.2 0.0 copy-start.10
  67.2 0.0 copy-start.6
  67.2 0.0 copy-start.7
  67.2 0.0 copy-start.8
  67.2 1.7 %project.4 = (bf16[256,128]{1,0:T(8,128)(2,1)S(1)}, bf16[2,256,128]{2,1,0:T(8,128)(2,1)S(1)}) custom-call(bf16[32,528,128]{2,1,0:T(8,128)(2,1)S(1)} %copy-done.1, bf16[32,16,128]{2,1,0:T(8,128)(2,1)S(1)} %slice.4.gain_ref, bf16[4096,384]{1,0:T(8,128)(2,1)S(1)} %bitcast.14), custom_call_target="tpu_custom_call" | custom-call | flops 805306368 | bytes 8388608 | tf_op jit(solution)/shard_map/project/pallas_call | solution.py:77
  69.0 3.5 %collective-permute-start = (bf16[2,256,128]{2,1,0:T(8,128)(2,1)S(1)}, bf16[2,256,128]{2,1,0:T(8,128)(2,1)S(1)}, u32[]{:S(2)}, u32[]{:S(2)}) collective-permute-start(bf16[2,256,128]{2,1,0:T(8,128)(2,1)S(1)} %get-tuple-element.19.b_ref), channel_id=1, source_target_pairs={{0,32},{32,64},{64,96},{96,128},{128,160},{160,192},{192,224},{224... | collective-permute-start | bytes 393224 | tf_op jit(solution)/shard_map/ppermute | solution.py:152
  72.5 2.3 %collective-permute-start.1 = (bf16[2,256,128]{2,1,0:T(8,128)(2,1)S(1)}, bf16[2,256,128]{2,1,0:T(8,128)(2,1)S(1)}, u32[]{:S(2)}, u32[]{:S(2)}) collective-permute-start(bf16[2,256,128]{2,1,0:T(8,128)(2,1)S(1)} %get-tuple-element.20.a_ref), channel_id=1, source_target_pairs={{32,0},{64,32},{96,64},{128,96},{160,128},{192,160},{224,192},{256... | collective-permute-start | bytes 393224 | tf_op jit(solution)/shard_map/ppermute | solution.py:154
  74.8 0.1 pad_add_fusion.at_ref
  74.9 0.0 copy-done.9
  74.9 0.0 copy-done.10
  74.9 0.4 biases.1
  75.4 0.0 copy-start.4
  75.4 0.8 copy-done.4
  76.1 0.0 copy-done.6
  76.1 0.0 copy-done.8
  76.2 0.4 collective-permute-done.low_ref
  76.6 5.4 %collective-permute-done.1.high_ref = bf16[2,256,128]{2,1,0:T(8,128)(2,1)S(1)} collective-permute-done((bf16[2,256,128]{2,1,0:T(8,128)(2,1)S(1)}, bf16[2,256,128]{2,1,0:T(8,128)(2,1)S(1)}, u32[]{:S(2)}, u32[]{:S(2)}) %collective-permute-start.1) | collective-permute-done | bytes 131104 | tf_op jit(solution)/shard_map/ppermute | solution.py:154
  82.0 3.4 %attend.2.x_ref = bf16[512,128]{1,0:T(8,128)(2,1)S(1)} custom-call(s32[2]{0:T(128)S(1)} %pad_add_fusion.at_ref, bf16[256,128]{1,0:T(8,128)(2,1)S(1)} %get-tuple-element.17.qa_ref, bf16[256,128]{1,0:T(8,128)(2,1)S(1)} %get-tuple-element.18.qb_ref, bf16[2,256,128]{2,1,0:T(8,128)(2,1)S(1)} %collective-permute-done.low_ref, ...), custom_call_target="tpu_custom_call" | custom-call | flops 134217728 | bytes 2097152 | tf_op jit(solution)/shard_map/attend/pallas_call | solution.py:132
  85.4 2.1 %broadcast_in_dim.5 = bf16[16,256,384]{2,1,0:T(8,128)(2,1)} broadcast(bf16[256,384]{1,0:T(8,128)(2,1)S(1)} %pad_maximum_fusion.1), dimensions={1,2} | broadcast | bytes 3342336 | tf_op jit(solution)/shard_map/broadcast_in_dim | solution.py:160
  87.5 6.5 %all-to-all-start.1 = ((bf16[16,256,384]{2,1,0:T(8,128)(2,1)}), bf16[16,256,384]{2,1,0:T(8,128)(2,1)S(1)}, u32[]{:S(2)}, u32[]{:S(2)}) async-start(bf16[16,256,384]{2,1,0:T(8,128)(2,1)} %broadcast_in_dim.5), calls=%async_computation.1 | async-start | bytes 6291456 | tf_op jit(solution)/shard_map/all_to_all | solution.py:164
  94.0 42.5 %all-gather.4 = f16[16384,128]{1,0:T(8,128)(2,1)S(1)} all-gather(f16[512,128]{1,0:T(8,128)(2,1)S(1)} %multiply_convert_fusion.1), channel_id=2, replica_groups=mesh['sp'=16,'tp'=32] {'tp'}, dimensions={0}, use_global_device_ids=true | all-gather | bytes 4325376 | tf_op jit(solution)/shard_map/all_gather | solution.py:198
  136.4 2.2 %convert_element_type.40 = bf16[16384,128]{1,0:T(8,128)(2,1)} convert(f16[16384,128]{1,0:T(8,128)(2,1)S(1)} %all-gather.4) | non-fusion elementwise | flops 2097152 | bytes 8388608 | tf_op jit(solution)/shard_map/convert_element_type | solution.py:198
  138.6 0.0 all-to-all-done.1
  138.6 2.2 %copy-done.2 = bf16[16384,128]{1,0:T(8,128)(2,1)S(1)} copy-done((bf16[16384,128]{1,0:T(8,128)(2,1)S(1)}, bf16[16384,128]{1,0:T(8,128)(2,1)}, u32[]{:S(2)}) %copy-start.2) | copy-done | bytes 4194328
  140.8 1.8 %project.7 = (bf16[256,128]{1,0:T(8,128)(2,1)S(1)}, bf16[2,256,128]{2,1,0:T(8,128)(2,1)S(1)}) custom-call(bf16[32,512,128]{2,1,0:T(8,128)(2,1)S(1)} %bitcast.9, bf16[32,16,128]{2,1,0:T(8,128)(2,1)S(1)} %slice.4.gain_ref, bf16[4096,384]{1,0:T(8,128)(2,1)S(1)} %bitcast.11), custom_call_target="tpu_custom_call" | custom-call | flops 805306368 | bytes 8388608 | tf_op jit(solution)/shard_map/project/pallas_call | solution.py:77
  142.7 1.8 %project.6 = (bf16[256,128]{1,0:T(8,128)(2,1)S(1)}, bf16[2,256,128]{2,1,0:T(8,128)(2,1)S(1)}) custom-call(bf16[32,512,128]{2,1,0:T(8,128)(2,1)S(1)} %bitcast.10, bf16[32,16,128]{2,1,0:T(8,128)(2,1)S(1)} %slice.4.gain_ref, bf16[4096,384]{1,0:T(8,128)(2,1)S(1)} %bitcast.12), custom_call_target="tpu_custom_call" | custom-call | flops 805306368 | bytes 8388608 | tf_op jit(solution)/shard_map/project/pallas_call | solution.py:77
  144.5 3.4 %collective-permute-start.2 = (bf16[2,256,128]{2,1,0:T(8,128)(2,1)S(1)}, bf16[2,256,128]{2,1,0:T(8,128)(2,1)S(1)}, u32[]{:S(2)}, u32[]{:S(2)}) collective-permute-start(bf16[2,256,128]{2,1,0:T(8,128)(2,1)S(1)} %get-tuple-element.26.b_ref), channel_id=1, source_target_pairs={{0,32},{32,64},{64,96},{96,128},{128,160},{160,192},{192,224},{224... | collective-permute-start | bytes 393224 | tf_op jit(solution)/shard_map/ppermute | solution.py:152
  147.9 2.5 %collective-permute-start.3 = (bf16[2,256,128]{2,1,0:T(8,128)(2,1)S(1)}, bf16[2,256,128]{2,1,0:T(8,128)(2,1)S(1)}, u32[]{:S(2)}, u32[]{:S(2)}) collective-permute-start(bf16[2,256,128]{2,1,0:T(8,128)(2,1)S(1)} %get-tuple-element.27.a_ref), channel_id=1, source_target_pairs={{32,0},{64,32},{96,64},{128,96},{160,128},{192,160},{224,192},{256... | collective-permute-start | bytes 393224 | tf_op jit(solution)/shard_map/ppermute | solution.py:154
  150.4 1.8 %collective-permute-done.2.low_ref = bf16[2,256,128]{2,1,0:T(8,128)(2,1)S(1)} collective-permute-done((bf16[2,256,128]{2,1,0:T(8,128)(2,1)S(1)}, bf16[2,256,128]{2,1,0:T(8,128)(2,1)S(1)}, u32[]{:S(2)}, u32[]{:S(2)}) %collective-permute-start.2) | collective-permute-done | bytes 131104 | tf_op jit(solution)/shard_map/ppermute | solution.py:152
  152.1 5.2 %collective-permute-done.3.high_ref = bf16[2,256,128]{2,1,0:T(8,128)(2,1)S(1)} collective-permute-done((bf16[2,256,128]{2,1,0:T(8,128)(2,1)S(1)}, bf16[2,256,128]{2,1,0:T(8,128)(2,1)S(1)}, u32[]{:S(2)}, u32[]{:S(2)}) %collective-permute-start.3) | collective-permute-done | bytes 131104 | tf_op jit(solution)/shard_map/ppermute | solution.py:154
  157.4 4.0 %attend.3 = bf16[512,128]{1,0:T(8,128)(2,1)} custom-call(s32[2]{0:T(128)S(1)} %pad_add_fusion.at_ref, bf16[256,128]{1,0:T(8,128)(2,1)S(1)} %get-tuple-element.24.qa_ref, bf16[256,128]{1,0:T(8,128)(2,1)S(1)} %get-tuple-element.25.qb_ref, bf16[2,256,128]{2,1,0:T(8,128)(2,1)S(1)} %collective-permute-done.2.low_ref, ...), custom_call_target="tpu_custom_call" | custom-call | flops 134217728 | bytes 2097152 | tf_op jit(solution)/shard_map/attend/pallas_call | solution.py:132
  (12 shorter events, 0.1 us)
Async XLA Ops:
  0.9 11.5 %copy-start.11 = (bf16[128]{0:T(256)(128)(2,1)S(1)}, bf16[128]{0:T(256)(128)(2,1)}, u32[]{:S(2)}) copy-start(bf16[128]{0:T(256)(128)(2,1)} %param.17) | copy-start | bytes 772
  0.9 11.5 %copy-start.12 = (bf16[128]{0:T(256)(128)(2,1)S(1)}, bf16[128]{0:T(256)(128)(2,1)}, u32[]{:S(2)}) copy-start(bf16[128]{0:T(256)(128)(2,1)} %param.12) | copy-start | bytes 772
  1.0 11.5 %copy-start.3 = (bf16[512,128]{1,0:T(8,128)(2,1)S(1)}, bf16[512,128]{1,0:T(8,128)(2,1)}, u32[]{:S(2)}) copy-start(bf16[512,128]{1,0:T(8,128)(2,1)} %x_ref.1) | copy-start | bytes 393220
  3.1 60.1 %all-to-all-start = ((bf16[16,256,384]{2,1,0:T(8,128)(2,1)}), bf16[16,256,384]{2,1,0:T(8,128)(2,1)S(1)}, u32[]{:S(2)}, u32[]{:S(2)}) async-start(bf16[16,256,384]{2,1,0:T(8,128)(2,1)} %broadcast_in_dim.4), calls=%async_computation | async-start | bytes 6291456 | tf_op jit(solution)/shard_map/all_to_all | solution.py:164
  61.2 2.0 %copy-start = (bf16[32,528,128]{2,1,0:T(8,128)(2,1)}, bf16[32,528,128]{2,1,0:T(8,128)(2,1)S(1)}, u32[]{:S(2)}) copy-start(bf16[32,528,128]{2,1,0:T(8,128)(2,1)S(1)} %convert_element_type.36.x_ref) | copy-start | bytes 12976132
  63.2 2.2 %copy-start.1 = (bf16[32,528,128]{2,1,0:T(8,128)(2,1)S(1)}, bf16[32,528,128]{2,1,0:T(8,128)(2,1)}, u32[]{:S(2)}) copy-start(bf16[32,528,128]{2,1,0:T(8,128)(2,1)} %copy-done) | copy-start | bytes 12976132
  67.2 7.7 %copy-start.9 = (f32[1,15,31]{2,0,1:T(1,128)S(1)}, f32[1,15,31]{2,0,1:T(1,128)}, u32[]{:S(2)}) copy-start(f32[1,15,31]{2,0,1:T(1,128)} %param.16) | copy-start | bytes 5584
  67.2 7.7 %copy-start.10 = (f32[1,15,31]{2,0,1:T(1,128)S(1)}, f32[1,15,31]{2,0,1:T(1,128)}, u32[]{:S(2)}) copy-start(f32[1,15,31]{2,0,1:T(1,128)} %param.21) | copy-start | bytes 5584
  67.2 8.9 %copy-start.6 = (bf16[256,128]{1,0:T(8,128)(2,1)S(1)}, bf16[256,128]{1,0:T(8,128)(2,1)}, u32[]{:S(2)}) copy-start(bf16[256,128]{1,0:T(8,128)(2,1)} %param.20) | copy-start | bytes 196612
  67.2 8.9 %copy-start.7 = (bf16[256,128]{1,0:T(8,128)(2,1)S(1)}, bf16[256,128]{1,0:T(8,128)(2,1)}, u32[]{:S(2)}) copy-start(bf16[256,128]{1,0:T(8,128)(2,1)} %param.19) | copy-start | bytes 196612
  67.2 8.9 %copy-start.8 = (bf16[256,128]{1,0:T(8,128)(2,1)S(1)}, bf16[256,128]{1,0:T(8,128)(2,1)}, u32[]{:S(2)}) copy-start(bf16[256,128]{1,0:T(8,128)(2,1)} %param.18) | copy-start | bytes 196612
  69.0 7.7 %collective-permute-start = (bf16[2,256,128]{2,1,0:T(8,128)(2,1)S(1)}, bf16[2,256,128]{2,1,0:T(8,128)(2,1)S(1)}, u32[]{:S(2)}, u32[]{:S(2)}) collective-permute-start(bf16[2,256,128]{2,1,0:T(8,128)(2,1)S(1)} %get-tuple-element.19.b_ref), channel_id=1, source_target_pairs={{0,32},{32,64},{64,96},{96,128},{128,160},{160,192},{192,224},{224... | collective-permute-start | bytes 393224 | tf_op jit(solution)/shard_map/ppermute | solution.py:152
  72.5 9.5 %collective-permute-start.1 = (bf16[2,256,128]{2,1,0:T(8,128)(2,1)S(1)}, bf16[2,256,128]{2,1,0:T(8,128)(2,1)S(1)}, u32[]{:S(2)}, u32[]{:S(2)}) collective-permute-start(bf16[2,256,128]{2,1,0:T(8,128)(2,1)S(1)} %get-tuple-element.20.a_ref), channel_id=1, source_target_pairs={{32,0},{64,32},{96,64},{128,96},{160,128},{192,160},{224,192},{256... | collective-permute-start | bytes 393224 | tf_op jit(solution)/shard_map/ppermute | solution.py:154
  75.4 0.8 copy-start.4
  87.5 51.1 %all-to-all-start.1 = ((bf16[16,256,384]{2,1,0:T(8,128)(2,1)}), bf16[16,256,384]{2,1,0:T(8,128)(2,1)S(1)}, u32[]{:S(2)}, u32[]{:S(2)}) async-start(bf16[16,256,384]{2,1,0:T(8,128)(2,1)} %broadcast_in_dim.5), calls=%async_computation.1 | async-start | bytes 6291456 | tf_op jit(solution)/shard_map/all_to_all | solution.py:164
  138.6 2.2 %copy-start.2 = (bf16[16384,128]{1,0:T(8,128)(2,1)S(1)}, bf16[16384,128]{1,0:T(8,128)(2,1)}, u32[]{:S(2)}) copy-start(bf16[16384,128]{1,0:T(8,128)(2,1)} %convert_element_type.40) | copy-start | bytes 12582916
  142.6 14.7 %copy-start.5 = (f32[14,64,128]{2,1,0:T(8,128)S(1)}, f32[14,64,128]{2,1,0:T(8,128)}, u32[]{:S(2)}) copy-start(f32[14,64,128]{2,1,0:T(8,128)} %copy-done.4) | copy-start | bytes 1376260
  144.5 7.6 %collective-permute-start.2 = (bf16[2,256,128]{2,1,0:T(8,128)(2,1)S(1)}, bf16[2,256,128]{2,1,0:T(8,128)(2,1)S(1)}, u32[]{:S(2)}, u32[]{:S(2)}) collective-permute-start(bf16[2,256,128]{2,1,0:T(8,128)(2,1)S(1)} %get-tuple-element.26.b_ref), channel_id=1, source_target_pairs={{0,32},{32,64},{64,96},{96,128},{128,160},{160,192},{192,224},{224... | collective-permute-start | bytes 393224 | tf_op jit(solution)/shard_map/ppermute | solution.py:152
  147.9 9.5 %collective-permute-start.3 = (bf16[2,256,128]{2,1,0:T(8,128)(2,1)S(1)}, bf16[2,256,128]{2,1,0:T(8,128)(2,1)S(1)}, u32[]{:S(2)}, u32[]{:S(2)}) collective-permute-start(bf16[2,256,128]{2,1,0:T(8,128)(2,1)S(1)} %get-tuple-element.27.a_ref), channel_id=1, source_target_pairs={{32,0},{64,32},{96,64},{128,96},{160,128},{192,160},{224,192},{256... | collective-permute-start | bytes 393224 | tf_op jit(solution)/shard_map/ppermute | solution.py:154

commit v4 on v3

--- a/solution.py
+++ b/solution.py
@@ -2,11 +2,11 @@
 
 import jax
 import jax.numpy as jnp
-import numpy as np
 from jax import lax
 from jax.experimental import pallas as pl
 from jax.experimental.pallas import tpu as pltpu
 from jax.sharding import PartitionSpec as P
+
 
 GRID_W = 64
 EPSILON = 1e-06
@@ -23,32 +23,29 @@
     return pl.BlockSpec(memory_space=pltpu.VMEM)
 
 
-def bias_kernel(first_ref, second_ref, first_out, second_out):
+def bias_kernel(table_ref, out_ref):
     width = GRID_W
     col = lax.broadcasted_iota(jnp.int32, (width, 2 * width), 0)
     key = lax.broadcasted_iota(jnp.int32, (width, 2 * width), 1) % width
     start = jnp.clip(col - 8, 0, width - 16)
     inside = (key >= start) & (key < start + 16)
-    for table_ref, out_ref in ((first_ref, first_out), (second_ref, second_out)):
-        table = table_ref[0]
-        low = jnp.pad(table, ((0, 1), (0, 2 * width - 31)))
-        both = low + pltpu.roll(pltpu.roll(low, 15, 0), width, 1)
-        for m in range(14):
-            row = jnp.broadcast_to(both[m : m + 1, :], (width, 2 * width))
-            turned = pltpu.roll(row, 2 * width - 15, 1, stride=1, stride_axis=0)
-            out_ref[m] = jnp.where(inside, turned, MASKED)
-
-
-def biases(first, second):
-    shape = jax.ShapeDtypeStruct((14, GRID_W, 2 * GRID_W), jnp.float32)
+    low = jnp.pad(table_ref[0], ((0, 1), (0, 2 * width - table_ref.shape[2])))
+    both = low + pltpu.roll(pltpu.roll(low, 15, 0), width, 1)
+    for m in range(14):
+        row = jnp.broadcast_to(both[m : m + 1, :], (width, 2 * width))
+        turned = pltpu.roll(row, 2 * width - 15, 1, stride=1, stride_axis=0)
+        out_ref[m] = jnp.where(inside, turned, MASKED)
+
+
+def bias_of(table):
     return pl.pallas_call(
         bias_kernel,
-        out_shape=(shape, shape),
-        in_specs=[vmem(), vmem()],
-        out_specs=(vmem(), vmem()),
+        out_shape=jax.ShapeDtypeStruct((14, GRID_W, 2 * GRID_W), jnp.float32),
+        in_specs=[vmem()],
+        out_specs=vmem(),
         compiler_params=pltpu.CompilerParams(vmem_limit_bytes=ATTEND_VMEM),
-        name="biases",
-    )(first, second)
+        name="bias",
+    )(table)
 
 
 def project_kernel(half, gain_row, scale, x_ref, gain_ref, w_ref, q_ref, kv_ref, normed):
@@ -143,7 +140,7 @@
     )(at, *queries, low, *own, high, bias, x)
 
 
-def layer(x, gathered, gain_row, scale, gains, weights, bias, at):
+def layer(x, gathered, gain_row, scale, gains, weights, table, at, following=None):
     tokens = x.shape[0]
     count = lax.axis_size("sp")
     forward = [(i, i + 1) for i in range(count - 1)]
@@ -152,7 +149,12 @@
     low = lax.ppermute(own_high, "sp", forward)
     query_low, own_low = project(0, gain_row, scale, gathered, gains, weights, tokens)
     high = lax.ppermute(own_low, "sp", backward)
-    return attend(at, (query_low, query_high), low, (own_low, own_high), high, bias, x)
+    if following is not None:
+        query_low, following = lax.optimization_barrier((query_low, following))
+        following = spread(following)
+    bias = bias_of(table)
+    out = attend(at, (query_low, query_high), low, (own_low, own_high), high, bias, x)
+    return out, following
 
 
 def replicated(weights):
@@ -178,25 +180,28 @@
     value_second,
     offset_second,
 ):
-    tokens, size = stream.shape
+    tokens, _ = stream.shape
     rows = tokens // GRID_W
     first_set = spread(replicated((query_first, key_first, value_first)))
     second_blocks = replicated((query_second, key_second, value_second))
-    bias_first, bias_second = biases(offset_first, offset_second)
     start = lax.axis_index("sp") * rows
     total_rows = rows * lax.axis_size("sp")
     at = jnp.stack([start, jnp.int32(total_rows - WINDOW_ROWS)]).astype(jnp.int32)
 
-    gains = jnp.pad(jnp.stack([gain_first, gain_second]), ((0, 14), (0, 0)))
+    gains = jnp.pad(jnp.stack([gain_first, gain_second]), ((0, 6), (0, 0)))
     sent = (jnp.concatenate([stream, gains]).astype(jnp.float32) * SCALE_FIRST).astype(jnp.float16)
-    held = lax.all_gather(sent, "tp", axis=0, tiled=False).astype(jnp.bfloat16)
+    held = lax.all_gather(sent, "tp", axis=0, tiled=False)
+    held, first_set = lax.optimization_barrier((held, first_set))
+    held = held.astype(jnp.bfloat16)
     gains = held[:, tokens:]
-    middle = layer(stream, held, 0, SCALE_FIRST, gains, first_set, bias_first, at)
-    middle, second_blocks = lax.optimization_barrier((middle, second_blocks))
-    second_set = spread(second_blocks)
+    middle, second_set = layer(
+        stream, held, 0, SCALE_FIRST, gains, first_set, offset_first, at, second_blocks
+    )
     sent = (middle.astype(jnp.float32) * SCALE_SECOND).astype(jnp.float16)
-    again = lax.all_gather(sent, "tp", axis=0, tiled=False).astype(jnp.bfloat16)
-    return layer(middle, again, 1, SCALE_SECOND, gains, second_set, bias_second, at)
+    again = lax.all_gather(sent, "tp", axis=0, tiled=False)
+    again, second_set = lax.optimization_barrier((again, second_set))
+    again = again.astype(jnp.bfloat16)
+    return layer(middle, again, 1, SCALE_SECOND, gains, second_set, offset_second, at)[0]
 
 
 def solution(mesh):

time: 162 us -> 204 us (1.26)
  waiting for transfers between devices: 12.8 us -> 41 us
  other arithmetic: 4.04 us -> 8.91 us
  local copies, waits for them, and re-layouts: 11.4 us -> 14.5 us
  blocking collectives: 90.4 us -> 93 us
    ppermute x2, waiting for transfers between devices: 2.23 us -> 35.5 us  [layer(): low = lax.ppermute(own_high, 'sp', forward)]
    ppermute x2, waiting for transfers between devices: 10.6 us -> 5.5 us  [layer(): high = lax.ppermute(own_low, 'sp', backward)]
    convert_element_type x2, other arithmetic: 2.91 us -> 7.1 us  [the longest x1 4.07 us: body(): held = held.astype(jnp.bfloat16)]
    unnamed x28 -> x40, local copies, waits for them, and re-layouts: 7.22 us -> 10.4 us
    all_gather x2, blocking collectives: 90.4 us -> 93 us  [the longest x1 49.2 us: body(): held = lax.all_gather(sent, 'tp', axis=0, tiled=False)]
  transfers between devices with their start and end apart: 6 -> 6, of which waited for: 4 -> 3; matrix products, arithmetic and copies ran while one was open for 2% -> 0% of each run, Pallas kernels for 0% -> 3%
where the time goes in v4:
time: 204 us; the launch traced here: 203 us
  blocking collectives  93 us (46%)
  waiting for transfers between devices  41 us (20%)
  starting transfers between devices  28.5 us (14%)
  Pallas kernels  16.4 us (8%)
  local copies, waits for them, and re-layouts  14.5 us (7%)
  other arithmetic  8.91 us (4%)
    all_gather x1, blocking collectives, body(): held = lax.all_gather(sent, 'tp', axis=0, tiled=False)  49.2 us
    all_gather x1, blocking collectives, body(): again = lax.all_gather(sent, 'tp', axis=0, tiled=False)  43.8 us
    ppermute x2, waiting for transfers between devices, layer(): low = lax.ppermute(own_high, 'sp', forward)  35.5 us
    all_to_all x2, starting transfers between devices, spread(): got = lax.all_to_all(blocks, 'sp', 0, 0, tiled=True)  16.8 us
    unnamed x40, local copies, waits for them, and re-layouts  10.4 us
    pallas_call x4, Pallas kernels, project(): pl.pallas_call(functools.partial(project_kernel, half, gain_row, scale),...  8 us
    pallas_call x2, Pallas kernels, attend(): pl.pallas_call(attend_kernel, out_shape=jax.ShapeDtypeStruct((tokens, siz...  7.93 us
    ppermute x2, starting transfers between devices, layer(): low = lax.ppermute(own_high, 'sp', forward)  7.02 us
  transfers between devices with their start and end apart: 6, of which 3 were waited for; matrix products, arithmetic and copies ran while one was open for 0% of the time, Pallas kernels for 3%

profile of v4, /device:TPU:6, one launch (start us, length us, event | category | flops | bytes accessed | tf_op | source)
XLA Modules:
  0.0 202.7 jit_solution(14008650651329188578)
XLA Ops:
  0.0 0.9 pad_maximum_fusion
  0.9 0.0 copy-start.17
  0.9 0.0 copy-start.18
  1.0 0.0 copy-start.6
  1.0 0.0 copy-start.12
  1.0 0.0 copy-start.13
  1.0 0.0 copy-start.14
  1.0 2.1 %broadcast_in_dim.4 = bf16[16,256,384]{2,1,0:T(8,128)(2,1)} broadcast(bf16[256,384]{1,0:T(8,128)(2,1)S(1)} %pad_maximum_fusion), dimensions={1,2} | broadcast | bytes 3342336 | tf_op jit(solution)/shard_map/broadcast_in_dim | solution.py:162
  3.1 9.4 %all-to-all-start = ((bf16[16,256,384]{2,1,0:T(8,128)(2,1)}), bf16[16,256,384]{2,1,0:T(8,128)(2,1)S(1)}, u32[]{:S(2)}, u32[]{:S(2)}) async-start(bf16[16,256,384]{2,1,0:T(8,128)(2,1)} %broadcast_in_dim.4), calls=%async_computation | async-start | bytes 6291456 | tf_op jit(solution)/shard_map/all_to_all | solution.py:166
  12.5 0.0 copy-done.6
  12.5 0.7 pad_maximum_fusion.1
  13.3 49.2 %all-gather.3 = f16[32,520,128]{2,1,0:T(8,128)(2,1)} all-gather(f16[1,520,128]{2,1,0:T(8,128)(2,1)S(1)} %multiply_convert_fusion), channel_id=1, replica_groups=mesh['sp'=16,'tp'=32] {'tp'}, dimensions={0}, use_global_device_ids=true | all-gather | bytes 4392960 | tf_op jit(solution)/shard_map/all_gather | solution.py:193
  62.5 0.0 all-to-all-done
  62.5 4.1 %convert_element_type.36.x_ref = bf16[32,520,128]{2,1,0:T(8,128)(2,1)S(1)} convert(f16[32,520,128]{2,1,0:T(8,128)(2,1)} %all-gather.3) | non-fusion elementwise | flops 2129920 | bytes 8519680 | tf_op jit(solution)/shard_map/convert_element_type | solution.py:195
  66.6 1.9 project.4
  68.5 2.1 %copy-done = bf16[32,520,128]{2,1,0:T(8,128)(2,1)} copy-done((bf16[32,520,128]{2,1,0:T(8,128)(2,1)}, bf16[32,520,128]{2,1,0:T(8,128)(2,1)S(1)}, u32[]{:S(2)}) %copy-start) | copy-done | bytes 4259864
  70.6 0.0 copy-done.11
  70.6 2.0 %broadcast_in_dim.5 = bf16[16,256,384]{2,1,0:T(8,128)(2,1)} broadcast(bf16[256,384]{1,0:T(8,128)(2,1)S(1)} %copy-done.11), dimensions={1,2} | broadcast | bytes 3342336 | tf_op jit(solution)/shard_map/broadcast_in_dim | solution.py:162
  72.6 7.4 %all-to-all-start.1 = ((bf16[16,256,384]{2,1,0:T(8,128)(2,1)}), bf16[16,256,384]{2,1,0:T(8,128)(2,1)S(1)}, u32[]{:S(2)}, u32[]{:S(2)}) async-start(bf16[16,256,384]{2,1,0:T(8,128)(2,1)} %broadcast_in_dim.5), calls=%async_computation.1 | async-start | bytes 6291456 | tf_op jit(solution)/shard_map/all_to_all | solution.py:166
  80.1 2.2 %copy-done.1 = bf16[32,520,128]{2,1,0:T(8,128)(2,1)S(1)} copy-done((bf16[32,520,128]{2,1,0:T(8,128)(2,1)S(1)}, bf16[32,520,128]{2,1,0:T(8,128)(2,1)}, u32[]{:S(2)}) %copy-start.1) | copy-done | bytes 4259864
  82.3 1.9 copy-done.3
  84.2 2.5 %project.5 = (bf16[256,128]{1,0:T(8,128)(2,1)S(1)}, bf16[2,256,128]{2,1,0:T(8,128)(2,1)}) custom-call(bf16[32,520,128]{2,1,0:T(8,128)(2,1)S(1)} %copy-done.1, bf16[32,8,128]{2,1,0:T(8,128)(2,1)S(1)} %slice.4.gain_ref, bf16[4096,384]{1,0:T(8,128)(2,1)S(1)} %bitcast.12), custom_call_target="tpu_custom_call" | custom-call | flops 805306368 | bytes 8388608 | tf_op jit(solution)/shard_map/project/pallas_call | solution.py:74
  86.6 0.6 copy-done.9
  87.3 3.4 %collective-permute-start = (bf16[2,256,128]{2,1,0:T(8,128)(2,1)}, bf16[2,256,128]{2,1,0:T(8,128)(2,1)}, u32[]{:S(2)}, u32[]{:S(2)}) collective-permute-start(bf16[2,256,128]{2,1,0:T(8,128)(2,1)} %get-tuple-element.24.b_ref), channel_id=1, source_target_pairs={{0,32},{32,64},{64,96},{96,128},{128,160},{160,192},{192,224},{224... | collective-permute-start | bytes 393224 | tf_op jit(solution)/shard_map/ppermute | solution.py:149
  90.7 2.5 %collective-permute-start.1 = (bf16[2,256,128]{2,1,0:T(8,128)(2,1)S(1)}, bf16[2,256,128]{2,1,0:T(8,128)(2,1)}, u32[]{:S(2)}, u32[]{:S(2)}) collective-permute-start(bf16[2,256,128]{2,1,0:T(8,128)(2,1)S(1)} %get-tuple-element.25.a_ref), channel_id=1, source_target_pairs={{32,0},{64,32},{96,64},{128,96},{160,128},{192,160},{224,192},{256... | collective-permute-start | bytes 393224 | tf_op jit(solution)/shard_map/ppermute | solution.py:151
  93.1 0.0 copy-done.15
  93.2 0.3 bias.2.bias_ref
  93.4 0.0 copy-start.4
  93.4 0.8 copy-done.4
  94.2 0.1 pad_add_fusion.at_ref
  94.3 34.0 %collective-permute-done.low_ref = bf16[2,256,128]{2,1,0:T(8,128)(2,1)} collective-permute-done((bf16[2,256,128]{2,1,0:T(8,128)(2,1)}, bf16[2,256,128]{2,1,0:T(8,128)(2,1)}, u32[]{:S(2)}, u32[]{:S(2)}) %collective-permute-start) | collective-permute-done | bytes 131104 | tf_op jit(solution)/shard_map/ppermute | solution.py:149
  128.3 0.0 collective-permute-done.1.high_ref
  128.3 1.0 copy-done.5
  129.3 0.9 copy-done.8
  130.2 0.8 copy-done.10
  131.0 3.9 %attend.2.x_ref = bf16[512,128]{1,0:T(8,128)(2,1)S(1)} custom-call(s32[2]{0:T(128)S(1)} %pad_add_fusion.at_ref, bf16[256,128]{1,0:T(8,128)(2,1)S(1)} %get-tuple-element.22.qa_ref, bf16[256,128]{1,0:T(8,128)(2,1)S(1)} %copy-done.10, bf16[2,256,128]{2,1,0:T(8,128)(2,1)} %collective-permute-done.low_ref, bf16[2,256,128]{2,1,0:T(8,128)(2,1)S(1)} %copy-done.8, ...), custom_call_target="tpu_custom_call" | custom-call | flops 134217728 | bytes 2097152 | tf_op jit(solution)/shard_map/attend/pallas_call | solution.py:129
  135.0 43.8 %all-gather.4 = f16[16384,128]{1,0:T(8,128)(2,1)} all-gather(f16[512,128]{1,0:T(8,128)(2,1)S(1)} %multiply_convert_fusion.1), channel_id=2, replica_groups=mesh['sp'=16,'tp'=32] {'tp'}, dimensions={0}, use_global_device_ids=true | all-gather | bytes 4325376 | tf_op jit(solution)/shard_map/all_gather | solution.py:201
  178.8 0.0 all-to-all-done.1
  178.8 3.0 %convert_element_type.39.x_ref = bf16[32,512,128]{2,1,0:T(8,128)(2,1)S(1)} convert(f16[32,512,128]{2,1,0:T(8,128)(2,1)} %bitcast.14) | non-fusion elementwise | flops 2097152 | bytes 8388608 | tf_op jit(solution)/shard_map/convert_element_type | solution.py:203
  181.8 1.8 project.7
  183.7 0.0 copy-start.16
  183.7 1.8 project.6
  185.5 3.7 %collective-permute-start.2 = (bf16[2,256,128]{2,1,0:T(8,128)(2,1)S(1)}, bf16[2,256,128]{2,1,0:T(8,128)(2,1)S(1)}, u32[]{:S(2)}, u32[]{:S(2)}) collective-permute-start(bf16[2,256,128]{2,1,0:T(8,128)(2,1)S(1)} %get-tuple-element.31.b_ref), channel_id=1, source_target_pairs={{0,32},{32,64},{64,96},{96,128},{128,160},{160,192},{192,224},{224... | collective-permute-start | bytes 393224 | tf_op jit(solution)/shard_map/ppermute | solution.py:149
  189.2 2.2 %collective-permute-start.3 = (bf16[2,256,128]{2,1,0:T(8,128)(2,1)S(1)}, bf16[2,256,128]{2,1,0:T(8,128)(2,1)S(1)}, u32[]{:S(2)}, u32[]{:S(2)}) collective-permute-start(bf16[2,256,128]{2,1,0:T(8,128)(2,1)S(1)} %get-tuple-element.32.a_ref), channel_id=1, source_target_pairs={{32,0},{64,32},{96,64},{128,96},{160,128},{192,160},{224,192},{256... | collective-permute-start | bytes 393224 | tf_op jit(solution)/shard_map/ppermute | solution.py:151
  191.4 0.3 bias.3.bias_ref
  191.7 1.5 collective-permute-done.2.low_ref
  193.2 5.5 %collective-permute-done.3.high_ref = bf16[2,256,128]{2,1,0:T(8,128)(2,1)S(1)} collective-permute-done((bf16[2,256,128]{2,1,0:T(8,128)(2,1)S(1)}, bf16[2,256,128]{2,1,0:T(8,128)(2,1)S(1)}, u32[]{:S(2)}, u32[]{:S(2)}) %collective-permute-start.3) | collective-permute-done | bytes 131104 | tf_op jit(solution)/shard_map/ppermute | solution.py:151
  198.7 4.0 %attend.3 = bf16[512,128]{1,0:T(8,128)(2,1)} custom-call(s32[2]{0:T(128)S(1)} %pad_add_fusion.at_ref, bf16[256,128]{1,0:T(8,128)(2,1)S(1)} %get-tuple-element.29.qa_ref, bf16[256,128]{1,0:T(8,128)(2,1)S(1)} %get-tuple-element.30.qb_ref, bf16[2,256,128]{2,1,0:T(8,128)(2,1)S(1)} %collective-permute-done.2.low_ref, ...), custom_call_target="tpu_custom_call" | custom-call | flops 134217728 | bytes 2097152 | tf_op jit(solution)/shard_map/attend/pallas_call | solution.py:129
  (25 shorter events, 0.1 us)
Async XLA Ops:
  0.9 11.5 %copy-start.17 = (bf16[128]{0:T(256)(128)(2,1)S(1)}, bf16[128]{0:T(256)(128)(2,1)}, u32[]{:S(2)}) copy-start(bf16[128]{0:T(256)(128)(2,1)} %param.17) | copy-start | bytes 772
  0.9 11.5 %copy-start.18 = (bf16[128]{0:T(256)(128)(2,1)S(1)}, bf16[128]{0:T(256)(128)(2,1)}, u32[]{:S(2)}) copy-start(bf16[128]{0:T(256)(128)(2,1)} %param.12) | copy-start | bytes 772
  1.0 11.5 %copy-start.6 = (bf16[512,128]{1,0:T(8,128)(2,1)S(1)}, bf16[512,128]{1,0:T(8,128)(2,1)}, u32[]{:S(2)}) copy-start(bf16[512,128]{1,0:T(8,128)(2,1)} %x_ref.1) | copy-start | bytes 393220
  1.0 11.6 %copy-start.12 = (bf16[256,128]{1,0:T(8,128)(2,1)S(1)}, bf16[256,128]{1,0:T(8,128)(2,1)}, u32[]{:S(2)}) copy-start(bf16[256,128]{1,0:T(8,128)(2,1)} %param.20) | copy-start | bytes 196612
  1.0 11.5 %copy-start.13 = (bf16[256,128]{1,0:T(8,128)(2,1)S(1)}, bf16[256,128]{1,0:T(8,128)(2,1)}, u32[]{:S(2)}) copy-start(bf16[256,128]{1,0:T(8,128)(2,1)} %param.19) | copy-start | bytes 196612
  1.0 11.5 %copy-start.14 = (bf16[256,128]{1,0:T(8,128)(2,1)S(1)}, bf16[256,128]{1,0:T(8,128)(2,1)}, u32[]{:S(2)}) copy-start(bf16[256,128]{1,0:T(8,128)(2,1)} %param.18) | copy-start | bytes 196612
  3.1 59.4 %all-to-all-start = ((bf16[16,256,384]{2,1,0:T(8,128)(2,1)}), bf16[16,256,384]{2,1,0:T(8,128)(2,1)S(1)}, u32[]{:S(2)}, u32[]{:S(2)}) async-start(bf16[16,256,384]{2,1,0:T(8,128)(2,1)} %broadcast_in_dim.4), calls=%async_computation | async-start | bytes 6291456 | tf_op jit(solution)/shard_map/all_to_all | solution.py:166
  62.5 4.1 %copy-start.2 = (bf16[16,256,384]{2,1,0:T(8,128)(2,1)}, bf16[16,256,384]{2,1,0:T(8,128)(2,1)S(1)}, u32[]{:S(2)}) copy-start(bf16[16,256,384]{2,1,0:T(8,128)(2,1)S(1)} %all-to-all-done) | copy-start | bytes 9437188
  66.6 4.0 %copy-start.11 = (bf16[256,384]{1,0:T(8,128)(2,1)S(1)}, bf16[256,384]{1,0:T(8,128)(2,1)}, u32[]{:S(2)}) copy-start(bf16[256,384]{1,0:T(8,128)(2,1)} %pad_maximum_fusion.1) | copy-start | bytes 589828
  68.5 2.1 %copy-start = (bf16[32,520,128]{2,1,0:T(8,128)(2,1)}, bf16[32,520,128]{2,1,0:T(8,128)(2,1)S(1)}, u32[]{:S(2)}) copy-start(bf16[32,520,128]{2,1,0:T(8,128)(2,1)S(1)} %convert_element_type.36.x_ref) | copy-start | bytes 12779524
  70.6 20.1 %copy-start.7 = (bf16[2,256,128]{2,1,0:T(8,128)(2,1)}, bf16[2,256,128]{2,1,0:T(8,128)(2,1)S(1)}, u32[]{:S(2)}) copy-start(bf16[2,256,128]{2,1,0:T(8,128)(2,1)S(1)} %get-tuple-element.25.a_ref) | copy-start | bytes 393220
  72.6 106.2 %all-to-all-start.1 = ((bf16[16,256,384]{2,1,0:T(8,128)(2,1)}), bf16[16,256,384]{2,1,0:T(8,128)(2,1)S(1)}, u32[]{:S(2)}, u32[]{:S(2)}) async-start(bf16[16,256,384]{2,1,0:T(8,128)(2,1)} %broadcast_in_dim.5), calls=%async_computation.1 | async-start | bytes 6291456 | tf_op jit(solution)/shard_map/all_to_all | solution.py:166
  80.1 2.2 %copy-start.1 = (bf16[32,520,128]{2,1,0:T(8,128)(2,1)S(1)}, bf16[32,520,128]{2,1,0:T(8,128)(2,1)}, u32[]{:S(2)}) copy-start(bf16[32,520,128]{2,1,0:T(8,128)(2,1)} %copy-done) | copy-start | bytes 12779524
  82.3 1.9 copy-start.3
  84.2 9.0 %copy-start.15 = (f32[1,15,31]{2,0,1:T(1,128)S(1)}, f32[1,15,31]{2,0,1:T(1,128)}, u32[]{:S(2)}) copy-start(f32[1,15,31]{2,0,1:T(1,128)} %param.16) | copy-start | bytes 5584
  86.6 0.6 copy-start.9
  87.3 41.0 %collective-permute-start = (bf16[2,256,128]{2,1,0:T(8,128)(2,1)}, bf16[2,256,128]{2,1,0:T(8,128)(2,1)}, u32[]{:S(2)}, u32[]{:S(2)}) collective-permute-start(bf16[2,256,128]{2,1,0:T(8,128)(2,1)} %get-tuple-element.24.b_ref), channel_id=1, source_target_pairs={{0,32},{32,64},{64,96},{96,128},{128,160},{160,192},{192,224},{224... | collective-permute-start | bytes 393224 | tf_op jit(solution)/shard_map/ppermute | solution.py:149
  90.7 37.6 %collective-permute-start.1 = (bf16[2,256,128]{2,1,0:T(8,128)(2,1)S(1)}, bf16[2,256,128]{2,1,0:T(8,128)(2,1)}, u32[]{:S(2)}, u32[]{:S(2)}) collective-permute-start(bf16[2,256,128]{2,1,0:T(8,128)(2,1)S(1)} %get-tuple-element.25.a_ref), channel_id=1, source_target_pairs={{32,0},{64,32},{96,64},{128,96},{160,128},{192,160},{224,192},{256... | collective-permute-start | bytes 393224 | tf_op jit(solution)/shard_map/ppermute | solution.py:151
  93.4 0.8 copy-start.4
  128.3 1.0 copy-start.5
  129.3 0.9 copy-start.8
  130.2 0.8 copy-start.10
  183.7 7.7 %copy-start.16 = (f32[1,15,31]{2,0,1:T(1,128)S(1)}, f32[1,15,31]{2,0,1:T(1,128)}, u32[]{:S(2)}) copy-start(f32[1,15,31]{2,0,1:T(1,128)} %param.21) | copy-start | bytes 5584
  185.5 7.7 %collective-permute-start.2 = (bf16[2,256,128]{2,1,0:T(8,128)(2,1)S(1)}, bf16[2,256,128]{2,1,0:T(8,128)(2,1)S(1)}, u32[]{:S(2)}, u32[]{:S(2)}) collective-permute-start(bf16[2,256,128]{2,1,0:T(8,128)(2,1)S(1)} %get-tuple-element.31.b_ref), channel_id=1, source_target_pairs={{0,32},{32,64},{64,96},{96,128},{128,160},{160,192},{192,224},{224... | collective-permute-start | bytes 393224 | tf_op jit(solution)/shard_map/ppermute | solution.py:149
  189.2 9.5 %collective-permute-start.3 = (bf16[2,256,128]{2,1,0:T(8,128)(2,1)S(1)}, bf16[2,256,128]{2,1,0:T(8,128)(2,1)S(1)}, u32[]{:S(2)}, u32[]{:S(2)}) collective-permute-start(bf16[2,256,128]{2,1,0:T(8,128)(2,1)S(1)} %get-tuple-element.32.a_ref), channel_id=1, source_target_pairs={{32,0},{64,32},{96,64},{128,96},{160,128},{192,160},{224,192},{256... | collective-permute-start | bytes 393224 | tf_op jit(solution)/shard_map/ppermute | solution.py:151

commit v5 on v4

v5 whole, which is shorter than its diff:
```python
import functools

import jax
import jax.numpy as jnp
from jax import lax
from jax.experimental import pallas as pl
from jax.experimental.pallas import tpu as pltpu
from jax.sharding import PartitionSpec as P


GRID_W = 64
EPSILON = 1e-06
SCALE_FIRST = 2.0**13
SCALE_SECOND = 2.0**6
WINDOW_ROWS = 8
HALO = 4
MASKED = -1e30
PROJECT_VMEM = 63_000_000
ATTEND_VMEM = 12 << 20
COPIES_VMEM = 66_000_000


def vmem():
    return pl.BlockSpec(memory_space=pltpu.VMEM)


def bias_kernel(table_ref, out_ref):
    width = GRID_W
    col = lax.broadcasted_iota(jnp.int32, (width, 2 * width), 0)
    key = lax.broadcasted_iota(jnp.int32, (width, 2 * width), 1) % width
    start = jnp.clip(col - 8, 0, width - 16)
    inside = (key >= start) & (key < start + 16)
    low = jnp.pad(table_ref[0], ((0, 1), (0, 2 * width - table_ref.shape[2])))
    both = low + pltpu.roll(pltpu.roll(low, 15, 0), width, 1)
    for m in range(14):
        row = jnp.broadcast_to(both[m : m + 1, :], (width, 2 * width))
        turned = pltpu.roll(row, 2 * width - 15, 1, stride=1, stride_axis=0)
        out_ref[m] = jnp.where(inside, turned, MASKED)


def bias_of(table):
    return pl.pallas_call(
        bias_kernel,
        out_shape=jax.ShapeDtypeStruct((14, GRID_W, 2 * GRID_W), jnp.float32),
        in_specs=[vmem()],
        out_specs=vmem(),
        compiler_params=pltpu.CompilerParams(vmem_limit_bytes=ATTEND_VMEM),
        name="bias",
    )(table)


def core_of_chip():
    return lax.rem(lax.axis_index("tp"), 2)


def project_kernel(gain_row, scale, x_hbm, gain_ref, w_ref, q_ref, a_ref, b_ref, x_ref, normed, sems):
    blocks, tokens, size = x_ref.shape
    half = tokens // 2
    core = core_of_chip()
    copies = [
        pltpu.make_async_copy(x_hbm.at[f, pl.ds(0, tokens)], x_ref.at[f], sems.at[f])
        for f in range(blocks)
    ]
    for copy in copies:
        copy.start()
    total = jnp.zeros((tokens, size), jnp.float32)
    for f in range(blocks):
        copies[f].wait()
        part = x_ref[f].astype(jnp.float32)
        total = total + part * part
    mean = jnp.sum(total, axis=1, keepdims=True) * (1.0 / (blocks * size * scale * scale))
    rate = lax.rsqrt(mean + EPSILON) * (1.0 / scale)
    for f in range(blocks):
        part = x_ref[f].astype(jnp.float32)
        gain = gain_ref[f, gain_row : gain_row + 1, :].astype(jnp.float32) * (1.0 / SCALE_FIRST)
        normed[:, f * size : (f + 1) * size] = (part * rate * gain).astype(jnp.bfloat16)
    for out_ref, number in ((a_ref, 1 - core), (b_ref, core)):
        rows = pl.ds(pl.multiple_of(number * half, half), half)
        out = jnp.dot(normed[rows, :], w_ref[...], preferred_element_type=jnp.float32)
        out = out.astype(jnp.bfloat16)
        q_ref[rows, :] = out[:, :size]
        out_ref[0] = out[:, size : 2 * size]
        out_ref[1] = out[:, 2 * size :]


def project(gain_row, scale, x, gain, weights, tokens):
    blocks, _, size = x.shape
    kv = jax.ShapeDtypeStruct((2, tokens // 2, size), jnp.bfloat16)
    return pl.pallas_call(
        functools.partial(project_kernel, gain_row, scale),
        out_shape=(jax.ShapeDtypeStruct((tokens, size), jnp.bfloat16), kv, kv),
        in_specs=[pl.BlockSpec(memory_space=pltpu.HBM), vmem(), vmem()],
        out_specs=(vmem(),) * 3,
        scratch_shapes=[
            pltpu.VMEM((blocks, tokens, size), jnp.bfloat16),
            pltpu.VMEM((tokens, blocks * size), jnp.bfloat16),
            pltpu.SemaphoreType.DMA((blocks,)),
        ],
        cost_estimate=pl.CostEstimate(
            flops=2 * tokens * blocks * size * 3 * size, bytes_accessed=8 << 20, transcendentals=0
        ),
        compiler_params=pltpu.CompilerParams(vmem_limit_bytes=PROJECT_VMEM),
        name="project",
    )(x, gain, weights)


def attend_kernel(last, q_ref, a_in, a_own, b_own, b_in, bias_ref, x_ref, out_ref, keys, values):
    width = GRID_W
    tokens, size = q_ref.shape
    half = tokens // 2
    rows = tokens // width
    core = core_of_chip()
    row_start = lax.axis_index("sp") * rows
    placed = (
        (a_in, core * 3),
        (a_own, 2 - core),
        (b_own, 1 + core),
        (b_in, (1 - core) * 3),
    )
    for ref, number in placed:
        span = pl.ds(pl.multiple_of(number * half, half), half)
        keys[span, :] = ref[0]
        values[span, :] = ref[1]
    factor = size ** (-0.5)
    spans, scored = [], []
    for r in range(rows):
        grid_row = row_start + r
        first = jnp.clip(grid_row - HALO, 0, last)
        at = pl.multiple_of((first - row_start + HALO) * width, width)
        offset = first - grid_row + 7
        spans.append(pl.ds(at, WINDOW_ROWS * width))
        scores = lax.dot_general(
            q_ref[r * width : (r + 1) * width, :],
            keys[spans[r], :],
            (((1,), (1,)), ((), ())),
            preferred_element_type=jnp.float32,
        )
        scored.append(
            [
                scores[:, 2 * p * width : 2 * (p + 1) * width] * factor + bias_ref[offset + 2 * p]
                for p in range(WINDOW_ROWS // 2)
            ]
        )
    weights = []
    for parts in scored:
        top = jnp.max(functools.reduce(jnp.maximum, parts), axis=1, keepdims=True)
        parts = [jnp.exp(part - top) for part in parts]
        total = jnp.sum(functools.reduce(jnp.add, parts), axis=1, keepdims=True)
        inverse = 1.0 / total
        weights.append(jnp.concatenate([(part * inverse).astype(jnp.bfloat16) for part in parts], 1))
    for r in range(rows):
        attended = jnp.dot(weights[r], values[spans[r], :], preferred_element_type=jnp.float32)
        here = slice(r * width, (r + 1) * width)
        out_ref[here, :] = (x_ref[here, :].astype(jnp.float32) + attended).astype(jnp.bfloat16)


def attend(last, query, a_in, a_own, b_own, b_in, bias, x):
    tokens, size = x.shape
    return pl.pallas_call(
        functools.partial(attend_kernel, last),
        out_shape=jax.ShapeDtypeStruct((tokens, size), jnp.bfloat16),
        in_specs=[vmem()] * 7,
        out_specs=vmem(),
        scratch_shapes=[pltpu.VMEM((2 * tokens, size), jnp.bfloat16)] * 2,
        cost_estimate=pl.CostEstimate(
            flops=4 * tokens * size * WINDOW_ROWS * GRID_W, bytes_accessed=2 << 20, transcendentals=tokens * 512
        ),
        compiler_params=pltpu.CompilerParams(vmem_limit_bytes=ATTEND_VMEM),
        name="attend",
    )(query, a_in, a_own, b_own, b_in, bias, x)


def halo_pairs(first):
    count, across = lax.axis_size("sp"), lax.axis_size("tp")
    pairs = []
    for s in range(count):
        for t in range(across):
            target = s + 1 if (t % 2 == 0) == first else s - 1
            if 0 <= target < count:
                pairs.append((s * across + t, target * across + t))
    return pairs


def layer(x, gathered, gain_row, scale, gains, weights, table, following=None):
    tokens = x.shape[0]
    last = lax.axis_size("sp") * tokens // GRID_W - WINDOW_ROWS
    query, a_own, b_own = project(gain_row, scale, gathered, gains, weights, tokens)
    a_in = lax.ppermute(a_own, ("sp", "tp"), halo_pairs(True))
    b_in = lax.ppermute(b_own, ("sp", "tp"), halo_pairs(False))
    if following is not None:
        query, *following = lax.optimization_barrier((query, *following))
        following = spread(following)
    bias = bias_of(table)
    out = attend(last, query, a_in, a_own, b_own, b_in, bias, x)
    return out, following


def copies_kernel(first_ref, second_ref, third_ref, out_ref, block, sems):
    size = first_ref.shape[1]
    for i, ref in enumerate((first_ref, second_ref, third_ref)):
        block[:, i * size : (i + 1) * size] = ref[...]
    copies = [pltpu.make_async_copy(block, out_ref.at[i], sems.at[i]) for i in range(out_ref.shape[0])]
    for copy in copies:
        copy.start()
    for copy in copies:
        copy.wait()


def spread(weights):
    rows, size = weights[0].shape
    count = lax.axis_size("sp")
    blocks = pl.pallas_call(
        copies_kernel,
        out_shape=jax.ShapeDtypeStruct((count, rows, 3 * size), jnp.bfloat16),
        in_specs=[vmem()] * 3,
        out_specs=pl.BlockSpec(memory_space=pltpu.HBM),
        scratch_shapes=[pltpu.VMEM((rows, 3 * size), jnp.bfloat16), pltpu.SemaphoreType.DMA((count,))],
        compiler_params=pltpu.CompilerParams(vmem_limit_bytes=COPIES_VMEM),
        name="copies",
    )(*weights)
    return lax.all_to_all(blocks, "sp", 0, 0, tiled=True).reshape(-1, 3 * size)


def body(
    stream,
    gain_first,
    query_first,
    key_first,
    value_first,
    offset_first,
    gain_second,
    query_second,
    key_second,
    value_second,
    offset_second,
):
    tokens, _ = stream.shape
    first_set = spread((query_first, key_first, value_first))
    gains = jnp.pad(jnp.stack([gain_first, gain_second]), ((0, 6), (0, 0)))
    sent = (jnp.concatenate([stream, gains]).astype(jnp.float32) * SCALE_FIRST).astype(jnp.float16)
    held = lax.all_gather(sent, "tp", axis=0, tiled=False)
    gains = held[:, tokens:].astype(jnp.bfloat16)
    held = held.astype(jnp.bfloat16)
    middle, second_set = layer(
        stream,
        held,
        0,
        SCALE_FIRST,
        gains,
        first_set,
        offset_first,
        (query_second, key_second, value_second),
    )
    sent = (middle.astype(jnp.float32) * SCALE_SECOND).astype(jnp.float16)
    again = lax.all_gather(sent, "tp", axis=0, tiled=False).astype(jnp.bfloat16)
    return layer(middle, again, 1, SCALE_SECOND, gains, second_set, offset_second)[0]


def solution(mesh):
    placed = (
        P("sp", "tp"),
        P("tp"),
        P("sp", "tp"),
        P("sp", "tp"),
        P("sp", "tp"),
        P("tp", None, None),
        P("tp"),
        P("sp", "tp"),
        P("sp", "tp"),
        P("sp", "tp"),
        P("tp", None, None),
    )
    return jax.shard_map(body, mesh=mesh, in_specs=placed, out_specs=P("sp", "tp"), check_vma=False)
```

time: 204 us -> 205 us (level)
  local copies, waits for them, and re-layouts: 14.5 us -> 2.75 us
  Pallas kernels: 16.4 us -> 26.1 us
  waiting for transfers between devices: 41 us -> 48.2 us
  blocking collectives: 93 us -> 89.5 us
  other arithmetic: 8.91 us -> 5.6 us
    pallas_call x6, Pallas kernels: 15.9 us -> 25.6 us  [the longest x2 17.4 us: project(): pl.pallas_call(functools.partial(project_kernel, gain_row, scale), out_sh...]
    unnamed x40 -> x24, local copies, waits for them, and re-layouts: 10.4 us -> 2.75 us
    ppermute x4, waiting for transfers between devices: 41 us -> 48.2 us  [the longest x2 42.8 us: layer(): a_in = lax.ppermute(a_own, ('sp', 'tp'), halo_pairs(True))]
    broadcast_in_dim x2 -> x0, local copies, waits for them, and re-layouts: 4.09 us -> none  [replicated(): return jnp.broadcast_to(block[None], (lax.axis_size('sp'), *block.shape))]
    all_gather x1, blocking collectives: 49.2 us -> 46.6 us  [body(): held = lax.all_gather(sent, 'tp', axis=0, tiled=False)]
  transfers between devices with their start and end apart: 6 -> 6, of which waited for: 3 -> 3; matrix products, arithmetic and copies ran while one was open for 0% -> 3% of each run, Pallas kernels for 3% -> 1%
where the time goes in v5:
time: 205 us; the launch traced here: 202 us
  blocking collectives  89.5 us (44%)
  waiting for transfers between devices  48.2 us (24%)
  starting transfers between devices  29.5 us (14%)
  Pallas kernels  26.1 us (13%)
  other arithmetic  5.6 us (3%)
  local copies, waits for them, and re-layouts  2.75 us (1%)
    all_gather x1, blocking collectives, body(): held = lax.all_gather(sent, 'tp', axis=0, tiled=False)  46.6 us
    all_gather x1, blocking collectives, body(): again = lax.all_gather(sent, 'tp', axis=0, tiled=False).astype(jnp.bfloat16)  42.9 us
    ppermute x2, waiting for transfers between devices, layer(): a_in = lax.ppermute(a_own, ('sp', 'tp'), halo_pairs(True))  42.8 us
    all_to_all x2, starting transfers between devices, spread(): return lax.all_to_all(blocks, 'sp', 0, 0, tiled=True).reshape(-1, 3 * size)  17.8 us
    pallas_call x2, Pallas kernels, project(): pl.pallas_call(functools.partial(project_kernel, gain_row, scale), out_sh...  17.4 us
    ppermute x2, starting transfers between devices, layer(): a_in = lax.ppermute(a_own, ('sp', 'tp'), halo_pairs(True))  6.85 us
    pallas_call x2, Pallas kernels, spread(): pl.pallas_call(copies_kernel, out_shape=jax.ShapeDtypeStruct((count, rows...  5.72 us
    ppermute x2, waiting for transfers between devices, layer(): b_in = lax.ppermute(b_own, ('sp', 'tp'), halo_pairs(False))  5.41 us
  transfers between devices with their start and end apart: 6, of which 3 were waited for; matrix products, arithmetic and copies ran while one was open for 3% of the time, Pallas kernels for 1%

profile of v5, /device:TPU:6, one launch (start us, length us, event | category | flops | bytes accessed | tf_op | source)
XLA Modules:
  0.0 201.9 jit_solution(10816926683239361165)
XLA Ops:
  0.0 0.0 copy-start.10
  0.0 0.0 copy-start.9
  0.0 0.0 copy-start
  0.0 2.9 %copies.2 = bf16[16,256,384]{2,1,0:T(8,128)(2,1)} custom-call(bf16[256,128]{1,0:T(8,128)(2,1)} %first_ref.1, bf16[256,128]{1,0:T(8,128)(2,1)} %second_ref.1, bf16[256,128]{1,0:T(8,128)(2,1)} %third_ref.1), custom_call_target="tpu_custom_call" | custom-call | tf_op jit(solution)/shard_map/copies/pallas_call | solution.py:212
  2.9 10.1 %all-to-all-start = ((bf16[16,256,384]{2,1,0:T(8,128)(2,1)}), bf16[16,256,384]{2,1,0:T(8,128)(2,1)}, u32[]{:S(2)}, u32[]{:S(2)}) async-start(bf16[16,256,384]{2,1,0:T(8,128)(2,1)} %copies.2), calls=%async_computation | async-start | bytes 6291456 | tf_op jit(solution)/shard_map/all_to_all | solution.py:221
  13.0 0.0 copy-done.10
  13.0 0.0 copy-done.9
  13.0 0.0 copy-done
  13.1 46.6 %all-gather.3 = f16[32,520,128]{2,1,0:T(8,128)(2,1)S(1)} all-gather(f16[1,520,128]{2,1,0:T(8,128)(2,1)S(1)} %multiply_convert_fusion), channel_id=1, replica_groups=mesh['sp'=16,'tp'=32] {'tp'}, dimensions={0}, use_global_device_ids=true | all-gather | bytes 4392960 | tf_op jit(solution)/shard_map/all_gather | solution.py:241
  59.6 2.7 %convert_element_type.39.x_hbm = bf16[32,520,128]{2,1,0:T(8,128)(2,1)} convert(f16[32,520,128]{2,1,0:T(8,128)(2,1)S(1)} %all-gather.3) | non-fusion elementwise | flops 2129920 | bytes 8519680 | tf_op jit(solution)/shard_map/convert_element_type | solution.py:243
  62.3 0.6 slice_convert_fusion.gain_ref
  63.0 0.0 all-to-all-done
  63.0 8.7 %project.2 = (bf16[512,128]{1,0:T(8,128)(2,1)}, bf16[2,256,128]{2,1,0:T(8,128)(2,1)}, bf16[2,256,128]{2,1,0:T(8,128)(2,1)}) custom-call(bf16[32,520,128]{2,1,0:T(8,128)(2,1)} %convert_element_type.39.x_hbm, bf16[32,8,128]{2,1,0:T(8,128)(2,1)} %slice_convert_fusion.gain_ref, bf16[4096,384]{1,0:T(8,128)(2,1)} %bitcast.4.w_ref), custom_call_target="tpu_custom_call" | custom-call | flops 1610612736 | bytes 8388608 | tf_op jit(solution)/shard_map/project/pallas_call | solution.py:89
  71.7 0.0 copy-start.2
  71.7 0.0 copy-start.3
  71.7 0.0 copy-start.7
  71.7 2.9 %copies.3 = bf16[16,256,384]{2,1,0:T(8,128)(2,1)} custom-call(bf16[256,128]{1,0:T(8,128)(2,1)} %first_ref.2, bf16[256,128]{1,0:T(8,128)(2,1)} %second_ref.2, bf16[256,128]{1,0:T(8,128)(2,1)} %third_ref.2), custom_call_target="tpu_custom_call" | custom-call | tf_op jit(solution)/shard_map/copies/pallas_call | solution.py:212
  74.6 0.0 copy-start.1
  74.6 7.7 %all-to-all-start.1 = ((bf16[16,256,384]{2,1,0:T(8,128)(2,1)}), bf16[16,256,384]{2,1,0:T(8,128)(2,1)}, u32[]{:S(2)}, u32[]{:S(2)}) async-start(bf16[16,256,384]{2,1,0:T(8,128)(2,1)} %copies.3), calls=%async_computation.1 | async-start | bytes 6291456 | tf_op jit(solution)/shard_map/all_to_all | solution.py:221
  82.3 0.0 copy-done.2
  82.3 3.4 %collective-permute-start = (bf16[2,256,128]{2,1,0:T(8,128)(2,1)S(1)}, bf16[2,256,128]{2,1,0:T(8,128)(2,1)S(1)}, u32[]{:S(2)}, u32[]{:S(2)}) collective-permute-start(bf16[2,256,128]{2,1,0:T(8,128)(2,1)S(1)} %copy-done.2), channel_id=1, source_target_pairs={{0,32},{2,34},{4,36},{6,38},{8,40},{10,42},{12,44},{14,46},{16,48}... | collective-permute-start | bytes 393224 | tf_op jit(solution)/shard_map/ppermute | solution.py:188
  85.7 0.0 copy-done.3
  85.7 2.5 %collective-permute-start.1 = (bf16[2,256,128]{2,1,0:T(8,128)(2,1)S(1)}, bf16[2,256,128]{2,1,0:T(8,128)(2,1)S(1)}, u32[]{:S(2)}, u32[]{:S(2)}) collective-permute-start(bf16[2,256,128]{2,1,0:T(8,128)(2,1)S(1)} %copy-done.3), channel_id=1, source_target_pairs={{1,33},{3,35},{5,37},{7,39},{9,41},{11,43},{13,45},{15,47},{17,49}... | collective-permute-start | bytes 393224 | tf_op jit(solution)/shard_map/ppermute | solution.py:189
  88.2 0.0 copy-done.7
  88.2 0.3 bias.2.bias_ref
  88.5 41.7 %collective-permute-done.a_in = bf16[2,256,128]{2,1,0:T(8,128)(2,1)S(1)} collective-permute-done((bf16[2,256,128]{2,1,0:T(8,128)(2,1)S(1)}, bf16[2,256,128]{2,1,0:T(8,128)(2,1)S(1)}, u32[]{:S(2)}, u32[]{:S(2)}) %collective-permute-start) | collective-permute-done | bytes 131104 | tf_op jit(solution)/shard_map/ppermute | solution.py:188
  130.2 0.0 collective-permute-done.1.b_in
  130.2 0.0 copy-done.1
  130.2 0.9 attend.2.x_ref
  131.1 42.9 %all-gather.4 = f16[16384,128]{1,0:T(8,128)(2,1)S(1)} all-gather(f16[512,128]{1,0:T(8,128)(2,1)S(1)} %multiply_convert_fusion.1), channel_id=2, replica_groups=mesh['sp'=16,'tp'=32] {'tp'}, dimensions={0}, use_global_device_ids=true | all-gather | bytes 4325376 | tf_op jit(solution)/shard_map/all_gather | solution.py:255
  174.0 2.2 %convert_element_type.44 = bf16[16384,128]{1,0:T(8,128)(2,1)} convert(f16[16384,128]{1,0:T(8,128)(2,1)S(1)} %all-gather.4) | non-fusion elementwise | flops 2097152 | bytes 8388608 | tf_op jit(solution)/shard_map/convert_element_type | solution.py:255
  176.2 0.0 copy-start.8
  176.2 0.0 all-to-all-done.1
  176.2 8.7 %project.3 = (bf16[512,128]{1,0:T(8,128)(2,1)}, bf16[2,256,128]{2,1,0:T(8,128)(2,1)}, bf16[2,256,128]{2,1,0:T(8,128)(2,1)}) custom-call(bf16[32,512,128]{2,1,0:T(8,128)(2,1)} %bitcast.9, bf16[32,8,128]{2,1,0:T(8,128)(2,1)} %slice_convert_fusion.gain_ref, bf16[4096,384]{1,0:T(8,128)(2,1)} %bitcast.6.w_ref), custom_call_target="tpu_custom_call" | custom-call | flops 1610612736 | bytes 8388608 | tf_op jit(solution)/shard_map/project/pallas_call | solution.py:89
  184.9 3.5 %collective-permute-start.2 = (bf16[2,256,128]{2,1,0:T(8,128)(2,1)}, bf16[2,256,128]{2,1,0:T(8,128)(2,1)S(1)}, u32[]{:S(2)}, u32[]{:S(2)}) collective-permute-start(bf16[2,256,128]{2,1,0:T(8,128)(2,1)} %get-tuple-element.23.a_own), channel_id=1, source_target_pairs={{0,32},{2,34},{4,36},{6,38},{8,40},{10,42},{12,44},{14,46},{16,48}... | collective-permute-start | bytes 393224 | tf_op jit(solution)/shard_map/ppermute | solution.py:188
  188.4 2.4 %collective-permute-start.3 = (bf16[2,256,128]{2,1,0:T(8,128)(2,1)}, bf16[2,256,128]{2,1,0:T(8,128)(2,1)S(1)}, u32[]{:S(2)}, u32[]{:S(2)}) collective-permute-start(bf16[2,256,128]{2,1,0:T(8,128)(2,1)} %get-tuple-element.24.b_own), channel_id=1, source_target_pairs={{1,33},{3,35},{5,37},{7,39},{9,41},{11,43},{13,45},{15,47},{17,49}... | collective-permute-start | bytes 393224 | tf_op jit(solution)/shard_map/ppermute | solution.py:189
  190.8 0.0 copy-done.8
  190.8 0.3 bias.3.bias_ref
  191.1 1.1 collective-permute-done.2.a_in
  192.2 5.4 %collective-permute-done.3.b_in = bf16[2,256,128]{2,1,0:T(8,128)(2,1)S(1)} collective-permute-done((bf16[2,256,128]{2,1,0:T(8,128)(2,1)}, bf16[2,256,128]{2,1,0:T(8,128)(2,1)S(1)}, u32[]{:S(2)}, u32[]{:S(2)}) %collective-permute-start.3) | collective-permute-done | bytes 131104 | tf_op jit(solution)/shard_map/ppermute | solution.py:189
  197.6 0.0 copy-start.4
  197.6 0.9 copy-done.4
  198.5 0.0 copy-start.5
  198.5 0.9 copy-done.5
  199.4 0.0 copy-start.6
  199.4 0.9 copy-done.6
  200.3 1.5 attend.3
  (5 shorter events, 0.1 us)
Async XLA Ops:
  0.0 13.0 %copy-start.10 = (bf16[128]{0:T(256)(128)(2,1)S(1)}, bf16[128]{0:T(256)(128)(2,1)}, u32[]{:S(2)}) copy-start(bf16[128]{0:T(256)(128)(2,1)} %param.12) | copy-start | bytes 772
  0.0 13.0 %copy-start.9 = (bf16[128]{0:T(256)(128)(2,1)S(1)}, bf16[128]{0:T(256)(128)(2,1)}, u32[]{:S(2)}) copy-start(bf16[128]{0:T(256)(128)(2,1)} %param.17) | copy-start | bytes 772
  0.0 13.0 %copy-start = (bf16[512,128]{1,0:T(8,128)(2,1)S(1)}, bf16[512,128]{1,0:T(8,128)(2,1)}, u32[]{:S(2)}) copy-start(bf16[512,128]{1,0:T(8,128)(2,1)} %x_ref.1) | copy-start | bytes 393220
  2.9 60.1 %all-to-all-start = ((bf16[16,256,384]{2,1,0:T(8,128)(2,1)}), bf16[16,256,384]{2,1,0:T(8,128)(2,1)}, u32[]{:S(2)}, u32[]{:S(2)}) async-start(bf16[16,256,384]{2,1,0:T(8,128)(2,1)} %copies.2), calls=%async_computation | async-start | bytes 6291456 | tf_op jit(solution)/shard_map/all_to_all | solution.py:221
  71.7 10.6 %copy-start.2 = (bf16[2,256,128]{2,1,0:T(8,128)(2,1)S(1)}, bf16[2,256,128]{2,1,0:T(8,128)(2,1)}, u32[]{:S(2)}) copy-start(bf16[2,256,128]{2,1,0:T(8,128)(2,1)} %get-tuple-element.17.a_own) | copy-start | bytes 393220
  71.7 14.0 %copy-start.3 = (bf16[2,256,128]{2,1,0:T(8,128)(2,1)S(1)}, bf16[2,256,128]{2,1,0:T(8,128)(2,1)}, u32[]{:S(2)}) copy-start(bf16[2,256,128]{2,1,0:T(8,128)(2,1)} %get-tuple-element.18.b_own) | copy-start | bytes 393220
  71.7 16.5 %copy-start.7 = (f32[1,15,31]{2,0,1:T(1,128)S(1)}, f32[1,15,31]{2,0,1:T(1,128)}, u32[]{:S(2)}) copy-start(f32[1,15,31]{2,0,1:T(1,128)} %param.16) | copy-start | bytes 5584
  74.6 55.6 %copy-start.1 = (bf16[512,128]{1,0:T(8,128)(2,1)S(1)}, bf16[512,128]{1,0:T(8,128)(2,1)}, u32[]{:S(2)}) copy-start(bf16[512,128]{1,0:T(8,128)(2,1)} %get-tuple-element.16.q_ref) | copy-start | bytes 393220
  74.6 101.6 %all-to-all-start.1 = ((bf16[16,256,384]{2,1,0:T(8,128)(2,1)}), bf16[16,256,384]{2,1,0:T(8,128)(2,1)}, u32[]{:S(2)}, u32[]{:S(2)}) async-start(bf16[16,256,384]{2,1,0:T(8,128)(2,1)} %copies.3), calls=%async_computation.1 | async-start | bytes 6291456 | tf_op jit(solution)/shard_map/all_to_all | solution.py:221
  82.3 47.8 %collective-permute-start = (bf16[2,256,128]{2,1,0:T(8,128)(2,1)S(1)}, bf16[2,256,128]{2,1,0:T(8,128)(2,1)S(1)}, u32[]{:S(2)}, u32[]{:S(2)}) collective-permute-start(bf16[2,256,128]{2,1,0:T(8,128)(2,1)S(1)} %copy-done.2), channel_id=1, source_target_pairs={{0,32},{2,34},{4,36},{6,38},{8,40},{10,42},{12,44},{14,46},{16,48}... | collective-permute-start | bytes 393224 | tf_op jit(solution)/shard_map/ppermute | solution.py:188
  85.7 44.5 %collective-permute-start.1 = (bf16[2,256,128]{2,1,0:T(8,128)(2,1)S(1)}, bf16[2,256,128]{2,1,0:T(8,128)(2,1)S(1)}, u32[]{:S(2)}, u32[]{:S(2)}) collective-permute-start(bf16[2,256,128]{2,1,0:T(8,128)(2,1)S(1)} %copy-done.3), channel_id=1, source_target_pairs={{1,33},{3,35},{5,37},{7,39},{9,41},{11,43},{13,45},{15,47},{17,49}... | collective-permute-start | bytes 393224 | tf_op jit(solution)/shard_map/ppermute | solution.py:189
  176.2 14.6 %copy-start.8 = (f32[1,15,31]{2,0,1:T(1,128)S(1)}, f32[1,15,31]{2,0,1:T(1,128)}, u32[]{:S(2)}) copy-start(f32[1,15,31]{2,0,1:T(1,128)} %param.21) | copy-start | bytes 5584
  184.9 7.3 %collective-permute-start.2 = (bf16[2,256,128]{2,1,0:T(8,128)(2,1)}, bf16[2,256,128]{2,1,0:T(8,128)(2,1)S(1)}, u32[]{:S(2)}, u32[]{:S(2)}) collective-permute-start(bf16[2,256,128]{2,1,0:T(8,128)(2,1)} %get-tuple-element.23.a_own), channel_id=1, source_target_pairs={{0,32},{2,34},{4,36},{6,38},{8,40},{10,42},{12,44},{14,46},{16,48}... | collective-permute-start | bytes 393224 | tf_op jit(solution)/shard_map/ppermute | solution.py:188
  188.4 9.2 %collective-permute-start.3 = (bf16[2,256,128]{2,1,0:T(8,128)(2,1)}, bf16[2,256,128]{2,1,0:T(8,128)(2,1)S(1)}, u32[]{:S(2)}, u32[]{:S(2)}) collective-permute-start(bf16[2,256,128]{2,1,0:T(8,128)(2,1)} %get-tuple-element.24.b_own), channel_id=1, source_target_pairs={{1,33},{3,35},{5,37},{7,39},{9,41},{11,43},{13,45},{15,47},{17,49}... | collective-permute-start | bytes 393224 | tf_op jit(solution)/shard_map/ppermute | solution.py:189
  197.6 0.9 copy-start.4
  198.5 0.9 copy-start.5
  199.4 0.9 copy-start.6

commit v6 on v5

--- a/solution.py
+++ b/solution.py
@@ -15,9 +15,9 @@
 WINDOW_ROWS = 8
 HALO = 4
 MASKED = -1e30
-PROJECT_VMEM = 63_000_000
+PROJECT_VMEM = 24 << 20
 ATTEND_VMEM = 12 << 20
-COPIES_VMEM = 66_000_000
+COPIES_VMEM = (66_000_000, 2 << 20)
 
 
 def vmem():
@@ -53,25 +53,19 @@
     return lax.rem(lax.axis_index("tp"), 2)
 
 
-def project_kernel(gain_row, scale, x_hbm, gain_ref, w_ref, q_ref, a_ref, b_ref, x_ref, normed, sems):
-    blocks, tokens, size = x_ref.shape
+def project_kernel(gain_row, scale, x_ref, gain_ref, w_ref, q_ref, a_ref, b_ref, normed):
+    blocks, _, size = x_ref.shape
+    tokens = q_ref.shape[0]
     half = tokens // 2
     core = core_of_chip()
-    copies = [
-        pltpu.make_async_copy(x_hbm.at[f, pl.ds(0, tokens)], x_ref.at[f], sems.at[f])
-        for f in range(blocks)
-    ]
-    for copy in copies:
-        copy.start()
     total = jnp.zeros((tokens, size), jnp.float32)
     for f in range(blocks):
-        copies[f].wait()
-        part = x_ref[f].astype(jnp.float32)
+        part = x_ref[f, :tokens, :].astype(jnp.float32)
         total = total + part * part
     mean = jnp.sum(total, axis=1, keepdims=True) * (1.0 / (blocks * size * scale * scale))
     rate = lax.rsqrt(mean + EPSILON) * (1.0 / scale)
     for f in range(blocks):
-        part = x_ref[f].astype(jnp.float32)
+        part = x_ref[f, :tokens, :].astype(jnp.float32)
         gain = gain_ref[f, gain_row : gain_row + 1, :].astype(jnp.float32) * (1.0 / SCALE_FIRST)
         normed[:, f * size : (f + 1) * size] = (part * rate * gain).astype(jnp.bfloat16)
     for out_ref, number in ((a_ref, 1 - core), (b_ref, core)):
@@ -89,13 +83,9 @@
     return pl.pallas_call(
         functools.partial(project_kernel, gain_row, scale),
         out_shape=(jax.ShapeDtypeStruct((tokens, size), jnp.bfloat16), kv, kv),
-        in_specs=[pl.BlockSpec(memory_space=pltpu.HBM), vmem(), vmem()],
+        in_specs=[vmem()] * 3,
         out_specs=(vmem(),) * 3,
-        scratch_shapes=[
-            pltpu.VMEM((blocks, tokens, size), jnp.bfloat16),
-            pltpu.VMEM((tokens, blocks * size), jnp.bfloat16),
-            pltpu.SemaphoreType.DMA((blocks,)),
-        ],
+        scratch_shapes=[pltpu.VMEM((tokens, blocks * size), jnp.bfloat16)],
         cost_estimate=pl.CostEstimate(
             flops=2 * tokens * blocks * size * 3 * size, bytes_accessed=8 << 20, transcendentals=0
         ),
@@ -188,7 +178,7 @@
     a_in = lax.ppermute(a_own, ("sp", "tp"), halo_pairs(True))
     b_in = lax.ppermute(b_own, ("sp", "tp"), halo_pairs(False))
     if following is not None:
-        query, *following = lax.optimization_barrier((query, *following))
+        query, following = lax.optimization_barrier((query, following))
         following = spread(following)
     bias = bias_of(table)
     out = attend(last, query, a_in, a_own, b_own, b_in, bias, x)
@@ -206,19 +196,22 @@
         copy.wait()
 
 
-def spread(weights):
+def replicated(weights, grant):
     rows, size = weights[0].shape
     count = lax.axis_size("sp")
-    blocks = pl.pallas_call(
+    return pl.pallas_call(
         copies_kernel,
         out_shape=jax.ShapeDtypeStruct((count, rows, 3 * size), jnp.bfloat16),
         in_specs=[vmem()] * 3,
         out_specs=pl.BlockSpec(memory_space=pltpu.HBM),
         scratch_shapes=[pltpu.VMEM((rows, 3 * size), jnp.bfloat16), pltpu.SemaphoreType.DMA((count,))],
-        compiler_params=pltpu.CompilerParams(vmem_limit_bytes=COPIES_VMEM),
+        compiler_params=pltpu.CompilerParams(vmem_limit_bytes=grant),
         name="copies",
     )(*weights)
-    return lax.all_to_all(blocks, "sp", 0, 0, tiled=True).reshape(-1, 3 * size)
+
+
+def spread(blocks):
+    return lax.all_to_all(blocks, "sp", 0, 0, tiled=True).reshape(-1, blocks.shape[2])
 
 
 def body(
@@ -235,9 +228,15 @@
     offset_second,
 ):
     tokens, _ = stream.shape
-    first_set = spread((query_first, key_first, value_first))
+    first_blocks = replicated((query_first, key_first, value_first), COPIES_VMEM[0])
+    first_blocks, *second = lax.optimization_barrier(
+        (first_blocks, query_second, key_second, value_second)
+    )
+    second_blocks = replicated(second, COPIES_VMEM[1])
+    first_set = spread(first_blocks)
     gains = jnp.pad(jnp.stack([gain_first, gain_second]), ((0, 6), (0, 0)))
     sent = (jnp.concatenate([stream, gains]).astype(jnp.float32) * SCALE_FIRST).astype(jnp.float16)
+    sent, second_blocks = lax.optimization_barrier((sent, second_blocks))
     held = lax.all_gather(sent, "tp", axis=0, tiled=False)
     gains = held[:, tokens:].astype(jnp.bfloat16)
     held = held.astype(jnp.bfloat16)
@@ -249,7 +248,7 @@
         gains,
         first_set,
         offset_first,
-        (query_second, key_second, value_second),
+        second_blocks,
     )
     sent = (middle.astype(jnp.float32) * SCALE_SECOND).astype(jnp.float16)
     again = lax.all_gather(sent, "tp", axis=0, tiled=False).astype(jnp.bfloat16)

time: 205 us -> 203 us (level)
  Pallas kernels: 26.1 us -> 18.7 us
  local copies, waits for them, and re-layouts: 2.75 us -> 10.1 us
    pallas_call x2, Pallas kernels: 17.4 us -> 8.67 us  [project(): pl.pallas_call(functools.partial(project_kernel, gain_row, scale), out_sh...]
    unnamed x24 -> x36, local copies, waits for them, and re-layouts: 2.75 us -> 10.1 us
  transfers between devices with their start and end apart: 6 -> 6, of which waited for: 3 -> 3; matrix products, arithmetic and copies ran while one was open for 3% -> 2% of each run, Pallas kernels for 1% -> 3%
where the time goes in v6:
time: 203 us; the launch traced here: 200 us
  blocking collectives  89.5 us (44%)
  waiting for transfers between devices  48 us (24%)
  starting transfers between devices  28.5 us (14%)
  Pallas kernels  18.7 us (9%)
  local copies, waits for them, and re-layouts  10.1 us (5%)
  other arithmetic  4.97 us (2%)
    all_gather x1, blocking collectives, body(): held = lax.all_gather(sent, 'tp', axis=0, tiled=False)  47.7 us
    ppermute x2, waiting for transfers between devices, layer(): a_in = lax.ppermute(a_own, ('sp', 'tp'), halo_pairs(True))  42.6 us
    all_gather x1, blocking collectives, body(): again = lax.all_gather(sent, 'tp', axis=0, tiled=False).astype(jnp.bfloat16)  41.8 us
    all_to_all x2, starting transfers between devices, spread(): lax.all_to_all(blocks, 'sp', 0, 0, tiled=True).reshape(-1, blocks.shape[2])  16.9 us
    unnamed x36, local copies, waits for them, and re-layouts  10.1 us
    pallas_call x2, Pallas kernels, project(): pl.pallas_call(functools.partial(project_kernel, gain_row, scale), out_sh...  8.67 us
    pallas_call x2, Pallas kernels, replicated(): pl.pallas_call(copies_kernel, out_shape=jax.ShapeDtypeStruct((count, rows...  7.12 us
    ppermute x2, starting transfers between devices, layer(): a_in = lax.ppermute(a_own, ('sp', 'tp'), halo_pairs(True))  6.85 us
  transfers between devices with their start and end apart: 6, of which 3 were waited for; matrix products, arithmetic and copies ran while one was open for 2% of the time, Pallas kernels for 3%

profile of v6, /device:TPU:6, one launch (start us, length us, event | category | flops | bytes accessed | tf_op | source)
XLA Modules:
  0.0 200.1 jit_solution(824225177951786758)
XLA Ops:
  0.0 0.0 copy-start.10
  0.0 2.9 %copies.2 = bf16[16,256,384]{2,1,0:T(8,128)(2,1)} custom-call(bf16[256,128]{1,0:T(8,128)(2,1)} %first_ref.1, bf16[256,128]{1,0:T(8,128)(2,1)} %second_ref.1, bf16[256,128]{1,0:T(8,128)(2,1)} %third_ref.1), custom_call_target="tpu_custom_call" | custom-call | tf_op jit(solution)/shard_map/copies/pallas_call | solution.py:202
  2.9 0.0 copy-start.15
  2.9 0.0 copy-start.16
  2.9 0.0 copy-start.3
  2.9 9.5 %all-to-all-start = ((bf16[16,256,384]{2,1,0:T(8,128)(2,1)}), bf16[16,256,384]{2,1,0:T(8,128)(2,1)S(1)}, u32[]{:S(2)}, u32[]{:S(2)}) async-start(bf16[16,256,384]{2,1,0:T(8,128)(2,1)} %copies.2), calls=%async_computation | async-start | bytes 6291456 | tf_op jit(solution)/shard_map/all_to_all | solution.py:214
  12.4 0.0 copy-done.10
  12.4 0.0 copy-done.11
  12.4 0.0 copy-done.12
  12.5 4.3 %copies.3 = bf16[16,256,384]{2,1,0:T(8,128)(2,1)S(1)} custom-call(bf16[256,128]{1,0:T(8,128)(2,1)S(1)} %copy-done.10, bf16[256,128]{1,0:T(8,128)(2,1)S(1)} %copy-done.11, bf16[256,128]{1,0:T(8,128)(2,1)S(1)} %copy-done.12), custom_call_target="tpu_custom_call" | custom-call | tf_op jit(solution)/shard_map/copies/pallas_call | solution.py:202
  16.7 0.0 copy-start.2
  16.7 1.7 copy-done.2
  18.4 0.0 copy-done.15
  18.4 0.0 copy-done.16
  18.4 0.0 copy-done.3
  18.5 47.7 %all-gather.4 = f16[16640,128]{1,0:T(8,128)(2,1)S(1)} all-gather(f16[520,128]{1,0:T(8,128)(2,1)S(1)} %multiply_convert_fusion), channel_id=2, replica_groups=mesh['sp'=16,'tp'=32] {'tp'}, dimensions={0}, use_global_device_ids=true | all-gather | bytes 4392960 | tf_op jit(solution)/shard_map/all_gather | solution.py:240
  66.2 2.7 %convert_element_type.25.x_ref = bf16[32,520,128]{2,1,0:T(8,128)(2,1)} convert(f16[32,520,128]{2,1,0:T(8,128)(2,1)S(1)} %bitcast.9) | non-fusion elementwise | flops 2129920 | bytes 8519680 | tf_op jit(solution)/shard_map/convert_element_type | solution.py:242
  68.9 0.0 all-to-all-done
  68.9 0.0 copy-start
  68.9 2.2 %copy-done = bf16[32,520,128]{2,1,0:T(8,128)(2,1)S(1)} copy-done((bf16[32,520,128]{2,1,0:T(8,128)(2,1)S(1)}, bf16[32,520,128]{2,1,0:T(8,128)(2,1)}, u32[]{:S(2)}) %copy-start) | copy-done | bytes 4259864
  71.1 4.3 %project.2 = (bf16[512,128]{1,0:T(8,128)(2,1)S(1)}, bf16[2,256,128]{2,1,0:T(8,128)(2,1)S(1)}, bf16[2,256,128]{2,1,0:T(8,128)(2,1)S(1)}) custom-call(bf16[32,520,128]{2,1,0:T(8,128)(2,1)S(1)} %copy-done, bf16[32,8,128]{2,1,0:T(8,128)(2,1)S(1)} %slice_convert_fusion.gain_ref, bf16[4096,384]{1,0:T(8,128)(2,1)S(1)} %bitcast.8), custom_call_target="tpu_custom_call" | custom-call | flops 1610612736 | bytes 8388608 | tf_op jit(solution)/shard_map/project/pallas_call | solution.py:83
  75.4 0.0 copy-start.4
  75.5 0.6 copy-done.4
  76.1 0.7 copy-done.8
  76.8 7.4 %all-to-all-start.1 = ((bf16[16,256,384]{2,1,0:T(8,128)(2,1)}), bf16[16,256,384]{2,1,0:T(8,128)(2,1)S(1)}, u32[]{:S(2)}, u32[]{:S(2)}) async-start(bf16[16,256,384]{2,1,0:T(8,128)(2,1)} %copy-done.2), calls=%async_computation.1 | async-start | bytes 6291456 | tf_op jit(solution)/shard_map/all_to_all | solution.py:214
  84.1 3.4 %collective-permute-start = (bf16[2,256,128]{2,1,0:T(8,128)(2,1)S(1)}, bf16[2,256,128]{2,1,0:T(8,128)(2,1)S(1)}, u32[]{:S(2)}, u32[]{:S(2)}) collective-permute-start(bf16[2,256,128]{2,1,0:T(8,128)(2,1)S(1)} %get-tuple-element.27.a_own), channel_id=1, source_target_pairs={{0,32},{2,34},{4,36},{6,38},{8,40},{10,42},{12,44},{14,46},{16,48}... | collective-permute-start | bytes 393224 | tf_op jit(solution)/shard_map/ppermute | solution.py:178
  87.5 2.5 %collective-permute-start.1 = (bf16[2,256,128]{2,1,0:T(8,128)(2,1)}, bf16[2,256,128]{2,1,0:T(8,128)(2,1)S(1)}, u32[]{:S(2)}, u32[]{:S(2)}) collective-permute-start(bf16[2,256,128]{2,1,0:T(8,128)(2,1)} %copy-done.8), channel_id=1, source_target_pairs={{1,33},{3,35},{5,37},{7,39},{9,41},{11,43},{13,45},{15,47},{17,49}... | collective-permute-start | bytes 393224 | tf_op jit(solution)/shard_map/ppermute | solution.py:179
  90.0 0.0 copy-done.13
  90.0 0.3 bias.2.bias_ref
  90.2 41.7 %collective-permute-done.a_in = bf16[2,256,128]{2,1,0:T(8,128)(2,1)S(1)} collective-permute-done((bf16[2,256,128]{2,1,0:T(8,128)(2,1)S(1)}, bf16[2,256,128]{2,1,0:T(8,128)(2,1)S(1)}, u32[]{:S(2)}, u32[]{:S(2)}) %collective-permute-start) | collective-permute-done | bytes 131104 | tf_op jit(solution)/shard_map/ppermute | solution.py:178
  131.9 0.0 copy-done.6
  131.9 0.0 collective-permute-done.1.b_in
  132.0 0.9 copy-done.5
  132.9 0.9 copy-done.7
  133.8 0.9 copy-done.9
  134.7 0.9 attend.2.x_ref
  135.6 41.8 %all-gather.5 = f16[16384,128]{1,0:T(8,128)(2,1)S(1)} all-gather(f16[512,128]{1,0:T(8,128)(2,1)S(1)} %multiply_convert_fusion.1), channel_id=3, replica_groups=mesh['sp'=16,'tp'=32] {'tp'}, dimensions={0}, use_global_device_ids=true | all-gather | bytes 4325376 | tf_op jit(solution)/shard_map/all_gather | solution.py:254
  177.4 2.2 %convert_element_type.30 = bf16[16384,128]{1,0:T(8,128)(2,1)} convert(f16[16384,128]{1,0:T(8,128)(2,1)S(1)} %all-gather.5) | non-fusion elementwise | flops 2097152 | bytes 8388608 | tf_op jit(solution)/shard_map/convert_element_type | solution.py:254
  179.6 0.0 all-to-all-done.1
  179.6 2.2 %copy-done.1 = bf16[16384,128]{1,0:T(8,128)(2,1)S(1)} copy-done((bf16[16384,128]{1,0:T(8,128)(2,1)S(1)}, bf16[16384,128]{1,0:T(8,128)(2,1)}, u32[]{:S(2)}) %copy-start.1) | copy-done | bytes 4194328
  181.8 4.3 %project.3 = (bf16[512,128]{1,0:T(8,128)(2,1)S(1)}, bf16[2,256,128]{2,1,0:T(8,128)(2,1)S(1)}, bf16[2,256,128]{2,1,0:T(8,128)(2,1)S(1)}) custom-call(bf16[32,512,128]{2,1,0:T(8,128)(2,1)S(1)} %bitcast.6, bf16[32,8,128]{2,1,0:T(8,128)(2,1)S(1)} %slice_convert_fusion.gain_ref, bf16[4096,384]{1,0:T(8,128)(2,1)S(1)} %bitcast.7), custom_call_target="tpu_custom_call" | custom-call | flops 1610612736 | bytes 8388608 | tf_op jit(solution)/shard_map/project/pallas_call | solution.py:83
  186.1 3.5 %collective-permute-start.2 = (bf16[2,256,128]{2,1,0:T(8,128)(2,1)S(1)}, bf16[2,256,128]{2,1,0:T(8,128)(2,1)S(1)}, u32[]{:S(2)}, u32[]{:S(2)}) collective-permute-start(bf16[2,256,128]{2,1,0:T(8,128)(2,1)S(1)} %get-tuple-element.31.a_own), channel_id=1, source_target_pairs={{0,32},{2,34},{4,36},{6,38},{8,40},{10,42},{12,44},{14,46},{16,48}... | collective-permute-start | bytes 393224 | tf_op jit(solution)/shard_map/ppermute | solution.py:178
  189.6 2.4 %collective-permute-start.3 = (bf16[2,256,128]{2,1,0:T(8,128)(2,1)S(1)}, bf16[2,256,128]{2,1,0:T(8,128)(2,1)S(1)}, u32[]{:S(2)}, u32[]{:S(2)}) collective-permute-start(bf16[2,256,128]{2,1,0:T(8,128)(2,1)S(1)} %get-tuple-element.32.b_own), channel_id=1, source_target_pairs={{1,33},{3,35},{5,37},{7,39},{9,41},{11,43},{13,45},{15,47},{17,49}... | collective-permute-start | bytes 393224 | tf_op jit(solution)/shard_map/ppermute | solution.py:179
  191.9 0.0 copy-done.14
  192.0 0.3 bias.3.bias_ref
  192.2 0.9 collective-permute-done.2.a_in
  193.1 5.4 %collective-permute-done.3.b_in = bf16[2,256,128]{2,1,0:T(8,128)(2,1)S(1)} collective-permute-done((bf16[2,256,128]{2,1,0:T(8,128)(2,1)S(1)}, bf16[2,256,128]{2,1,0:T(8,128)(2,1)S(1)}, u32[]{:S(2)}, u32[]{:S(2)}) %collective-permute-start.3) | collective-permute-done | bytes 131104 | tf_op jit(solution)/shard_map/ppermute | solution.py:179
  198.6 1.5 attend.3
  (16 shorter events, 0.1 us)
Async XLA Ops:
  0.0 12.4 %copy-start.10 = (bf16[256,128]{1,0:T(8,128)(2,1)S(1)}, bf16[256,128]{1,0:T(8,128)(2,1)}, u32[]{:S(2)}) copy-start(bf16[256,128]{1,0:T(8,128)(2,1)} %first_ref.2) | copy-start | bytes 196612
  0.0 12.4 %copy-start.11 = (bf16[256,128]{1,0:T(8,128)(2,1)S(1)}, bf16[256,128]{1,0:T(8,128)(2,1)}, u32[]{:S(2)}) copy-start(bf16[256,128]{1,0:T(8,128)(2,1)} %second_ref.2) | copy-start | bytes 196612
  0.0 12.4 %copy-start.12 = (bf16[256,128]{1,0:T(8,128)(2,1)S(1)}, bf16[256,128]{1,0:T(8,128)(2,1)}, u32[]{:S(2)}) copy-start(bf16[256,128]{1,0:T(8,128)(2,1)} %third_ref.2) | copy-start | bytes 196612
  2.9 15.5 %copy-start.15 = (bf16[128]{0:T(256)(128)(2,1)S(1)}, bf16[128]{0:T(256)(128)(2,1)}, u32[]{:S(2)}) copy-start(bf16[128]{0:T(256)(128)(2,1)} %param.17) | copy-start | bytes 772
  2.9 15.5 %copy-start.16 = (bf16[128]{0:T(256)(128)(2,1)S(1)}, bf16[128]{0:T(256)(128)(2,1)}, u32[]{:S(2)}) copy-start(bf16[128]{0:T(256)(128)(2,1)} %param.12) | copy-start | bytes 772
  2.9 15.5 %copy-start.3 = (bf16[512,128]{1,0:T(8,128)(2,1)S(1)}, bf16[512,128]{1,0:T(8,128)(2,1)}, u32[]{:S(2)}) copy-start(bf16[512,128]{1,0:T(8,128)(2,1)} %x_ref.1) | copy-start | bytes 393220
  2.9 66.0 %all-to-all-start = ((bf16[16,256,384]{2,1,0:T(8,128)(2,1)}), bf16[16,256,384]{2,1,0:T(8,128)(2,1)S(1)}, u32[]{:S(2)}, u32[]{:S(2)}) async-start(bf16[16,256,384]{2,1,0:T(8,128)(2,1)} %copies.2), calls=%async_computation | async-start | bytes 6291456 | tf_op jit(solution)/shard_map/all_to_all | solution.py:214
  16.7 1.7 copy-start.2
  68.9 2.2 %copy-start = (bf16[32,520,128]{2,1,0:T(8,128)(2,1)S(1)}, bf16[32,520,128]{2,1,0:T(8,128)(2,1)}, u32[]{:S(2)}) copy-start(bf16[32,520,128]{2,1,0:T(8,128)(2,1)} %convert_element_type.25.x_ref) | copy-start | bytes 12779524
  75.4 0.7 copy-start.4
  76.1 0.7 copy-start.8
  76.8 55.2 %copy-start.6 = (bf16[2,256,128]{2,1,0:T(8,128)(2,1)}, bf16[2,256,128]{2,1,0:T(8,128)(2,1)S(1)}, u32[]{:S(2)}) copy-start(bf16[2,256,128]{2,1,0:T(8,128)(2,1)S(1)} %get-tuple-element.27.a_own) | copy-start | bytes 393220
  76.8 13.2 %copy-start.13 = (f32[1,15,31]{2,0,1:T(1,128)S(1)}, f32[1,15,31]{2,0,1:T(1,128)}, u32[]{:S(2)}) copy-start(f32[1,15,31]{2,0,1:T(1,128)} %param.16) | copy-start | bytes 5584
  76.8 102.8 %all-to-all-start.1 = ((bf16[16,256,384]{2,1,0:T(8,128)(2,1)}), bf16[16,256,384]{2,1,0:T(8,128)(2,1)S(1)}, u32[]{:S(2)}, u32[]{:S(2)}) async-start(bf16[16,256,384]{2,1,0:T(8,128)(2,1)} %copy-done.2), calls=%async_computation.1 | async-start | bytes 6291456 | tf_op jit(solution)/shard_map/all_to_all | solution.py:214
  84.1 47.8 %collective-permute-start = (bf16[2,256,128]{2,1,0:T(8,128)(2,1)S(1)}, bf16[2,256,128]{2,1,0:T(8,128)(2,1)S(1)}, u32[]{:S(2)}, u32[]{:S(2)}) collective-permute-start(bf16[2,256,128]{2,1,0:T(8,128)(2,1)S(1)} %get-tuple-element.27.a_own), channel_id=1, source_target_pairs={{0,32},{2,34},{4,36},{6,38},{8,40},{10,42},{12,44},{14,46},{16,48}... | collective-permute-start | bytes 393224 | tf_op jit(solution)/shard_map/ppermute | solution.py:178
  87.5 44.5 %collective-permute-start.1 = (bf16[2,256,128]{2,1,0:T(8,128)(2,1)}, bf16[2,256,128]{2,1,0:T(8,128)(2,1)S(1)}, u32[]{:S(2)}, u32[]{:S(2)}) collective-permute-start(bf16[2,256,128]{2,1,0:T(8,128)(2,1)} %copy-done.8), channel_id=1, source_target_pairs={{1,33},{3,35},{5,37},{7,39},{9,41},{11,43},{13,45},{15,47},{17,49}... | collective-permute-start | bytes 393224 | tf_op jit(solution)/shard_map/ppermute | solution.py:179
  132.0 0.9 copy-start.5
  132.9 0.9 copy-start.7
  133.8 0.9 copy-start.9
  177.4 14.6 %copy-start.14 = (f32[1,15,31]{2,0,1:T(1,128)S(1)}, f32[1,15,31]{2,0,1:T(1,128)}, u32[]{:S(2)}) copy-start(f32[1,15,31]{2,0,1:T(1,128)} %param.21) | copy-start | bytes 5584
  179.6 2.2 %copy-start.1 = (bf16[16384,128]{1,0:T(8,128)(2,1)S(1)}, bf16[16384,128]{1,0:T(8,128)(2,1)}, u32[]{:S(2)}) copy-start(bf16[16384,128]{1,0:T(8,128)(2,1)} %convert_element_type.30) | copy-start | bytes 12582916
  186.1 7.0 %collective-permute-start.2 = (bf16[2,256,128]{2,1,0:T(8,128)(2,1)S(1)}, bf16[2,256,128]{2,1,0:T(8,128)(2,1)S(1)}, u32[]{:S(2)}, u32[]{:S(2)}) collective-permute-start(bf16[2,256,128]{2,1,0:T(8,128)(2,1)S(1)} %get-tuple-element.31.a_own), channel_id=1, source_target_pairs={{0,32},{2,34},{4,36},{6,38},{8,40},{10,42},{12,44},{14,46},{16,48}... | collective-permute-start | bytes 393224 | tf_op jit(solution)/shard_map/ppermute | solution.py:178
  189.6 9.0 %collective-permute-start.3 = (bf16[2,256,128]{2,1,0:T(8,128)(2,1)S(1)}, bf16[2,256,128]{2,1,0:T(8,128)(2,1)S(1)}, u32[]{:S(2)}, u32[]{:S(2)}) collective-permute-start(bf16[2,256,128]{2,1,0:T(8,128)(2,1)S(1)} %get-tuple-element.32.b_own), channel_id=1, source_target_pairs={{1,33},{3,35},{5,37},{7,39},{9,41},{11,43},{13,45},{15,47},{17,49}... | collective-permute-start | bytes 393224 | tf_op jit(solution)/shard_map/ppermute | solution.py:179

commit v7 on v6

--- a/solution.py
+++ b/solution.py
@@ -17,7 +17,8 @@
 MASKED = -1e30
 PROJECT_VMEM = 24 << 20
 ATTEND_VMEM = 12 << 20
-COPIES_VMEM = (66_000_000, 2 << 20)
+COPIES_VMEM = 66_000_000
+BIAS_VMEM = (64_000_000, 12 << 20)
 
 
 def vmem():
@@ -38,13 +39,13 @@
         out_ref[m] = jnp.where(inside, turned, MASKED)
 
 
-def bias_of(table):
+def bias_of(table, grant):
     return pl.pallas_call(
         bias_kernel,
         out_shape=jax.ShapeDtypeStruct((14, GRID_W, 2 * GRID_W), jnp.float32),
         in_specs=[vmem()],
         out_specs=vmem(),
-        compiler_params=pltpu.CompilerParams(vmem_limit_bytes=ATTEND_VMEM),
+        compiler_params=pltpu.CompilerParams(vmem_limit_bytes=grant),
         name="bias",
     )(table)
 
@@ -68,13 +69,17 @@
         part = x_ref[f, :tokens, :].astype(jnp.float32)
         gain = gain_ref[f, gain_row : gain_row + 1, :].astype(jnp.float32) * (1.0 / SCALE_FIRST)
         normed[:, f * size : (f + 1) * size] = (part * rate * gain).astype(jnp.bfloat16)
-    for out_ref, number in ((a_ref, 1 - core), (b_ref, core)):
-        rows = pl.ds(pl.multiple_of(number * half, half), half)
+    outs = []
+    for number in range(2):
+        rows = slice(number * half, (number + 1) * half)
         out = jnp.dot(normed[rows, :], w_ref[...], preferred_element_type=jnp.float32)
         out = out.astype(jnp.bfloat16)
         q_ref[rows, :] = out[:, :size]
-        out_ref[0] = out[:, size : 2 * size]
-        out_ref[1] = out[:, 2 * size :]
+        outs.append(out[:, size:])
+    for out_ref, turn in ((a_ref, core), (b_ref, 1 - core)):
+        out = jnp.where(turn == 0, outs[1], outs[0])
+        out_ref[0] = out[:, :size]
+        out_ref[1] = out[:, size:]
 
 
 def project(gain_row, scale, x, gain, weights, tokens):
@@ -180,7 +185,7 @@
     if following is not None:
         query, following = lax.optimization_barrier((query, following))
         following = spread(following)
-    bias = bias_of(table)
+    bias = bias_of(table, BIAS_VMEM[gain_row])
     out = attend(last, query, a_in, a_own, b_own, b_in, bias, x)
     return out, following
 
@@ -196,7 +201,7 @@
         copy.wait()
 
 
-def replicated(weights, grant):
+def replicated(weights):
     rows, size = weights[0].shape
     count = lax.axis_size("sp")
     return pl.pallas_call(
@@ -205,7 +210,7 @@
         in_specs=[vmem()] * 3,
         out_specs=pl.BlockSpec(memory_space=pltpu.HBM),
         scratch_shapes=[pltpu.VMEM((rows, 3 * size), jnp.bfloat16), pltpu.SemaphoreType.DMA((count,))],
-        compiler_params=pltpu.CompilerParams(vmem_limit_bytes=grant),
+        compiler_params=pltpu.CompilerParams(vmem_limit_bytes=COPIES_VMEM),
         name="copies",
     )(*weights)
 
@@ -228,11 +233,12 @@
     offset_second,
 ):
     tokens, _ = stream.shape
-    first_blocks = replicated((query_first, key_first, value_first), COPIES_VMEM[0])
+    first_blocks = replicated((query_first, key_first, value_first))
     first_blocks, *second = lax.optimization_barrier(
         (first_blocks, query_second, key_second, value_second)
     )
-    second_blocks = replicated(second, COPIES_VMEM[1])
+    second_blocks = jnp.concatenate(second, 1)
+    second_blocks = jnp.broadcast_to(second_blocks[None], first_blocks.shape)
     first_set = spread(first_blocks)
     gains = jnp.pad(jnp.stack([gain_first, gain_second]), ((0, 6), (0, 0)))
     sent = (jnp.concatenate([stream, gains]).astype(jnp.float32) * SCALE_FIRST).astype(jnp.float16)

time: 203 us -> 198 us (0.975)
  Pallas kernels: 18.7 us -> 15.9 us
    pallas_call x2 -> x1, Pallas kernels: 7.12 us -> 2.91 us  [replicated(): pl.pallas_call(copies_kernel, out_shape=jax.ShapeDtypeStruct((count, rows...]
    unnamed x36 -> x32, local copies, waits for them, and re-layouts: 10.1 us -> 7.34 us
    broadcast_in_dim x0 -> x1, local copies, waits for them, and re-layouts: none -> 2.09 us  [body(): second_blocks = jnp.broadcast_to(second_blocks[None], first_blocks.shape)]
  transfers between devices with their start and end apart: 6 -> 6, of which waited for: 3 -> 3; matrix products, arithmetic and copies ran while one was open for 2% -> 4% of each run, Pallas kernels for 3% -> 1%
where the time goes in v7:
time: 198 us; the launch traced here: 195 us
  blocking collectives  89.4 us (45%)
  waiting for transfers between devices  46.4 us (23%)
  starting transfers between devices  28.4 us (14%)
  Pallas kernels  15.9 us (8%)
  local copies, waits for them, and re-layouts  9.43 us (5%)
  other arithmetic  5 us (3%)
    all_gather x1, blocking collectives, body(): held = lax.all_gather(sent, 'tp', axis=0, tiled=False)  47.7 us
    all_gather x1, blocking collectives, body(): again = lax.all_gather(sent, 'tp', axis=0, tiled=False).astype(jnp.bfloat16)  41.7 us
    ppermute x2, waiting for transfers between devices, layer(): a_in = lax.ppermute(a_own, ('sp', 'tp'), halo_pairs(True))  40.7 us
    all_to_all x2, starting transfers between devices, spread(): lax.all_to_all(blocks, 'sp', 0, 0, tiled=True).reshape(-1, blocks.shape[2])  16.7 us
    pallas_call x2, Pallas kernels, project(): pl.pallas_call(functools.partial(project_kernel, gain_row, scale), out_sh...  8.6 us
    unnamed x32, local copies, waits for them, and re-layouts  7.34 us
    ppermute x2, starting transfers between devices, layer(): a_in = lax.ppermute(a_own, ('sp', 'tp'), halo_pairs(True))  7.03 us
    ppermute x2, waiting for transfers between devices, layer(): b_in = lax.ppermute(b_own, ('sp', 'tp'), halo_pairs(False))  5.71 us
  transfers between devices with their start and end apart: 6, of which 3 were waited for; matrix products, arithmetic and copies ran while one was open for 4% of the time, Pallas kernels for 1%

profile of v7, /device:TPU:6, one launch (start us, length us, event | category | flops | bytes accessed | tf_op | source)
XLA Modules:
  0.0 194.8 jit_solution(17384568167912977618)
XLA Ops:
  0.0 0.0 copy-start.10
  0.0 0.0 copy-start.9
  0.0 0.0 copy-start.8
  0.0 0.0 copy-start.14
  0.0 0.0 copy-start.13
  0.0 0.0 copy-start.3
  0.0 2.9 %copies.1 = bf16[16,256,384]{2,1,0:T(8,128)(2,1)} custom-call(bf16[256,128]{1,0:T(8,128)(2,1)} %first_ref.1, bf16[256,128]{1,0:T(8,128)(2,1)} %second_ref.1, bf16[256,128]{1,0:T(8,128)(2,1)} %third_ref.1), custom_call_target="tpu_custom_call" | custom-call | tf_op jit(solution)/shard_map/copies/pallas_call | solution.py:207
  3.0 9.3 %all-to-all-start = ((bf16[16,256,384]{2,1,0:T(8,128)(2,1)}), bf16[16,256,384]{2,1,0:T(8,128)(2,1)S(1)}, u32[]{:S(2)}, u32[]{:S(2)}) async-start(bf16[16,256,384]{2,1,0:T(8,128)(2,1)} %copies.1), calls=%async_computation | async-start | bytes 6291456 | tf_op jit(solution)/shard_map/all_to_all | solution.py:219
  12.3 0.0 copy-done.14
  12.3 0.0 copy-done.13
  12.3 0.0 copy-done.3
  12.4 0.0 copy-done.10
  12.4 0.0 copy-done.9
  12.4 0.0 copy-done.8
  12.5 2.1 %broadcast_in_dim.2 = bf16[16,256,384]{2,1,0:T(8,128)(2,1)} broadcast(bf16[256,384]{1,0:T(8,128)(2,1)S(1)} %pad_maximum_fusion), dimensions={1,2} | broadcast | bytes 3342336 | tf_op jit(solution)/shard_map/broadcast_in_dim | solution.py:241
  14.5 47.7 %all-gather.4 = f16[16640,128]{1,0:T(8,128)(2,1)S(1)} all-gather(f16[520,128]{1,0:T(8,128)(2,1)S(1)} %multiply_convert_fusion), channel_id=2, replica_groups=mesh['sp'=16,'tp'=32] {'tp'}, dimensions={0}, use_global_device_ids=true | all-gather | bytes 4392960 | tf_op jit(solution)/shard_map/all_gather | solution.py:246
  62.3 2.7 %convert_element_type.25.x_ref = bf16[32,520,128]{2,1,0:T(8,128)(2,1)} convert(f16[32,520,128]{2,1,0:T(8,128)(2,1)S(1)} %bitcast.8) | non-fusion elementwise | flops 2129920 | bytes 8519680 | tf_op jit(solution)/shard_map/convert_element_type | solution.py:248
  65.0 0.0 all-to-all-done
  65.0 0.0 copy-start
  65.0 2.2 %copy-done = bf16[32,520,128]{2,1,0:T(8,128)(2,1)S(1)} copy-done((bf16[32,520,128]{2,1,0:T(8,128)(2,1)S(1)}, bf16[32,520,128]{2,1,0:T(8,128)(2,1)}, u32[]{:S(2)}) %copy-start) | copy-done | bytes 4259864
  67.2 3.4 %project.2 = (bf16[512,128]{1,0:T(8,128)(2,1)S(1)}, bf16[2,256,128]{2,1,0:T(8,128)(2,1)S(1)}, bf16[2,256,128]{2,1,0:T(8,128)(2,1)S(1)}) custom-call(bf16[32,520,128]{2,1,0:T(8,128)(2,1)S(1)} %copy-done, bf16[32,8,128]{2,1,0:T(8,128)(2,1)S(1)} %slice_convert_fusion.gain_ref, bf16[4096,384]{1,0:T(8,128)(2,1)S(1)} %bitcast.7), custom_call_target="tpu_custom_call" | custom-call | flops 1610612736 | bytes 8388608 | tf_op jit(solution)/shard_map/project/pallas_call | solution.py:88
  70.6 0.0 copy-start.4
  70.6 0.6 copy-done.4
  71.2 0.6 copy-done.6
  71.9 7.4 %all-to-all-start.1 = ((bf16[16,256,384]{2,1,0:T(8,128)(2,1)}), bf16[16,256,384]{2,1,0:T(8,128)(2,1)}, u32[]{:S(2)}, u32[]{:S(2)}) async-start(bf16[16,256,384]{2,1,0:T(8,128)(2,1)} %broadcast_in_dim.2), calls=%async_computation.1 | async-start | bytes 6291456 | tf_op jit(solution)/shard_map/all_to_all | solution.py:219
  79.2 0.0 copy-done.5
  79.3 3.4 %collective-permute-start = (bf16[2,256,128]{2,1,0:T(8,128)(2,1)S(1)}, bf16[2,256,128]{2,1,0:T(8,128)(2,1)S(1)}, u32[]{:S(2)}, u32[]{:S(2)}) collective-permute-start(bf16[2,256,128]{2,1,0:T(8,128)(2,1)S(1)} %copy-done.5), channel_id=1, source_target_pairs={{0,32},{2,34},{4,36},{6,38},{8,40},{10,42},{12,44},{14,46},{16,48}... | collective-permute-start | bytes 393224 | tf_op jit(solution)/shard_map/ppermute | solution.py:183
  82.6 0.0 copy-done.7
  82.6 2.5 %collective-permute-start.1 = (bf16[2,256,128]{2,1,0:T(8,128)(2,1)S(1)}, bf16[2,256,128]{2,1,0:T(8,128)(2,1)S(1)}, u32[]{:S(2)}, u32[]{:S(2)}) collective-permute-start(bf16[2,256,128]{2,1,0:T(8,128)(2,1)S(1)} %copy-done.7), channel_id=1, source_target_pairs={{1,33},{3,35},{5,37},{7,39},{9,41},{11,43},{13,45},{15,47},{17,49}... | collective-permute-start | bytes 393224 | tf_op jit(solution)/shard_map/ppermute | solution.py:184
  85.1 0.0 copy-done.11
  85.1 0.6 copy.12.table_ref
  85.7 1.7 bias.2.bias_ref
  87.5 39.9 %collective-permute-done.a_in = bf16[2,256,128]{2,1,0:T(8,128)(2,1)S(1)} collective-permute-done((bf16[2,256,128]{2,1,0:T(8,128)(2,1)S(1)}, bf16[2,256,128]{2,1,0:T(8,128)(2,1)S(1)}, u32[]{:S(2)}, u32[]{:S(2)}) %collective-permute-start) | collective-permute-done | bytes 131104 | tf_op jit(solution)/shard_map/ppermute | solution.py:183
  127.3 0.0 collective-permute-done.1.b_in
  127.3 1.0 copy-done.2
  128.4 0.9 attend.2.x_ref
  129.3 41.7 %all-gather.5 = f16[16384,128]{1,0:T(8,128)(2,1)S(1)} all-gather(f16[512,128]{1,0:T(8,128)(2,1)S(1)} %multiply_convert_fusion.1), channel_id=3, replica_groups=mesh['sp'=16,'tp'=32] {'tp'}, dimensions={0}, use_global_device_ids=true | all-gather | bytes 4325376 | tf_op jit(solution)/shard_map/all_gather | solution.py:260
  171.0 2.2 %convert_element_type.30 = bf16[16384,128]{1,0:T(8,128)(2,1)} convert(f16[16384,128]{1,0:T(8,128)(2,1)S(1)} %all-gather.5) | non-fusion elementwise | flops 2097152 | bytes 8388608 | tf_op jit(solution)/shard_map/convert_element_type | solution.py:260
  173.2 0.0 all-to-all-done.1
  173.2 2.2 %copy-done.1 = bf16[16384,128]{1,0:T(8,128)(2,1)S(1)} copy-done((bf16[16384,128]{1,0:T(8,128)(2,1)S(1)}, bf16[16384,128]{1,0:T(8,128)(2,1)}, u32[]{:S(2)}) %copy-start.1) | copy-done | bytes 4194328
  175.3 5.2 %project.3 = (bf16[512,128]{1,0:T(8,128)(2,1)S(1)}, bf16[2,256,128]{2,1,0:T(8,128)(2,1)S(1)}, bf16[2,256,128]{2,1,0:T(8,128)(2,1)S(1)}) custom-call(bf16[32,512,128]{2,1,0:T(8,128)(2,1)S(1)} %bitcast.6, bf16[32,8,128]{2,1,0:T(8,128)(2,1)S(1)} %slice_convert_fusion.gain_ref, bf16[4096,384]{1,0:T(8,128)(2,1)} %bitcast.5.w_ref), custom_call_target="tpu_custom_call" | custom-call | flops 1610612736 | bytes 8388608 | tf_op jit(solution)/shard_map/project/pallas_call | solution.py:88
  180.6 3.7 %collective-permute-start.2 = (bf16[2,256,128]{2,1,0:T(8,128)(2,1)S(1)}, bf16[2,256,128]{2,1,0:T(8,128)(2,1)S(1)}, u32[]{:S(2)}, u32[]{:S(2)}) collective-permute-start(bf16[2,256,128]{2,1,0:T(8,128)(2,1)S(1)} %get-tuple-element.31.a_own), channel_id=1, source_target_pairs={{0,32},{2,34},{4,36},{6,38},{8,40},{10,42},{12,44},{14,46},{16,48}... | collective-permute-start | bytes 393224 | tf_op jit(solution)/shard_map/ppermute | solution.py:183
  184.2 2.2 %collective-permute-start.3 = (bf16[2,256,128]{2,1,0:T(8,128)(2,1)S(1)}, bf16[2,256,128]{2,1,0:T(8,128)(2,1)S(1)}, u32[]{:S(2)}, u32[]{:S(2)}) collective-permute-start(bf16[2,256,128]{2,1,0:T(8,128)(2,1)S(1)} %get-tuple-element.32.b_own), channel_id=1, source_target_pairs={{1,33},{3,35},{5,37},{7,39},{9,41},{11,43},{13,45},{15,47},{17,49}... | collective-permute-start | bytes 393224 | tf_op jit(solution)/shard_map/ppermute | solution.py:184
  186.4 0.0 copy-done.12
  186.4 0.3 bias.3.bias_ref
  186.7 0.8 collective-permute-done.2.a_in
  187.5 5.7 %collective-permute-done.3.b_in = bf16[2,256,128]{2,1,0:T(8,128)(2,1)S(1)} collective-permute-done((bf16[2,256,128]{2,1,0:T(8,128)(2,1)S(1)}, bf16[2,256,128]{2,1,0:T(8,128)(2,1)S(1)}, u32[]{:S(2)}, u32[]{:S(2)}) %collective-permute-start.3) | collective-permute-done | bytes 131104 | tf_op jit(solution)/shard_map/ppermute | solution.py:184
  193.2 1.6 attend.3
  (13 shorter events, 0.1 us)
Async XLA Ops:
  0.0 12.4 %copy-start.10 = (bf16[256,128]{1,0:T(8,128)(2,1)S(1)}, bf16[256,128]{1,0:T(8,128)(2,1)}, u32[]{:S(2)}) copy-start(bf16[256,128]{1,0:T(8,128)(2,1)} %param.18) | copy-start | bytes 196612
  0.0 12.4 %copy-start.9 = (bf16[256,128]{1,0:T(8,128)(2,1)S(1)}, bf16[256,128]{1,0:T(8,128)(2,1)}, u32[]{:S(2)}) copy-start(bf16[256,128]{1,0:T(8,128)(2,1)} %param.19) | copy-start | bytes 196612
  0.0 12.4 %copy-start.8 = (bf16[256,128]{1,0:T(8,128)(2,1)S(1)}, bf16[256,128]{1,0:T(8,128)(2,1)}, u32[]{:S(2)}) copy-start(bf16[256,128]{1,0:T(8,128)(2,1)} %param.20) | copy-start | bytes 196612
  0.0 12.3 %copy-start.14 = (bf16[128]{0:T(256)(128)(2,1)S(1)}, bf16[128]{0:T(256)(128)(2,1)}, u32[]{:S(2)}) copy-start(bf16[128]{0:T(256)(128)(2,1)} %param.12) | copy-start | bytes 772
  0.0 12.3 %copy-start.13 = (bf16[128]{0:T(256)(128)(2,1)S(1)}, bf16[128]{0:T(256)(128)(2,1)}, u32[]{:S(2)}) copy-start(bf16[128]{0:T(256)(128)(2,1)} %param.17) | copy-start | bytes 772
  0.0 12.3 %copy-start.3 = (bf16[512,128]{1,0:T(8,128)(2,1)S(1)}, bf16[512,128]{1,0:T(8,128)(2,1)}, u32[]{:S(2)}) copy-start(bf16[512,128]{1,0:T(8,128)(2,1)} %x_ref.1) | copy-start | bytes 393220
  3.0 62.0 %all-to-all-start = ((bf16[16,256,384]{2,1,0:T(8,128)(2,1)}), bf16[16,256,384]{2,1,0:T(8,128)(2,1)S(1)}, u32[]{:S(2)}, u32[]{:S(2)}) async-start(bf16[16,256,384]{2,1,0:T(8,128)(2,1)} %copies.1), calls=%async_computation | async-start | bytes 6291456 | tf_op jit(solution)/shard_map/all_to_all | solution.py:219
  65.0 2.2 %copy-start = (bf16[32,520,128]{2,1,0:T(8,128)(2,1)S(1)}, bf16[32,520,128]{2,1,0:T(8,128)(2,1)}, u32[]{:S(2)}) copy-start(bf16[32,520,128]{2,1,0:T(8,128)(2,1)} %convert_element_type.25.x_ref) | copy-start | bytes 12779524
  70.6 0.7 copy-start.4
  71.2 0.6 copy-start.6
  71.9 13.2 %copy-start.11 = (f32[1,15,31]{2,0,1:T(1,128)S(1)}, f32[1,15,31]{2,0,1:T(1,128)}, u32[]{:S(2)}) copy-start(f32[1,15,31]{2,0,1:T(1,128)} %param.16) | copy-start | bytes 5584
  71.9 7.4 %copy-start.5 = (bf16[2,256,128]{2,1,0:T(8,128)(2,1)S(1)}, bf16[2,256,128]{2,1,0:T(8,128)(2,1)}, u32[]{:S(2)}) copy-start(bf16[2,256,128]{2,1,0:T(8,128)(2,1)} %copy-done.4) | copy-start | bytes 393220
  71.9 10.7 %copy-start.7 = (bf16[2,256,128]{2,1,0:T(8,128)(2,1)S(1)}, bf16[2,256,128]{2,1,0:T(8,128)(2,1)}, u32[]{:S(2)}) copy-start(bf16[2,256,128]{2,1,0:T(8,128)(2,1)} %copy-done.6) | copy-start | bytes 393220
  71.9 101.3 %all-to-all-start.1 = ((bf16[16,256,384]{2,1,0:T(8,128)(2,1)}), bf16[16,256,384]{2,1,0:T(8,128)(2,1)}, u32[]{:S(2)}, u32[]{:S(2)}) async-start(bf16[16,256,384]{2,1,0:T(8,128)(2,1)} %broadcast_in_dim.2), calls=%async_computation.1 | async-start | bytes 6291456 | tf_op jit(solution)/shard_map/all_to_all | solution.py:219
  79.3 48.1 %collective-permute-start = (bf16[2,256,128]{2,1,0:T(8,128)(2,1)S(1)}, bf16[2,256,128]{2,1,0:T(8,128)(2,1)S(1)}, u32[]{:S(2)}, u32[]{:S(2)}) collective-permute-start(bf16[2,256,128]{2,1,0:T(8,128)(2,1)S(1)} %copy-done.5), channel_id=1, source_target_pairs={{0,32},{2,34},{4,36},{6,38},{8,40},{10,42},{12,44},{14,46},{16,48}... | collective-permute-start | bytes 393224 | tf_op jit(solution)/shard_map/ppermute | solution.py:183
  82.6 44.7 %collective-permute-start.1 = (bf16[2,256,128]{2,1,0:T(8,128)(2,1)S(1)}, bf16[2,256,128]{2,1,0:T(8,128)(2,1)S(1)}, u32[]{:S(2)}, u32[]{:S(2)}) collective-permute-start(bf16[2,256,128]{2,1,0:T(8,128)(2,1)S(1)} %copy-done.7), channel_id=1, source_target_pairs={{1,33},{3,35},{5,37},{7,39},{9,41},{11,43},{13,45},{15,47},{17,49}... | collective-permute-start | bytes 393224 | tf_op jit(solution)/shard_map/ppermute | solution.py:184
  127.3 1.0 copy-start.2
  171.0 15.4 %copy-start.12 = (f32[1,15,31]{2,0,1:T(1,128)S(1)}, f32[1,15,31]{2,0,1:T(1,128)}, u32[]{:S(2)}) copy-start(f32[1,15,31]{2,0,1:T(1,128)} %param.21) | copy-start | bytes 5584
  173.2 2.2 %copy-start.1 = (bf16[16384,128]{1,0:T(8,128)(2,1)S(1)}, bf16[16384,128]{1,0:T(8,128)(2,1)}, u32[]{:S(2)}) copy-start(bf16[16384,128]{1,0:T(8,128)(2,1)} %convert_element_type.30) | copy-start | bytes 12582916
  180.6 6.9 %collective-permute-start.2 = (bf16[2,256,128]{2,1,0:T(8,128)(2,1)S(1)}, bf16[2,256,128]{2,1,0:T(8,128)(2,1)S(1)}, u32[]{:S(2)}, u32[]{:S(2)}) collective-permute-start(bf16[2,256,128]{2,1,0:T(8,128)(2,1)S(1)} %get-tuple-element.31.a_own), channel_id=1, source_target_pairs={{0,32},{2,34},{4,36},{6,38},{8,40},{10,42},{12,44},{14,46},{16,48}... | collective-permute-start | bytes 393224 | tf_op jit(solution)/shard_map/ppermute | solution.py:183
  184.2 9.0 %collective-permute-start.3 = (bf16[2,256,128]{2,1,0:T(8,128)(2,1)S(1)}, bf16[2,256,128]{2,1,0:T(8,128)(2,1)S(1)}, u32[]{:S(2)}, u32[]{:S(2)}) collective-permute-start(bf16[2,256,128]{2,1,0:T(8,128)(2,1)S(1)} %get-tuple-element.32.b_own), channel_id=1, source_target_pairs={{1,33},{3,35},{5,37},{7,39},{9,41},{11,43},{13,45},{15,47},{17,49}... | collective-permute-start | bytes 393224 | tf_op jit(solution)/shard_map/ppermute | solution.py:184

commit v8 on v7

--- a/solution.py
+++ b/solution.py
@@ -16,16 +16,15 @@
 HALO = 4
 MASKED = -1e30
 PROJECT_VMEM = 24 << 20
+COPIES_VMEM = 66_000_000
 ATTEND_VMEM = 12 << 20
-COPIES_VMEM = 66_000_000
-BIAS_VMEM = (64_000_000, 12 << 20)
 
 
 def vmem():
     return pl.BlockSpec(memory_space=pltpu.VMEM)
 
 
-def bias_kernel(table_ref, out_ref):
+def fill_bias(table_ref, bias_ref):
     width = GRID_W
     col = lax.broadcasted_iota(jnp.int32, (width, 2 * width), 0)
     key = lax.broadcasted_iota(jnp.int32, (width, 2 * width), 1) % width
@@ -36,37 +35,36 @@
     for m in range(14):
         row = jnp.broadcast_to(both[m : m + 1, :], (width, 2 * width))
         turned = pltpu.roll(row, 2 * width - 15, 1, stride=1, stride_axis=0)
-        out_ref[m] = jnp.where(inside, turned, MASKED)
-
-
-def bias_of(table, grant):
-    return pl.pallas_call(
-        bias_kernel,
-        out_shape=jax.ShapeDtypeStruct((14, GRID_W, 2 * GRID_W), jnp.float32),
-        in_specs=[vmem()],
-        out_specs=vmem(),
-        compiler_params=pltpu.CompilerParams(vmem_limit_bytes=grant),
-        name="bias",
-    )(table)
+        bias_ref[m] = jnp.where(inside, turned, MASKED)
 
 
 def core_of_chip():
     return lax.rem(lax.axis_index("tp"), 2)
 
 
-def project_kernel(gain_row, scale, x_ref, gain_ref, w_ref, q_ref, a_ref, b_ref, normed):
-    blocks, _, size = x_ref.shape
-    tokens = q_ref.shape[0]
+def project_kernel(gain_row, scale, x_hbm, gain_hbm, w_ref, q_ref, a_ref, b_ref, x_ref, gain_ref, normed, sems):
+    blocks, tokens, size = x_ref.shape
     half = tokens // 2
     core = core_of_chip()
+    copies = [
+        pltpu.make_async_copy(x_hbm.at[f, pl.ds(0, tokens)], x_ref.at[f], sems.at[f])
+        for f in range(blocks)
+    ]
+    rows = gain_hbm.shape[1] - tokens
+    gains = pltpu.make_async_copy(gain_hbm.at[:, pl.ds(tokens, rows)], gain_ref, sems.at[blocks])
+    for copy in copies:
+        copy.start()
+    gains.start()
     total = jnp.zeros((tokens, size), jnp.float32)
     for f in range(blocks):
-        part = x_ref[f, :tokens, :].astype(jnp.float32)
+        copies[f].wait()
+        part = x_ref[f].astype(jnp.float32)
         total = total + part * part
     mean = jnp.sum(total, axis=1, keepdims=True) * (1.0 / (blocks * size * scale * scale))
     rate = lax.rsqrt(mean + EPSILON) * (1.0 / scale)
+    gains.wait()
     for f in range(blocks):
-        part = x_ref[f, :tokens, :].astype(jnp.float32)
+        part = x_ref[f].astype(jnp.float32)
         gain = gain_ref[f, gain_row : gain_row + 1, :].astype(jnp.float32) * (1.0 / SCALE_FIRST)
         normed[:, f * size : (f + 1) * size] = (part * rate * gain).astype(jnp.bfloat16)
     outs = []
@@ -82,24 +80,31 @@
         out_ref[1] = out[:, size:]
 
 
-def project(gain_row, scale, x, gain, weights, tokens):
+def project(gain_row, scale, x, held, weights, tokens):
     blocks, _, size = x.shape
     kv = jax.ShapeDtypeStruct((2, tokens // 2, size), jnp.bfloat16)
+    hbm = pl.BlockSpec(memory_space=pltpu.HBM)
     return pl.pallas_call(
         functools.partial(project_kernel, gain_row, scale),
         out_shape=(jax.ShapeDtypeStruct((tokens, size), jnp.bfloat16), kv, kv),
-        in_specs=[vmem()] * 3,
+        in_specs=[hbm, hbm, vmem()],
         out_specs=(vmem(),) * 3,
-        scratch_shapes=[pltpu.VMEM((tokens, blocks * size), jnp.bfloat16)],
+        scratch_shapes=[
+            pltpu.VMEM((blocks, tokens, size), jnp.bfloat16),
+            pltpu.VMEM((blocks, held.shape[1] - tokens, size), jnp.bfloat16),
+            pltpu.VMEM((tokens, blocks * size), jnp.bfloat16),
+            pltpu.SemaphoreType.DMA((blocks + 1,)),
+        ],
         cost_estimate=pl.CostEstimate(
             flops=2 * tokens * blocks * size * 3 * size, bytes_accessed=8 << 20, transcendentals=0
         ),
         compiler_params=pltpu.CompilerParams(vmem_limit_bytes=PROJECT_VMEM),
         name="project",
-    )(x, gain, weights)
-
-
-def attend_kernel(last, q_ref, a_in, a_own, b_own, b_in, bias_ref, x_ref, out_ref, keys, values):
+    )(x, held, weights)
+
+
+def attend_kernel(last, q_ref, a_in, a_own, b_own, b_in, table_ref, x_ref, out_ref, keys, values, bias_ref):
+    fill_bias(table_ref, bias_ref)
     width = GRID_W
     tokens, size = q_ref.shape
     half = tokens // 2
@@ -149,20 +154,24 @@
         out_ref[here, :] = (x_ref[here, :].astype(jnp.float32) + attended).astype(jnp.bfloat16)
 
 
-def attend(last, query, a_in, a_own, b_own, b_in, bias, x):
+def attend(last, query, a_in, a_own, b_own, b_in, table, x):
     tokens, size = x.shape
     return pl.pallas_call(
         functools.partial(attend_kernel, last),
         out_shape=jax.ShapeDtypeStruct((tokens, size), jnp.bfloat16),
         in_specs=[vmem()] * 7,
         out_specs=vmem(),
-        scratch_shapes=[pltpu.VMEM((2 * tokens, size), jnp.bfloat16)] * 2,
+        scratch_shapes=[
+            pltpu.VMEM((2 * tokens, size), jnp.bfloat16),
+            pltpu.VMEM((2 * tokens, size), jnp.bfloat16),
+            pltpu.VMEM((14, GRID_W, 2 * GRID_W), jnp.float32),
+        ],
         cost_estimate=pl.CostEstimate(
             flops=4 * tokens * size * WINDOW_ROWS * GRID_W, bytes_accessed=2 << 20, transcendentals=tokens * 512
         ),
         compiler_params=pltpu.CompilerParams(vmem_limit_bytes=ATTEND_VMEM),
         name="attend",
-    )(query, a_in, a_own, b_own, b_in, bias, x)
+    )(query, a_in, a_own, b_own, b_in, table, x)
 
 
 def halo_pairs(first):
@@ -176,17 +185,16 @@
     return pairs
 
 
-def layer(x, gathered, gain_row, scale, gains, weights, table, following=None):
+def layer(x, gathered, gain_row, scale, held, weights, table, following=None):
     tokens = x.shape[0]
     last = lax.axis_size("sp") * tokens // GRID_W - WINDOW_ROWS
-    query, a_own, b_own = project(gain_row, scale, gathered, gains, weights, tokens)
+    query, a_own, b_own = project(gain_row, scale, gathered, held, weights, tokens)
     a_in = lax.ppermute(a_own, ("sp", "tp"), halo_pairs(True))
     b_in = lax.ppermute(b_own, ("sp", "tp"), halo_pairs(False))
     if following is not None:
         query, following = lax.optimization_barrier((query, following))
         following = spread(following)
-    bias = bias_of(table, BIAS_VMEM[gain_row])
-    out = attend(last, query, a_in, a_own, b_own, b_in, bias, x)
+    out = attend(last, query, a_in, a_own, b_own, b_in, table, x)
     return out, following
 
 
@@ -232,7 +240,6 @@
     value_second,
     offset_second,
 ):
-    tokens, _ = stream.shape
     first_blocks = replicated((query_first, key_first, value_first))
     first_blocks, *second = lax.optimization_barrier(
         (first_blocks, query_second, key_second, value_second)
@@ -243,22 +250,22 @@
     gains = jnp.pad(jnp.stack([gain_first, gain_second]), ((0, 6), (0, 0)))
     sent = (jnp.concatenate([stream, gains]).astype(jnp.float32) * SCALE_FIRST).astype(jnp.float16)
     sent, second_blocks = lax.optimization_barrier((sent, second_blocks))
-    held = lax.all_gather(sent, "tp", axis=0, tiled=False)
-    gains = held[:, tokens:].astype(jnp.bfloat16)
-    held = held.astype(jnp.bfloat16)
+    held = lax.all_gather(sent, "tp", axis=0, tiled=False).astype(jnp.bfloat16)
+    held = pltpu.with_memory_space_constraint(held, pltpu.HBM)
     middle, second_set = layer(
         stream,
         held,
         0,
         SCALE_FIRST,
-        gains,
+        held,
         first_set,
         offset_first,
         second_blocks,
     )
     sent = (middle.astype(jnp.float32) * SCALE_SECOND).astype(jnp.float16)
     again = lax.all_gather(sent, "tp", axis=0, tiled=False).astype(jnp.bfloat16)
-    return layer(middle, again, 1, SCALE_SECOND, gains, second_set, offset_second)[0]
+    again = pltpu.with_memory_space_constraint(again, pltpu.HBM)
+    return layer(middle, again, 1, SCALE_SECOND, held, second_set, offset_second)[0]
 
 
 def solution(mesh):

time: 198 us -> 195 us (0.985)
  local copies, waits for them, and re-layouts: 9.43 us -> 4.6 us
  waiting for transfers between devices: 46.4 us -> 49 us
    unnamed x32 -> x26, local copies, waits for them, and re-layouts: 7.34 us -> 2.5 us
    ppermute x2, waiting for transfers between devices: 40.7 us -> 43.3 us  [layer(): a_in = lax.ppermute(a_own, ('sp', 'tp'), halo_pairs(True))]
    pallas_call x2 -> x0, Pallas kernels: 1.98 us -> none  [bias_of(): pl.pallas_call(bias_kernel, out_shape=jax.ShapeDtypeStruct((14, GRID_W, 2...]
where the time goes in v8:
time: 195 us; the launch traced here: 192 us
  blocking collectives  89.5 us (46%)
  waiting for transfers between devices  49 us (25%)
  starting transfers between devices  28.4 us (15%)
  Pallas kernels  15.6 us (8%)
  other arithmetic  4.88 us (3%)
  local copies, waits for them, and re-layouts  4.6 us (2%)
    all_gather x1, blocking collectives, body(): held = lax.all_gather(sent, 'tp', axis=0, tiled=False).astype(jnp.bfloat16)  47.7 us
    ppermute x2, waiting for transfers between devices, layer(): a_in = lax.ppermute(a_own, ('sp', 'tp'), halo_pairs(True))  43.3 us
    all_gather x1, blocking collectives, body(): again = lax.all_gather(sent, 'tp', axis=0, tiled=False).astype(jnp.bfloat16)  41.8 us
    all_to_all x2, starting transfers between devices, spread(): lax.all_to_all(blocks, 'sp', 0, 0, tiled=True).reshape(-1, blocks.shape[2])  16.7 us
    pallas_call x2, Pallas kernels, project(): pl.pallas_call(functools.partial(project_kernel, gain_row, scale), out_sh...  10.1 us
    ppermute x2, starting transfers between devices, layer(): a_in = lax.ppermute(a_own, ('sp', 'tp'), halo_pairs(True))  6.98 us
    ppermute x2, waiting for transfers between devices, layer(): b_in = lax.ppermute(b_own, ('sp', 'tp'), halo_pairs(False))  5.66 us
    ppermute x2, starting transfers between devices, layer(): b_in = lax.ppermute(b_own, ('sp', 'tp'), halo_pairs(False))  4.69 us
  transfers between devices with their start and end apart: 6, of which 3 were waited for; matrix products, arithmetic and copies ran while one was open for 4% of the time, Pallas kernels for 1%

profile of v8, /device:TPU:6, one launch (start us, length us, event | category | flops | bytes accessed | tf_op | source)
XLA Modules:
  0.0 192.1 jit_solution(10072335389724135721)
XLA Ops:
  0.0 0.0 copy-start.7
  0.0 0.0 copy-start.6
  0.0 0.0 copy-start.5
  0.0 0.0 copy-start.11
  0.0 0.0 copy-start.10
  0.0 0.0 copy-start
  0.0 2.8 %copies.1 = bf16[16,256,384]{2,1,0:T(8,128)(2,1)} custom-call(bf16[256,128]{1,0:T(8,128)(2,1)} %first_ref.1, bf16[256,128]{1,0:T(8,128)(2,1)} %second_ref.1, bf16[256,128]{1,0:T(8,128)(2,1)} %third_ref.1), custom_call_target="tpu_custom_call" | custom-call | tf_op jit(solution)/shard_map/copies/pallas_call | solution.py:215
  2.9 9.3 %all-to-all-start = ((bf16[16,256,384]{2,1,0:T(8,128)(2,1)}), bf16[16,256,384]{2,1,0:T(8,128)(2,1)S(1)}, u32[]{:S(2)}, u32[]{:S(2)}) async-start(bf16[16,256,384]{2,1,0:T(8,128)(2,1)} %copies.1), calls=%async_computation | async-start | bytes 6291456 | tf_op jit(solution)/shard_map/all_to_all | solution.py:227
  12.2 0.0 copy-done.11
  12.2 0.0 copy-done.10
  12.3 0.0 copy-done
  12.3 0.0 copy-done.7
  12.3 0.0 copy-done.6
  12.3 0.0 copy-done.5
  12.4 2.1 %broadcast_in_dim.2 = bf16[16,256,384]{2,1,0:T(8,128)(2,1)} broadcast(bf16[256,384]{1,0:T(8,128)(2,1)S(1)} %pad_maximum_fusion), dimensions={1,2} | broadcast | bytes 3342336 | tf_op jit(solution)/shard_map/broadcast_in_dim | solution.py:248
  14.5 47.7 %all-gather.4 = f16[16640,128]{1,0:T(8,128)(2,1)S(1)} all-gather(f16[520,128]{1,0:T(8,128)(2,1)S(1)} %multiply_convert_fusion), channel_id=2, replica_groups=mesh['sp'=16,'tp'=32] {'tp'}, dimensions={0}, use_global_device_ids=true | all-gather | bytes 4392960 | tf_op jit(solution)/shard_map/all_gather | solution.py:253
  62.2 2.5 %convert_element_type.26 = bf16[16640,128]{1,0:T(8,128)(2,1)} convert(f16[16640,128]{1,0:T(8,128)(2,1)S(1)} %all-gather.4) | non-fusion elementwise | flops 2129920 | bytes 8519680 | tf_op jit(solution)/shard_map/convert_element_type | solution.py:253
  64.7 0.0 all-to-all-done
  64.7 5.1 %project.2 = (bf16[512,128]{1,0:T(8,128)(2,1)S(1)}, bf16[2,256,128]{2,1,0:T(8,128)(2,1)S(1)}, bf16[2,256,128]{2,1,0:T(8,128)(2,1)S(1)}) custom-call(bf16[32,520,128]{2,1,0:T(8,128)(2,1)} %bitcast.8, bf16[32,520,128]{2,1,0:T(8,128)(2,1)} %bitcast.9, bf16[4096,384]{1,0:T(8,128)(2,1)S(1)} %bitcast.7), custom_call_target="tpu_custom_call" | custom-call | flops 1610612736 | bytes 8388608 | tf_op jit(solution)/shard_map/project/pallas_call | solution.py:87
  69.8 0.0 copy-start.3
  69.8 0.6 copy-done.3
  70.5 0.0 copy-start.1
  70.5 0.0 copy-start.8
  70.5 7.4 %all-to-all-start.1 = ((bf16[16,256,384]{2,1,0:T(8,128)(2,1)}), bf16[16,256,384]{2,1,0:T(8,128)(2,1)S(1)}, u32[]{:S(2)}, u32[]{:S(2)}) async-start(bf16[16,256,384]{2,1,0:T(8,128)(2,1)} %broadcast_in_dim.2), calls=%async_computation.1 | async-start | bytes 6291456 | tf_op jit(solution)/shard_map/all_to_all | solution.py:227
  77.8 3.4 %collective-permute-start = (bf16[2,256,128]{2,1,0:T(8,128)(2,1)S(1)}, bf16[2,256,128]{2,1,0:T(8,128)(2,1)S(1)}, u32[]{:S(2)}, u32[]{:S(2)}) collective-permute-start(bf16[2,256,128]{2,1,0:T(8,128)(2,1)S(1)} %get-tuple-element.27.a_own), channel_id=1, source_target_pairs={{0,32},{2,34},{4,36},{6,38},{8,40},{10,42},{12,44},{14,46},{16,48}... | collective-permute-start | bytes 393224 | tf_op jit(solution)/shard_map/ppermute | solution.py:192
  81.2 2.5 %collective-permute-start.1 = (bf16[2,256,128]{2,1,0:T(8,128)(2,1)}, bf16[2,256,128]{2,1,0:T(8,128)(2,1)S(1)}, u32[]{:S(2)}, u32[]{:S(2)}) collective-permute-start(bf16[2,256,128]{2,1,0:T(8,128)(2,1)} %copy-done.3), channel_id=1, source_target_pairs={{1,33},{3,35},{5,37},{7,39},{9,41},{11,43},{13,45},{15,47},{17,49}... | collective-permute-start | bytes 393224 | tf_op jit(solution)/shard_map/ppermute | solution.py:193
  83.7 0.0 copy-done.8
  83.7 42.2 %collective-permute-done.a_in = bf16[2,256,128]{2,1,0:T(8,128)(2,1)S(1)} collective-permute-done((bf16[2,256,128]{2,1,0:T(8,128)(2,1)S(1)}, bf16[2,256,128]{2,1,0:T(8,128)(2,1)S(1)}, u32[]{:S(2)}, u32[]{:S(2)}) %collective-permute-start) | collective-permute-done | bytes 131104 | tf_op jit(solution)/shard_map/ppermute | solution.py:192
  125.9 0.0 copy-done.1
  125.9 0.0 collective-permute-done.1.b_in
  125.9 0.0 copy-start.2
  125.9 0.9 copy-done.2
  126.8 0.0 copy-start.4
  126.8 0.9 copy-done.4
  127.7 1.0 attend.2.x_ref
  128.7 41.8 %all-gather.5 = f16[16384,128]{1,0:T(8,128)(2,1)S(1)} all-gather(f16[512,128]{1,0:T(8,128)(2,1)S(1)} %multiply_convert_fusion.1), channel_id=3, replica_groups=mesh['sp'=16,'tp'=32] {'tp'}, dimensions={0}, use_global_device_ids=true | all-gather | bytes 4325376 | tf_op jit(solution)/shard_map/all_gather | solution.py:266
  170.5 2.2 %convert_element_type.27 = bf16[16384,128]{1,0:T(8,128)(2,1)} convert(f16[16384,128]{1,0:T(8,128)(2,1)S(1)} %all-gather.5) | non-fusion elementwise | flops 2097152 | bytes 8388608 | tf_op jit(solution)/shard_map/convert_element_type | solution.py:266
  172.7 0.0 all-to-all-done.1
  172.7 0.0 copy-start.9
  172.7 5.1 %project.3 = (bf16[512,128]{1,0:T(8,128)(2,1)S(1)}, bf16[2,256,128]{2,1,0:T(8,128)(2,1)S(1)}, bf16[2,256,128]{2,1,0:T(8,128)(2,1)S(1)}) custom-call(bf16[32,512,128]{2,1,0:T(8,128)(2,1)} %bitcast.11, bf16[32,520,128]{2,1,0:T(8,128)(2,1)} %bitcast.10, bf16[4096,384]{1,0:T(8,128)(2,1)S(1)} %bitcast.6), custom_call_target="tpu_custom_call" | custom-call | flops 1610612736 | bytes 8388608 | tf_op jit(solution)/shard_map/project/pallas_call | solution.py:87
  177.8 3.6 %collective-permute-start.2 = (bf16[2,256,128]{2,1,0:T(8,128)(2,1)S(1)}, bf16[2,256,128]{2,1,0:T(8,128)(2,1)S(1)}, u32[]{:S(2)}, u32[]{:S(2)}) collective-permute-start(bf16[2,256,128]{2,1,0:T(8,128)(2,1)S(1)} %get-tuple-element.31.a_own), channel_id=1, source_target_pairs={{0,32},{2,34},{4,36},{6,38},{8,40},{10,42},{12,44},{14,46},{16,48}... | collective-permute-start | bytes 393224 | tf_op jit(solution)/shard_map/ppermute | solution.py:192
  181.5 2.2 %collective-permute-start.3 = (bf16[2,256,128]{2,1,0:T(8,128)(2,1)S(1)}, bf16[2,256,128]{2,1,0:T(8,128)(2,1)S(1)}, u32[]{:S(2)}, u32[]{:S(2)}) collective-permute-start(bf16[2,256,128]{2,1,0:T(8,128)(2,1)S(1)} %get-tuple-element.32.b_own), channel_id=1, source_target_pairs={{1,33},{3,35},{5,37},{7,39},{9,41},{11,43},{13,45},{15,47},{17,49}... | collective-permute-start | bytes 393224 | tf_op jit(solution)/shard_map/ppermute | solution.py:193
  183.7 0.0 copy-done.9
  183.7 1.1 collective-permute-done.2.a_in
  184.8 5.7 %collective-permute-done.3.b_in = bf16[2,256,128]{2,1,0:T(8,128)(2,1)S(1)} collective-permute-done((bf16[2,256,128]{2,1,0:T(8,128)(2,1)S(1)}, bf16[2,256,128]{2,1,0:T(8,128)(2,1)S(1)}, u32[]{:S(2)}, u32[]{:S(2)}) %collective-permute-start.3) | collective-permute-done | bytes 131104 | tf_op jit(solution)/shard_map/ppermute | solution.py:193
  190.4 1.6 attend.3
  (6 shorter events, 0.1 us)
Async XLA Ops:
  0.0 12.3 %copy-start.7 = (bf16[256,128]{1,0:T(8,128)(2,1)S(1)}, bf16[256,128]{1,0:T(8,128)(2,1)}, u32[]{:S(2)}) copy-start(bf16[256,128]{1,0:T(8,128)(2,1)} %param.18) | copy-start | bytes 196612
  0.0 12.3 %copy-start.6 = (bf16[256,128]{1,0:T(8,128)(2,1)S(1)}, bf16[256,128]{1,0:T(8,128)(2,1)}, u32[]{:S(2)}) copy-start(bf16[256,128]{1,0:T(8,128)(2,1)} %param.19) | copy-start | bytes 196612
  0.0 12.3 %copy-start.5 = (bf16[256,128]{1,0:T(8,128)(2,1)S(1)}, bf16[256,128]{1,0:T(8,128)(2,1)}, u32[]{:S(2)}) copy-start(bf16[256,128]{1,0:T(8,128)(2,1)} %param.20) | copy-start | bytes 196612
  0.0 12.2 %copy-start.11 = (bf16[128]{0:T(256)(128)(2,1)S(1)}, bf16[128]{0:T(256)(128)(2,1)}, u32[]{:S(2)}) copy-start(bf16[128]{0:T(256)(128)(2,1)} %param.12) | copy-start | bytes 772
  0.0 12.2 %copy-start.10 = (bf16[128]{0:T(256)(128)(2,1)S(1)}, bf16[128]{0:T(256)(128)(2,1)}, u32[]{:S(2)}) copy-start(bf16[128]{0:T(256)(128)(2,1)} %param.17) | copy-start | bytes 772
  0.0 12.2 %copy-start = (bf16[512,128]{1,0:T(8,128)(2,1)S(1)}, bf16[512,128]{1,0:T(8,128)(2,1)}, u32[]{:S(2)}) copy-start(bf16[512,128]{1,0:T(8,128)(2,1)} %x_ref.1) | copy-start | bytes 393220
  2.9 61.8 %all-to-all-start = ((bf16[16,256,384]{2,1,0:T(8,128)(2,1)}), bf16[16,256,384]{2,1,0:T(8,128)(2,1)S(1)}, u32[]{:S(2)}, u32[]{:S(2)}) async-start(bf16[16,256,384]{2,1,0:T(8,128)(2,1)} %copies.1), calls=%async_computation | async-start | bytes 6291456 | tf_op jit(solution)/shard_map/all_to_all | solution.py:227
  69.8 0.7 copy-start.3
  70.5 55.5 %copy-start.1 = (bf16[2,256,128]{2,1,0:T(8,128)(2,1)}, bf16[2,256,128]{2,1,0:T(8,128)(2,1)S(1)}, u32[]{:S(2)}) copy-start(bf16[2,256,128]{2,1,0:T(8,128)(2,1)S(1)} %get-tuple-element.27.a_own) | copy-start | bytes 393220
  70.5 13.2 %copy-start.8 = (f32[1,15,31]{2,0,1:T(1,128)S(1)}, f32[1,15,31]{2,0,1:T(1,128)}, u32[]{:S(2)}) copy-start(f32[1,15,31]{2,0,1:T(1,128)} %param.16) | copy-start | bytes 5584
  70.5 102.3 %all-to-all-start.1 = ((bf16[16,256,384]{2,1,0:T(8,128)(2,1)}), bf16[16,256,384]{2,1,0:T(8,128)(2,1)S(1)}, u32[]{:S(2)}, u32[]{:S(2)}) async-start(bf16[16,256,384]{2,1,0:T(8,128)(2,1)} %broadcast_in_dim.2), calls=%async_computation.1 | async-start | bytes 6291456 | tf_op jit(solution)/shard_map/all_to_all | solution.py:227
  77.8 48.1 %collective-permute-start = (bf16[2,256,128]{2,1,0:T(8,128)(2,1)S(1)}, bf16[2,256,128]{2,1,0:T(8,128)(2,1)S(1)}, u32[]{:S(2)}, u32[]{:S(2)}) collective-permute-start(bf16[2,256,128]{2,1,0:T(8,128)(2,1)S(1)} %get-tuple-element.27.a_own), channel_id=1, source_target_pairs={{0,32},{2,34},{4,36},{6,38},{8,40},{10,42},{12,44},{14,46},{16,48}... | collective-permute-start | bytes 393224 | tf_op jit(solution)/shard_map/ppermute | solution.py:192
  81.2 44.7 %collective-permute-start.1 = (bf16[2,256,128]{2,1,0:T(8,128)(2,1)}, bf16[2,256,128]{2,1,0:T(8,128)(2,1)S(1)}, u32[]{:S(2)}, u32[]{:S(2)}) collective-permute-start(bf16[2,256,128]{2,1,0:T(8,128)(2,1)} %copy-done.3), channel_id=1, source_target_pairs={{1,33},{3,35},{5,37},{7,39},{9,41},{11,43},{13,45},{15,47},{17,49}... | collective-permute-start | bytes 393224 | tf_op jit(solution)/shard_map/ppermute | solution.py:193
  125.9 0.9 copy-start.2
  126.8 0.9 copy-start.4
  172.7 10.9 %copy-start.9 = (f32[1,15,31]{2,0,1:T(1,128)S(1)}, f32[1,15,31]{2,0,1:T(1,128)}, u32[]{:S(2)}) copy-start(f32[1,15,31]{2,0,1:T(1,128)} %param.21) | copy-start | bytes 5584
  177.8 6.9 %collective-permute-start.2 = (bf16[2,256,128]{2,1,0:T(8,128)(2,1)S(1)}, bf16[2,256,128]{2,1,0:T(8,128)(2,1)S(1)}, u32[]{:S(2)}, u32[]{:S(2)}) collective-permute-start(bf16[2,256,128]{2,1,0:T(8,128)(2,1)S(1)} %get-tuple-element.31.a_own), channel_id=1, source_target_pairs={{0,32},{2,34},{4,36},{6,38},{8,40},{10,42},{12,44},{14,46},{16,48}... | collective-permute-start | bytes 393224 | tf_op jit(solution)/shard_map/ppermute | solution.py:192
  181.5 9.0 %collective-permute-start.3 = (bf16[2,256,128]{2,1,0:T(8,128)(2,1)S(1)}, bf16[2,256,128]{2,1,0:T(8,128)(2,1)S(1)}, u32[]{:S(2)}, u32[]{:S(2)}) collective-permute-start(bf16[2,256,128]{2,1,0:T(8,128)(2,1)S(1)} %get-tuple-element.32.b_own), channel_id=1, source_target_pairs={{1,33},{3,35},{5,37},{7,39},{9,41},{11,43},{13,45},{15,47},{17,49}... | collective-permute-start | bytes 393224 | tf_op jit(solution)/shard_map/ppermute | solution.py:193

commit v9 on v8

--- a/solution.py
+++ b/solution.py
@@ -17,6 +17,7 @@
 MASKED = -1e30
 PROJECT_VMEM = 24 << 20
 COPIES_VMEM = 66_000_000
+NEAR_BLOCKS = 22
 ATTEND_VMEM = 12 << 20
 
 
@@ -42,31 +43,46 @@
     return lax.rem(lax.axis_index("tp"), 2)
 
 
-def project_kernel(gain_row, scale, x_hbm, gain_hbm, w_ref, q_ref, a_ref, b_ref, x_ref, gain_ref, normed, sems):
-    blocks, tokens, size = x_ref.shape
+def project_kernel(gain_row, scale, near, *refs):
+    near_ref, refs = (refs[0], refs[1:]) if near else (None, refs)
+    x_hbm, gain_hbm, w_in, q_ref, a_ref, b_ref, x_ref, gain_ref, normed, sems, *rest = refs
+    far, tokens, size = x_ref.shape
+    blocks = near + far
     half = tokens // 2
     core = core_of_chip()
     copies = [
         pltpu.make_async_copy(x_hbm.at[f, pl.ds(0, tokens)], x_ref.at[f], sems.at[f])
-        for f in range(blocks)
+        for f in range(far)
     ]
+
+    def block_of(f):
+        return near_ref[f] if f < near else x_ref[f - near]
+
     rows = gain_hbm.shape[1] - tokens
     gains = pltpu.make_async_copy(gain_hbm.at[:, pl.ds(tokens, rows)], gain_ref, sems.at[blocks])
     for copy in copies:
         copy.start()
     gains.start()
+    w_ref = w_in
+    if rest:
+        (w_ref,) = rest
+        weights = pltpu.make_async_copy(w_in, w_ref, sems.at[blocks + 1])
+        weights.start()
     total = jnp.zeros((tokens, size), jnp.float32)
     for f in range(blocks):
-        copies[f].wait()
-        part = x_ref[f].astype(jnp.float32)
+        if f >= near:
+            copies[f - near].wait()
+        part = block_of(f).astype(jnp.float32)
         total = total + part * part
     mean = jnp.sum(total, axis=1, keepdims=True) * (1.0 / (blocks * size * scale * scale))
     rate = lax.rsqrt(mean + EPSILON) * (1.0 / scale)
     gains.wait()
     for f in range(blocks):
-        part = x_ref[f].astype(jnp.float32)
+        part = block_of(f).astype(jnp.float32)
         gain = gain_ref[f, gain_row : gain_row + 1, :].astype(jnp.float32) * (1.0 / SCALE_FIRST)
         normed[:, f * size : (f + 1) * size] = (part * rate * gain).astype(jnp.bfloat16)
+    if rest:
+        weights.wait()
     outs = []
     for number in range(2):
         rows = slice(number * half, (number + 1) * half)
@@ -81,26 +97,31 @@
 
 
 def project(gain_row, scale, x, held, weights, tokens):
-    blocks, _, size = x.shape
+    *nearer, x = x
+    near = nearer[0].shape[0] if nearer else 0
+    far, _, size = x.shape
+    blocks = near + far
     kv = jax.ShapeDtypeStruct((2, tokens // 2, size), jnp.bfloat16)
     hbm = pl.BlockSpec(memory_space=pltpu.HBM)
+    streamed = gain_row == 1
     return pl.pallas_call(
-        functools.partial(project_kernel, gain_row, scale),
+        functools.partial(project_kernel, gain_row, scale, near),
         out_shape=(jax.ShapeDtypeStruct((tokens, size), jnp.bfloat16), kv, kv),
-        in_specs=[hbm, hbm, vmem()],
+        in_specs=[vmem()] * len(nearer) + [hbm, hbm, hbm if streamed else vmem()],
         out_specs=(vmem(),) * 3,
         scratch_shapes=[
-            pltpu.VMEM((blocks, tokens, size), jnp.bfloat16),
+            pltpu.VMEM((far, tokens, size), jnp.bfloat16),
             pltpu.VMEM((blocks, held.shape[1] - tokens, size), jnp.bfloat16),
             pltpu.VMEM((tokens, blocks * size), jnp.bfloat16),
-            pltpu.SemaphoreType.DMA((blocks + 1,)),
-        ],
+            pltpu.SemaphoreType.DMA((blocks + 2,)),
+        ]
+        + [pltpu.VMEM(weights.shape, jnp.bfloat16)] * streamed,
         cost_estimate=pl.CostEstimate(
             flops=2 * tokens * blocks * size * 3 * size, bytes_accessed=8 << 20, transcendentals=0
         ),
         compiler_params=pltpu.CompilerParams(vmem_limit_bytes=PROJECT_VMEM),
         name="project",
-    )(x, held, weights)
+    )(*nearer, x, held, weights)
 
 
 def attend_kernel(last, q_ref, a_in, a_own, b_own, b_in, table_ref, x_ref, out_ref, keys, values, bias_ref):
@@ -193,7 +214,7 @@
     b_in = lax.ppermute(b_own, ("sp", "tp"), halo_pairs(False))
     if following is not None:
         query, following = lax.optimization_barrier((query, following))
-        following = spread(following)
+        following = pltpu.with_memory_space_constraint(spread(following), pltpu.HBM)
     out = attend(last, query, a_in, a_own, b_own, b_in, table, x)
     return out, following
 
@@ -254,7 +275,7 @@
     held = pltpu.with_memory_space_constraint(held, pltpu.HBM)
     middle, second_set = layer(
         stream,
-        held,
+        (held,),
         0,
         SCALE_FIRST,
         held,
@@ -263,8 +284,10 @@
         second_blocks,
     )
     sent = (middle.astype(jnp.float32) * SCALE_SECOND).astype(jnp.float16)
-    again = lax.all_gather(sent, "tp", axis=0, tiled=False).astype(jnp.bfloat16)
-    again = pltpu.with_memory_space_constraint(again, pltpu.HBM)
+    again = lax.all_gather(sent, "tp", axis=0, tiled=False)
+    near = again[:NEAR_BLOCKS].astype(jnp.bfloat16)
+    far = again[NEAR_BLOCKS:].astype(jnp.bfloat16)
+    again = (near, pltpu.with_memory_space_constraint(far, pltpu.HBM))
     return layer(middle, again, 1, SCALE_SECOND, held, second_set, offset_second)[0]
 
 

time: 195 us -> 152 us (0.78); the launches traced: 192 us -> 151 us
  waiting for transfers between devices: 49 us -> 7.88 us
  local copies, waits for them, and re-layouts: 4.6 us -> 2.15 us
  Pallas kernels: 15.6 us -> 17.7 us
    ppermute x2, waiting for transfers between devices: 43.3 us -> 0.96 us  [layer(): a_in = lax.ppermute(a_own, ('sp', 'tp'), halo_pairs(True))]
    unnamed x26 -> x18, local copies, waits for them, and re-layouts: 2.5 us -> 0.05 us
where the time goes in v9:
time: 152 us; the launch traced here: 151 us
  blocking collectives  90.7 us (60%)
  starting transfers between devices  28.6 us (19%)
  Pallas kernels  17.7 us (12%)
  waiting for transfers between devices  7.88 us (5%)
  other arithmetic  4.17 us (3%)
  local copies, waits for them, and re-layouts  2.15 us (1%)
    all_gather x1, blocking collectives, body(): held = lax.all_gather(sent, 'tp', axis=0, tiled=False).astype(jnp.bfloat16)  47.7 us
    all_gather x1, blocking collectives, body(): again = lax.all_gather(sent, 'tp', axis=0, tiled=False)  43.1 us
    all_to_all x2, starting transfers between devices, spread(): lax.all_to_all(blocks, 'sp', 0, 0, tiled=True).reshape(-1, blocks.shape[2])  16.7 us
    pallas_call x2, Pallas kernels, project(): pl.pallas_call(functools.partial(project_kernel, gain_row, scale, near),...  11.4 us
    ppermute x2, starting transfers between devices, layer(): a_in = lax.ppermute(a_own, ('sp', 'tp'), halo_pairs(True))  7.42 us
    ppermute x2, waiting for transfers between devices, layer(): b_in = lax.ppermute(b_own, ('sp', 'tp'), halo_pairs(False))  6.07 us
    ppermute x2, starting transfers between devices, layer(): b_in = lax.ppermute(b_own, ('sp', 'tp'), halo_pairs(False))  4.39 us
    pallas_call x2, Pallas kernels, attend(): pl.pallas_call(functools.partial(attend_kernel, last), out_shape=jax.Shap...  3.5 us
  transfers between devices with their start and end apart: 6, of which 3 were waited for; matrix products, arithmetic and copies ran while one was open for 4% of the time, Pallas kernels for 1%

profile of v9, /device:TPU:6, one launch (start us, length us, event | category | flops | bytes accessed | tf_op | source)
XLA Modules:
  0.0 151.5 jit_solution(8319989646687383737)
XLA Ops:
  0.0 2.8 %copies.1 = bf16[16,256,384]{2,1,0:T(8,128)(2,1)} custom-call(bf16[256,128]{1,0:T(8,128)(2,1)} %first_ref.1, bf16[256,128]{1,0:T(8,128)(2,1)} %second_ref.1, bf16[256,128]{1,0:T(8,128)(2,1)} %third_ref.1), custom_call_target="tpu_custom_call" | custom-call | tf_op jit(solution)/shard_map/copies/pallas_call | solution.py:236
  2.8 0.0 copy-start.6
  2.8 0.0 copy-start.7
  2.9 0.0 copy-start
  2.9 0.0 copy-start.1
  2.9 0.0 copy-start.2
  2.9 0.0 copy-start.3
  2.9 9.5 %all-to-all-start = ((bf16[16,256,384]{2,1,0:T(8,128)(2,1)}), bf16[16,256,384]{2,1,0:T(8,128)(2,1)S(1)}, u32[]{:S(2)}, u32[]{:S(2)}) async-start(bf16[16,256,384]{2,1,0:T(8,128)(2,1)} %copies.1), calls=%async_computation | async-start | bytes 6291456 | tf_op jit(solution)/shard_map/all_to_all | solution.py:248
  12.4 0.0 copy-done.6
  12.4 0.0 copy-done.7
  12.4 0.0 copy-done
  12.5 0.0 copy-done.1
  12.5 0.0 copy-done.2
  12.5 0.0 copy-done.3
  12.6 2.1 %broadcast_in_dim.2 = bf16[16,256,384]{2,1,0:T(8,128)(2,1)} broadcast(bf16[256,384]{1,0:T(8,128)(2,1)S(1)} %pad_maximum_fusion), dimensions={1,2} | broadcast | bytes 3342336 | tf_op jit(solution)/shard_map/broadcast_in_dim | solution.py:269
  14.7 47.7 %all-gather.4 = f16[16640,128]{1,0:T(8,128)(2,1)S(1)} all-gather(f16[520,128]{1,0:T(8,128)(2,1)S(1)} %multiply_convert_fusion), channel_id=2, replica_groups=mesh['sp'=16,'tp'=32] {'tp'}, dimensions={0}, use_global_device_ids=true | all-gather | bytes 4392960 | tf_op jit(solution)/shard_map/all_gather | solution.py:274
  62.4 2.5 %convert_element_type.30 = bf16[16640,128]{1,0:T(8,128)(2,1)} convert(f16[16640,128]{1,0:T(8,128)(2,1)S(1)} %all-gather.4) | non-fusion elementwise | flops 2129920 | bytes 8519680 | tf_op jit(solution)/shard_map/convert_element_type | solution.py:274
  64.9 0.0 all-to-all-done
  64.9 0.0 copy-start.4
  64.9 5.7 %project.2 = (bf16[512,128]{1,0:T(8,128)(2,1)S(1)}, bf16[2,256,128]{2,1,0:T(8,128)(2,1)S(1)}, bf16[2,256,128]{2,1,0:T(8,128)(2,1)}) custom-call(bf16[32,520,128]{2,1,0:T(8,128)(2,1)} %bitcast.9, bf16[32,520,128]{2,1,0:T(8,128)(2,1)} %bitcast.10, bf16[4096,384]{1,0:T(8,128)(2,1)S(1)} %bitcast.7), custom_call_target="tpu_custom_call" | custom-call | flops 1610612736 | bytes 8388608 | tf_op jit(solution)/shard_map/project/pallas_call | solution.py:107
  70.6 3.4 %collective-permute-start = (bf16[2,256,128]{2,1,0:T(8,128)(2,1)S(1)}, bf16[2,256,128]{2,1,0:T(8,128)(2,1)S(1)}, u32[]{:S(2)}, u32[]{:S(2)}) collective-permute-start(bf16[2,256,128]{2,1,0:T(8,128)(2,1)S(1)} %get-tuple-element.27.a_own), channel_id=1, source_target_pairs={{0,32},{2,34},{4,36},{6,38},{8,40},{10,42},{12,44},{14,46},{16,48}... | collective-permute-start | bytes 393224 | tf_op jit(solution)/shard_map/ppermute | solution.py:213
  74.0 2.5 %collective-permute-start.1 = (bf16[2,256,128]{2,1,0:T(8,128)(2,1)}, bf16[2,256,128]{2,1,0:T(8,128)(2,1)S(1)}, u32[]{:S(2)}, u32[]{:S(2)}) collective-permute-start(bf16[2,256,128]{2,1,0:T(8,128)(2,1)} %get-tuple-element.28.b_own), channel_id=1, source_target_pairs={{1,33},{3,35},{5,37},{7,39},{9,41},{11,43},{13,45},{15,47},{17,49}... | collective-permute-start | bytes 393224 | tf_op jit(solution)/shard_map/ppermute | solution.py:214
  76.5 0.0 copy-done.4
  76.5 7.2 %all-to-all-start.1 = ((bf16[16,256,384]{2,1,0:T(8,128)(2,1)}), bf16[16,256,384]{2,1,0:T(8,128)(2,1)}, u32[]{:S(2)}, u32[]{:S(2)}) async-start(bf16[16,256,384]{2,1,0:T(8,128)(2,1)} %broadcast_in_dim.2), calls=%async_computation.1 | async-start | bytes 6291456 | tf_op jit(solution)/shard_map/all_to_all | solution.py:248
  83.7 0.0 collective-permute-done.a_in
  83.7 0.0 collective-permute-done.1.b_in
  83.7 1.9 %attend.2.x_ref = bf16[512,128]{1,0:T(8,128)(2,1)S(1)} custom-call(bf16[512,128]{1,0:T(8,128)(2,1)S(1)} %get-tuple-element.26.q_ref, bf16[2,256,128]{2,1,0:T(8,128)(2,1)S(1)} %collective-permute-done.a_in, bf16[2,256,128]{2,1,0:T(8,128)(2,1)S(1)} %get-tuple-element.27.a_own, bf16[2,256,128]{2,1,0:T(8,128)(2,1)} %get-tuple-element.28.b_own, ...), custom_call_target="tpu_custom_call" | custom-call | flops 134217728 | bytes 2097152 | tf_op jit(solution)/shard_map/attend/pallas_call | solution.py:180
  85.7 43.1 %all-gather.5 = f16[16384,128]{1,0:T(8,128)(2,1)S(1)} all-gather(f16[512,128]{1,0:T(8,128)(2,1)S(1)} %multiply_convert_fusion.1), channel_id=3, replica_groups=mesh['sp'=16,'tp'=32] {'tp'}, dimensions={0}, use_global_device_ids=true | all-gather | bytes 4325376 | tf_op jit(solution)/shard_map/all_gather | solution.py:287
  128.7 1.2 slice_convert_fusion.1
  129.9 0.3 slice_convert_fusion
  130.3 0.9 all-to-all-done.1
  131.1 0.0 copy-start.5
  131.1 5.7 %project.3 = (bf16[512,128]{1,0:T(8,128)(2,1)S(1)}, bf16[2,256,128]{2,1,0:T(8,128)(2,1)S(1)}, bf16[2,256,128]{2,1,0:T(8,128)(2,1)S(1)}) custom-call(bf16[22,512,128]{2,1,0:T(8,128)(2,1)S(1)} %bitcast.8, bf16[10,512,128]{2,1,0:T(8,128)(2,1)} %bitcast.12, bf16[32,520,128]{2,1,0:T(8,128)(2,1)} %bitcast.11, bf16[4096,384]{1,0:T(8,128)(2,1)} %bitcast.6.refs_3_), custom_call_target="tpu_custom_call" | custom-call | flops 1610612736 | bytes 8388608 | tf_op jit(solution)/shard_map/project/pallas_call | solution.py:107
  136.8 4.0 %collective-permute-start.2 = (bf16[2,256,128]{2,1,0:T(8,128)(2,1)S(1)}, bf16[2,256,128]{2,1,0:T(8,128)(2,1)S(1)}, u32[]{:S(2)}, u32[]{:S(2)}) collective-permute-start(bf16[2,256,128]{2,1,0:T(8,128)(2,1)S(1)} %get-tuple-element.31.a_own), channel_id=1, source_target_pairs={{0,32},{2,34},{4,36},{6,38},{8,40},{10,42},{12,44},{14,46},{16,48}... | collective-permute-start | bytes 393224 | tf_op jit(solution)/shard_map/ppermute | solution.py:213
  140.9 1.9 %collective-permute-start.3 = (bf16[2,256,128]{2,1,0:T(8,128)(2,1)S(1)}, bf16[2,256,128]{2,1,0:T(8,128)(2,1)S(1)}, u32[]{:S(2)}, u32[]{:S(2)}) collective-permute-start(bf16[2,256,128]{2,1,0:T(8,128)(2,1)S(1)} %get-tuple-element.32.b_own), channel_id=1, source_target_pairs={{1,33},{3,35},{5,37},{7,39},{9,41},{11,43},{13,45},{15,47},{17,49}... | collective-permute-start | bytes 393224 | tf_op jit(solution)/shard_map/ppermute | solution.py:214
  142.8 0.0 copy-done.5
  142.8 1.0 collective-permute-done.2.a_in
  143.8 6.1 %collective-permute-done.3.b_in = bf16[2,256,128]{2,1,0:T(8,128)(2,1)S(1)} collective-permute-done((bf16[2,256,128]{2,1,0:T(8,128)(2,1)S(1)}, bf16[2,256,128]{2,1,0:T(8,128)(2,1)S(1)}, u32[]{:S(2)}, u32[]{:S(2)}) %collective-permute-start.3) | collective-permute-done | bytes 131104 | tf_op jit(solution)/shard_map/ppermute | solution.py:214
  149.8 1.6 %attend.3 = bf16[512,128]{1,0:T(8,128)(2,1)} custom-call(bf16[512,128]{1,0:T(8,128)(2,1)S(1)} %get-tuple-element.30.q_ref, bf16[2,256,128]{2,1,0:T(8,128)(2,1)S(1)} %collective-permute-done.2.a_in, bf16[2,256,128]{2,1,0:T(8,128)(2,1)S(1)} %get-tuple-element.31.a_own, bf16[2,256,128]{2,1,0:T(8,128)(2,1)S(1)} %get-tuple-element.32.b_own, ...), custom_call_target="tpu_custom_call" | custom-call | flops 134217728 | bytes 2097152 | tf_op jit(solution)/shard_map/attend/pallas_call | solution.py:180
  (6 shorter events, 0.1 us)
Async XLA Ops:
  2.8 9.6 %copy-start.6 = (bf16[128]{0:T(256)(128)(2,1)S(1)}, bf16[128]{0:T(256)(128)(2,1)}, u32[]{:S(2)}) copy-start(bf16[128]{0:T(256)(128)(2,1)} %param.17) | copy-start | bytes 772
  2.8 9.6 %copy-start.7 = (bf16[128]{0:T(256)(128)(2,1)S(1)}, bf16[128]{0:T(256)(128)(2,1)}, u32[]{:S(2)}) copy-start(bf16[128]{0:T(256)(128)(2,1)} %param.12) | copy-start | bytes 772
  2.9 9.6 %copy-start = (bf16[512,128]{1,0:T(8,128)(2,1)S(1)}, bf16[512,128]{1,0:T(8,128)(2,1)}, u32[]{:S(2)}) copy-start(bf16[512,128]{1,0:T(8,128)(2,1)} %x_ref.1) | copy-start | bytes 393220
  2.9 9.6 %copy-start.1 = (bf16[256,128]{1,0:T(8,128)(2,1)S(1)}, bf16[256,128]{1,0:T(8,128)(2,1)}, u32[]{:S(2)}) copy-start(bf16[256,128]{1,0:T(8,128)(2,1)} %param.20) | copy-start | bytes 196612
  2.9 9.6 %copy-start.2 = (bf16[256,128]{1,0:T(8,128)(2,1)S(1)}, bf16[256,128]{1,0:T(8,128)(2,1)}, u32[]{:S(2)}) copy-start(bf16[256,128]{1,0:T(8,128)(2,1)} %param.19) | copy-start | bytes 196612
  2.9 9.6 %copy-start.3 = (bf16[256,128]{1,0:T(8,128)(2,1)S(1)}, bf16[256,128]{1,0:T(8,128)(2,1)}, u32[]{:S(2)}) copy-start(bf16[256,128]{1,0:T(8,128)(2,1)} %param.18) | copy-start | bytes 196612
  2.9 62.0 %all-to-all-start = ((bf16[16,256,384]{2,1,0:T(8,128)(2,1)}), bf16[16,256,384]{2,1,0:T(8,128)(2,1)S(1)}, u32[]{:S(2)}, u32[]{:S(2)}) async-start(bf16[16,256,384]{2,1,0:T(8,128)(2,1)} %copies.1), calls=%async_computation | async-start | bytes 6291456 | tf_op jit(solution)/shard_map/all_to_all | solution.py:248
  64.9 11.6 %copy-start.4 = (f32[1,15,31]{2,0,1:T(1,128)S(1)}, f32[1,15,31]{2,0,1:T(1,128)}, u32[]{:S(2)}) copy-start(f32[1,15,31]{2,0,1:T(1,128)} %param.16) | copy-start | bytes 5584
  70.6 13.1 %collective-permute-start = (bf16[2,256,128]{2,1,0:T(8,128)(2,1)S(1)}, bf16[2,256,128]{2,1,0:T(8,128)(2,1)S(1)}, u32[]{:S(2)}, u32[]{:S(2)}) collective-permute-start(bf16[2,256,128]{2,1,0:T(8,128)(2,1)S(1)} %get-tuple-element.27.a_own), channel_id=1, source_target_pairs={{0,32},{2,34},{4,36},{6,38},{8,40},{10,42},{12,44},{14,46},{16,48}... | collective-permute-start | bytes 393224 | tf_op jit(solution)/shard_map/ppermute | solution.py:213
  74.0 9.7 %collective-permute-start.1 = (bf16[2,256,128]{2,1,0:T(8,128)(2,1)}, bf16[2,256,128]{2,1,0:T(8,128)(2,1)S(1)}, u32[]{:S(2)}, u32[]{:S(2)}) collective-permute-start(bf16[2,256,128]{2,1,0:T(8,128)(2,1)} %get-tuple-element.28.b_own), channel_id=1, source_target_pairs={{1,33},{3,35},{5,37},{7,39},{9,41},{11,43},{13,45},{15,47},{17,49}... | collective-permute-start | bytes 393224 | tf_op jit(solution)/shard_map/ppermute | solution.py:214
  76.5 54.7 %all-to-all-start.1 = ((bf16[16,256,384]{2,1,0:T(8,128)(2,1)}), bf16[16,256,384]{2,1,0:T(8,128)(2,1)}, u32[]{:S(2)}, u32[]{:S(2)}) async-start(bf16[16,256,384]{2,1,0:T(8,128)(2,1)} %broadcast_in_dim.2), calls=%async_computation.1 | async-start | bytes 6291456 | tf_op jit(solution)/shard_map/all_to_all | solution.py:248
  131.1 11.7 %copy-start.5 = (f32[1,15,31]{2,0,1:T(1,128)S(1)}, f32[1,15,31]{2,0,1:T(1,128)}, u32[]{:S(2)}) copy-start(f32[1,15,31]{2,0,1:T(1,128)} %param.21) | copy-start | bytes 5584
  136.8 7.0 %collective-permute-start.2 = (bf16[2,256,128]{2,1,0:T(8,128)(2,1)S(1)}, bf16[2,256,128]{2,1,0:T(8,128)(2,1)S(1)}, u32[]{:S(2)}, u32[]{:S(2)}) collective-permute-start(bf16[2,256,128]{2,1,0:T(8,128)(2,1)S(1)} %get-tuple-element.31.a_own), channel_id=1, source_target_pairs={{0,32},{2,34},{4,36},{6,38},{8,40},{10,42},{12,44},{14,46},{16,48}... | collective-permute-start | bytes 393224 | tf_op jit(solution)/shard_map/ppermute | solution.py:213
  140.9 9.0 %collective-permute-start.3 = (bf16[2,256,128]{2,1,0:T(8,128)(2,1)S(1)}, bf16[2,256,128]{2,1,0:T(8,128)(2,1)S(1)}, u32[]{:S(2)}, u32[]{:S(2)}) collective-permute-start(bf16[2,256,128]{2,1,0:T(8,128)(2,1)S(1)} %get-tuple-element.32.b_own), channel_id=1, source_target_pairs={{1,33},{3,35},{5,37},{7,39},{9,41},{11,43},{13,45},{15,47},{17,49}... | collective-permute-start | bytes 393224 | tf_op jit(solution)/shard_map/ppermute | solution.py:214

commit v10 on v9

--- a/solution.py
+++ b/solution.py
@@ -18,6 +18,7 @@
 PROJECT_VMEM = 24 << 20
 COPIES_VMEM = 66_000_000
 NEAR_BLOCKS = 22
+GROUP = 10
 ATTEND_VMEM = 12 << 20
 
 
@@ -70,8 +71,9 @@
         weights.start()
     total = jnp.zeros((tokens, size), jnp.float32)
     for f in range(blocks):
-        if f >= near:
-            copies[f - near].wait()
+        if f >= near and (f - near) % GROUP == 0:
+            for copy in copies[f - near : f - near + GROUP]:
+                copy.wait()
         part = block_of(f).astype(jnp.float32)
         total = total + part * part
     mean = jnp.sum(total, axis=1, keepdims=True) * (1.0 / (blocks * size * scale * scale))

time: 152 us -> 152 us (level)
  no operation moved by 1% of the time
where the time goes in v10:
time: 152 us
  blocking collectives  90.7 us (60%)
  starting transfers between devices  28.6 us (19%)
  Pallas kernels  18.1 us (12%)
  waiting for transfers between devices  7.89 us (5%)
  other arithmetic  4.17 us (3%)
  local copies, waits for them, and re-layouts  2.15 us (1%)
    all_gather x1, blocking collectives, body(): held = lax.all_gather(sent, 'tp', axis=0, tiled=False).astype(jnp.bfloat16)  47.7 us
    all_gather x1, blocking collectives, body(): again = lax.all_gather(sent, 'tp', axis=0, tiled=False)  43.1 us
    all_to_all x2, starting transfers between devices, spread(): lax.all_to_all(blocks, 'sp', 0, 0, tiled=True).reshape(-1, blocks.shape[2])  16.7 us
    pallas_call x2, Pallas kernels, project(): pl.pallas_call(functools.partial(project_kernel, gain_row, scale, near),...  11.8 us
    ppermute x2, starting transfers between devices, layer(): a_in = lax.ppermute(a_own, ('sp', 'tp'), halo_pairs(True))  7.42 us
    ppermute x2, waiting for transfers between devices, layer(): b_in = lax.ppermute(b_own, ('sp', 'tp'), halo_pairs(False))  6.06 us
    ppermute x2, starting transfers between devices, layer(): b_in = lax.ppermute(b_own, ('sp', 'tp'), halo_pairs(False))  4.39 us
    pallas_call x2, Pallas kernels, attend(): pl.pallas_call(functools.partial(attend_kernel, last), out_shape=jax.Shap...  3.51 us
  transfers between devices with their start and end apart: 6, of which 3 were waited for; matrix products, arithmetic and copies ran while one was open for 4% of the time, Pallas kernels for 1%

profile of v10, /device:TPU:6, one launch (start us, length us, event | category | flops | bytes accessed | tf_op | source)
XLA Modules:
  0.0 151.9 jit_solution(17236651765203806937)
XLA Ops:
  0.0 2.8 %copies.1 = bf16[16,256,384]{2,1,0:T(8,128)(2,1)} custom-call(bf16[256,128]{1,0:T(8,128)(2,1)} %first_ref.1, bf16[256,128]{1,0:T(8,128)(2,1)} %second_ref.1, bf16[256,128]{1,0:T(8,128)(2,1)} %third_ref.1), custom_call_target="tpu_custom_call" | custom-call | tf_op jit(solution)/shard_map/copies/pallas_call | solution.py:238
  2.8 0.0 copy-start.6
  2.8 0.0 copy-start.7
  2.9 0.0 copy-start
  2.9 0.0 copy-start.1
  2.9 0.0 copy-start.2
  2.9 0.0 copy-start.3
  2.9 9.5 %all-to-all-start = ((bf16[16,256,384]{2,1,0:T(8,128)(2,1)}), bf16[16,256,384]{2,1,0:T(8,128)(2,1)S(1)}, u32[]{:S(2)}, u32[]{:S(2)}) async-start(bf16[16,256,384]{2,1,0:T(8,128)(2,1)} %copies.1), calls=%async_computation | async-start | bytes 6291456 | tf_op jit(solution)/shard_map/all_to_all | solution.py:250
  12.4 0.0 copy-done.6
  12.4 0.0 copy-done.7
  12.4 0.0 copy-done
  12.5 0.0 copy-done.1
  12.5 0.0 copy-done.2
  12.5 0.0 copy-done.3
  12.6 2.1 %broadcast_in_dim.2 = bf16[16,256,384]{2,1,0:T(8,128)(2,1)} broadcast(bf16[256,384]{1,0:T(8,128)(2,1)S(1)} %pad_maximum_fusion), dimensions={1,2} | broadcast | bytes 3342336 | tf_op jit(solution)/shard_map/broadcast_in_dim | solution.py:271
  14.7 47.7 %all-gather.4 = f16[16640,128]{1,0:T(8,128)(2,1)S(1)} all-gather(f16[520,128]{1,0:T(8,128)(2,1)S(1)} %multiply_convert_fusion), channel_id=2, replica_groups=mesh['sp'=16,'tp'=32] {'tp'}, dimensions={0}, use_global_device_ids=true | all-gather | bytes 4392960 | tf_op jit(solution)/shard_map/all_gather | solution.py:276
  62.4 2.5 %convert_element_type.30 = bf16[16640,128]{1,0:T(8,128)(2,1)} convert(f16[16640,128]{1,0:T(8,128)(2,1)S(1)} %all-gather.4) | non-fusion elementwise | flops 2129920 | bytes 8519680 | tf_op jit(solution)/shard_map/convert_element_type | solution.py:276
  64.9 0.0 all-to-all-done
  64.9 0.0 copy-start.4
  64.9 6.0 %project.2 = (bf16[512,128]{1,0:T(8,128)(2,1)S(1)}, bf16[2,256,128]{2,1,0:T(8,128)(2,1)S(1)}, bf16[2,256,128]{2,1,0:T(8,128)(2,1)}) custom-call(bf16[32,520,128]{2,1,0:T(8,128)(2,1)} %bitcast.9, bf16[32,520,128]{2,1,0:T(8,128)(2,1)} %bitcast.10, bf16[4096,384]{1,0:T(8,128)(2,1)S(1)} %bitcast.7), custom_call_target="tpu_custom_call" | custom-call | flops 1610612736 | bytes 8388608 | tf_op jit(solution)/shard_map/project/pallas_call | solution.py:109
  70.8 3.4 %collective-permute-start = (bf16[2,256,128]{2,1,0:T(8,128)(2,1)S(1)}, bf16[2,256,128]{2,1,0:T(8,128)(2,1)S(1)}, u32[]{:S(2)}, u32[]{:S(2)}) collective-permute-start(bf16[2,256,128]{2,1,0:T(8,128)(2,1)S(1)} %get-tuple-element.27.a_own), channel_id=1, source_target_pairs={{0,32},{2,34},{4,36},{6,38},{8,40},{10,42},{12,44},{14,46},{16,48}... | collective-permute-start | bytes 393224 | tf_op jit(solution)/shard_map/ppermute | solution.py:215
  74.2 2.5 %collective-permute-start.1 = (bf16[2,256,128]{2,1,0:T(8,128)(2,1)}, bf16[2,256,128]{2,1,0:T(8,128)(2,1)S(1)}, u32[]{:S(2)}, u32[]{:S(2)}) collective-permute-start(bf16[2,256,128]{2,1,0:T(8,128)(2,1)} %get-tuple-element.28.b_own), channel_id=1, source_target_pairs={{1,33},{3,35},{5,37},{7,39},{9,41},{11,43},{13,45},{15,47},{17,49}... | collective-permute-start | bytes 393224 | tf_op jit(solution)/shard_map/ppermute | solution.py:216
  76.7 0.0 copy-done.4
  76.7 7.2 %all-to-all-start.1 = ((bf16[16,256,384]{2,1,0:T(8,128)(2,1)}), bf16[16,256,384]{2,1,0:T(8,128)(2,1)}, u32[]{:S(2)}, u32[]{:S(2)}) async-start(bf16[16,256,384]{2,1,0:T(8,128)(2,1)} %broadcast_in_dim.2), calls=%async_computation.1 | async-start | bytes 6291456 | tf_op jit(solution)/shard_map/all_to_all | solution.py:250
  83.9 0.0 collective-permute-done.a_in
  84.0 0.0 collective-permute-done.1.b_in
  84.0 1.9 %attend.2.x_ref = bf16[512,128]{1,0:T(8,128)(2,1)S(1)} custom-call(bf16[512,128]{1,0:T(8,128)(2,1)S(1)} %get-tuple-element.26.q_ref, bf16[2,256,128]{2,1,0:T(8,128)(2,1)S(1)} %collective-permute-done.a_in, bf16[2,256,128]{2,1,0:T(8,128)(2,1)S(1)} %get-tuple-element.27.a_own, bf16[2,256,128]{2,1,0:T(8,128)(2,1)} %get-tuple-element.28.b_own, ...), custom_call_target="tpu_custom_call" | custom-call | flops 134217728 | bytes 2097152 | tf_op jit(solution)/shard_map/attend/pallas_call | solution.py:182
  85.9 43.1 %all-gather.5 = f16[16384,128]{1,0:T(8,128)(2,1)S(1)} all-gather(f16[512,128]{1,0:T(8,128)(2,1)S(1)} %multiply_convert_fusion.1), channel_id=3, replica_groups=mesh['sp'=16,'tp'=32] {'tp'}, dimensions={0}, use_global_device_ids=true | all-gather | bytes 4325376 | tf_op jit(solution)/shard_map/all_gather | solution.py:289
  129.0 1.2 slice_convert_fusion.1
  130.2 0.3 slice_convert_fusion
  130.5 0.9 all-to-all-done.1
  131.4 0.0 copy-start.5
  131.4 5.8 %project.3 = (bf16[512,128]{1,0:T(8,128)(2,1)S(1)}, bf16[2,256,128]{2,1,0:T(8,128)(2,1)S(1)}, bf16[2,256,128]{2,1,0:T(8,128)(2,1)S(1)}) custom-call(bf16[22,512,128]{2,1,0:T(8,128)(2,1)S(1)} %bitcast.8, bf16[10,512,128]{2,1,0:T(8,128)(2,1)} %bitcast.12, bf16[32,520,128]{2,1,0:T(8,128)(2,1)} %bitcast.11, bf16[4096,384]{1,0:T(8,128)(2,1)} %bitcast.6.refs_3_), custom_call_target="tpu_custom_call" | custom-call | flops 1610612736 | bytes 8388608 | tf_op jit(solution)/shard_map/project/pallas_call | solution.py:109
  137.2 4.0 %collective-permute-start.2 = (bf16[2,256,128]{2,1,0:T(8,128)(2,1)S(1)}, bf16[2,256,128]{2,1,0:T(8,128)(2,1)S(1)}, u32[]{:S(2)}, u32[]{:S(2)}) collective-permute-start(bf16[2,256,128]{2,1,0:T(8,128)(2,1)S(1)} %get-tuple-element.31.a_own), channel_id=1, source_target_pairs={{0,32},{2,34},{4,36},{6,38},{8,40},{10,42},{12,44},{14,46},{16,48}... | collective-permute-start | bytes 393224 | tf_op jit(solution)/shard_map/ppermute | solution.py:215
  141.3 1.9 %collective-permute-start.3 = (bf16[2,256,128]{2,1,0:T(8,128)(2,1)S(1)}, bf16[2,256,128]{2,1,0:T(8,128)(2,1)S(1)}, u32[]{:S(2)}, u32[]{:S(2)}) collective-permute-start(bf16[2,256,128]{2,1,0:T(8,128)(2,1)S(1)} %get-tuple-element.32.b_own), channel_id=1, source_target_pairs={{1,33},{3,35},{5,37},{7,39},{9,41},{11,43},{13,45},{15,47},{17,49}... | collective-permute-start | bytes 393224 | tf_op jit(solution)/shard_map/ppermute | solution.py:216
  143.2 0.0 copy-done.5
  143.2 1.0 collective-permute-done.2.a_in
  144.2 6.1 %collective-permute-done.3.b_in = bf16[2,256,128]{2,1,0:T(8,128)(2,1)S(1)} collective-permute-done((bf16[2,256,128]{2,1,0:T(8,128)(2,1)S(1)}, bf16[2,256,128]{2,1,0:T(8,128)(2,1)S(1)}, u32[]{:S(2)}, u32[]{:S(2)}) %collective-permute-start.3) | collective-permute-done | bytes 131104 | tf_op jit(solution)/shard_map/ppermute | solution.py:216
  150.2 1.6 %attend.3 = bf16[512,128]{1,0:T(8,128)(2,1)} custom-call(bf16[512,128]{1,0:T(8,128)(2,1)S(1)} %get-tuple-element.30.q_ref, bf16[2,256,128]{2,1,0:T(8,128)(2,1)S(1)} %collective-permute-done.2.a_in, bf16[2,256,128]{2,1,0:T(8,128)(2,1)S(1)} %get-tuple-element.31.a_own, bf16[2,256,128]{2,1,0:T(8,128)(2,1)S(1)} %get-tuple-element.32.b_own, ...), custom_call_target="tpu_custom_call" | custom-call | flops 134217728 | bytes 2097152 | tf_op jit(solution)/shard_map/attend/pallas_call | solution.py:182
  (6 shorter events, 0.1 us)
Async XLA Ops:
  2.8 9.6 %copy-start.6 = (bf16[128]{0:T(256)(128)(2,1)S(1)}, bf16[128]{0:T(256)(128)(2,1)}, u32[]{:S(2)}) copy-start(bf16[128]{0:T(256)(128)(2,1)} %param.17) | copy-start | bytes 772
  2.8 9.6 %copy-start.7 = (bf16[128]{0:T(256)(128)(2,1)S(1)}, bf16[128]{0:T(256)(128)(2,1)}, u32[]{:S(2)}) copy-start(bf16[128]{0:T(256)(128)(2,1)} %param.12) | copy-start | bytes 772
  2.9 9.6 %copy-start = (bf16[512,128]{1,0:T(8,128)(2,1)S(1)}, bf16[512,128]{1,0:T(8,128)(2,1)}, u32[]{:S(2)}) copy-start(bf16[512,128]{1,0:T(8,128)(2,1)} %x_ref.1) | copy-start | bytes 393220
  2.9 9.6 %copy-start.1 = (bf16[256,128]{1,0:T(8,128)(2,1)S(1)}, bf16[256,128]{1,0:T(8,128)(2,1)}, u32[]{:S(2)}) copy-start(bf16[256,128]{1,0:T(8,128)(2,1)} %param.20) | copy-start | bytes 196612
  2.9 9.6 %copy-start.2 = (bf16[256,128]{1,0:T(8,128)(2,1)S(1)}, bf16[256,128]{1,0:T(8,128)(2,1)}, u32[]{:S(2)}) copy-start(bf16[256,128]{1,0:T(8,128)(2,1)} %param.19) | copy-start | bytes 196612
  2.9 9.6 %copy-start.3 = (bf16[256,128]{1,0:T(8,128)(2,1)S(1)}, bf16[256,128]{1,0:T(8,128)(2,1)}, u32[]{:S(2)}) copy-start(bf16[256,128]{1,0:T(8,128)(2,1)} %param.18) | copy-start | bytes 196612
  2.9 62.0 %all-to-all-start = ((bf16[16,256,384]{2,1,0:T(8,128)(2,1)}), bf16[16,256,384]{2,1,0:T(8,128)(2,1)S(1)}, u32[]{:S(2)}, u32[]{:S(2)}) async-start(bf16[16,256,384]{2,1,0:T(8,128)(2,1)} %copies.1), calls=%async_computation | async-start | bytes 6291456 | tf_op jit(solution)/shard_map/all_to_all | solution.py:250
  64.9 11.8 %copy-start.4 = (f32[1,15,31]{2,0,1:T(1,128)S(1)}, f32[1,15,31]{2,0,1:T(1,128)}, u32[]{:S(2)}) copy-start(f32[1,15,31]{2,0,1:T(1,128)} %param.16) | copy-start | bytes 5584
  70.8 13.1 %collective-permute-start = (bf16[2,256,128]{2,1,0:T(8,128)(2,1)S(1)}, bf16[2,256,128]{2,1,0:T(8,128)(2,1)S(1)}, u32[]{:S(2)}, u32[]{:S(2)}) collective-permute-start(bf16[2,256,128]{2,1,0:T(8,128)(2,1)S(1)} %get-tuple-element.27.a_own), channel_id=1, source_target_pairs={{0,32},{2,34},{4,36},{6,38},{8,40},{10,42},{12,44},{14,46},{16,48}... | collective-permute-start | bytes 393224 | tf_op jit(solution)/shard_map/ppermute | solution.py:215
  74.2 9.7 %collective-permute-start.1 = (bf16[2,256,128]{2,1,0:T(8,128)(2,1)}, bf16[2,256,128]{2,1,0:T(8,128)(2,1)S(1)}, u32[]{:S(2)}, u32[]{:S(2)}) collective-permute-start(bf16[2,256,128]{2,1,0:T(8,128)(2,1)} %get-tuple-element.28.b_own), channel_id=1, source_target_pairs={{1,33},{3,35},{5,37},{7,39},{9,41},{11,43},{13,45},{15,47},{17,49}... | collective-permute-start | bytes 393224 | tf_op jit(solution)/shard_map/ppermute | solution.py:216
  76.7 54.7 %all-to-all-start.1 = ((bf16[16,256,384]{2,1,0:T(8,128)(2,1)}), bf16[16,256,384]{2,1,0:T(8,128)(2,1)}, u32[]{:S(2)}, u32[]{:S(2)}) async-start(bf16[16,256,384]{2,1,0:T(8,128)(2,1)} %broadcast_in_dim.2), calls=%async_computation.1 | async-start | bytes 6291456 | tf_op jit(solution)/shard_map/all_to_all | solution.py:250
  131.4 11.8 %copy-start.5 = (f32[1,15,31]{2,0,1:T(1,128)S(1)}, f32[1,15,31]{2,0,1:T(1,128)}, u32[]{:S(2)}) copy-start(f32[1,15,31]{2,0,1:T(1,128)} %param.21) | copy-start | bytes 5584
  137.2 7.0 %collective-permute-start.2 = (bf16[2,256,128]{2,1,0:T(8,128)(2,1)S(1)}, bf16[2,256,128]{2,1,0:T(8,128)(2,1)S(1)}, u32[]{:S(2)}, u32[]{:S(2)}) collective-permute-start(bf16[2,256,128]{2,1,0:T(8,128)(2,1)S(1)} %get-tuple-element.31.a_own), channel_id=1, source_target_pairs={{0,32},{2,34},{4,36},{6,38},{8,40},{10,42},{12,44},{14,46},{16,48}... | collective-permute-start | bytes 393224 | tf_op jit(solution)/shard_map/ppermute | solution.py:215
  141.3 9.0 %collective-permute-start.3 = (bf16[2,256,128]{2,1,0:T(8,128)(2,1)S(1)}, bf16[2,256,128]{2,1,0:T(8,128)(2,1)S(1)}, u32[]{:S(2)}, u32[]{:S(2)}) collective-permute-start(bf16[2,256,128]{2,1,0:T(8,128)(2,1)S(1)} %get-tuple-element.32.b_own), channel_id=1, source_target_pairs={{1,33},{3,35},{5,37},{7,39},{9,41},{11,43},{13,45},{15,47},{17,49}... | collective-permute-start | bytes 393224 | tf_op jit(solution)/shard_map/ppermute | solution.py:216
